TPU v7x, 512 devices: a whole 4x8x8 slice. The times are simulated.
512 devices in a mesh: sp: 64 (over z, y), tp: 8 (over x, core).
Axes of the slice: x: 4, y: 8, z: 8, core: 2. Of those that a mesh axis runs over, the one named last changes fastest.
Arguments:
- tokens: bfloat16 [12288, 4096], P('sp'), may hold values from -6 to 6
- norm_gain: float32 [4096], replicated, may hold values from 0.1 to 1.9
- conv_value: bfloat16 [4096, 2048], P('sp', 'tp'), may hold values from -0.09375 to 0.09375
- conv_gate: bfloat16 [4096, 2048], P('sp', 'tp'), may hold values from -0.09375 to 0.09375
- state_feed: bfloat16 [4096, 2048], P('sp', 'tp'), may hold values from -0.09375 to 0.09375
- conv_taps: float32 [31, 2048], P(None, 'tp'), may hold values from -1 to 1
- chan_gain: float32 [2048], replicated, may hold values from 0.1 to 1.9
- chan_shift: float32 [2048], replicated, may hold values from -3 to 3
- conv_project: bfloat16 [2048, 4096], P('sp', 'tp'), may hold values from -0.125 to 0.125
- decay_rate: float32 [128, 64], P('tp'), may hold values from 0.1 to 3
- frequency: float32 [128, 64], P('tp'), may hold values from 0.1 to 3
- input_real: float32 [128, 64, 16], P('tp'), may hold values from -0.01953125 to 0.01953125
- input_imag: float32 [128, 64, 16], P('tp'), may hold values from -0.01953125 to 0.01953125
- output_real: float32 [128, 16, 64], P('tp'), may hold values from -0.5 to 0.5
- output_imag: float32 [128, 16, 64], P('tp'), may hold values from -0.5 to 0.5
- skip_gain: float32 [2048], P('tp'), may hold values from -3 to 3
- state_value: bfloat16 [2048, 4096], P('sp', 'tp'), may hold values from -0.125 to 0.125
- state_gate: bfloat16 [2048, 4096], P('sp', 'tp'), may hold values from -0.125 to 0.125
- initial_state: float32 [2, 128, 64], P(None, 'tp'), may hold values from -5 to 5
Outputs:
- mixer_out: bfloat16 [12288, 4096], P('sp', 'tp')
- final_state: float32 [2, 128, 64], P(None, 'tp')
All inputs are finite; a program needn't handle non-finite values.
Results may differ from a plain program's by a relative error of at most 0.0085.
Values may be sent and summed in bfloat16 or wider, within the bound.
No kernel may reach another device: no remote copies, remote signals or barrier semaphores. Data moves between devices by JAX's collectives and lax.ppermute only.
A program may use at most 64 MiB of HBM per device.

v0:
```python
import jax
import jax.numpy as jnp
from jax import lax
from jax.sharding import PartitionSpec as P


def passed_along(value, axis, steps):
    count = lax.axis_size(axis)
    leading, last = (max(0, -steps), min(count, count - steps))
    return lax.ppermute(value, axis, [(source, source + steps) for source in range(leading, last)])


def laid_out(pieces, dim):
    pieces = jnp.moveaxis(pieces, 0, dim)
    dims = pieces.shape
    return pieces.reshape(*dims[:dim], dims[dim] * dims[dim + 1], *dims[dim + 2 :])


def copy_for_each(shard, axis):
    length = lax.axis_size(axis)
    return lax.all_to_all(
        jnp.broadcast_to(shard[None], (length, *shard.shape)), axis, 0, 0, tiled=True
    )


def gathered_copies(shard, axis, dim):
    return laid_out(copy_for_each(shard, axis), dim)


def sent_together(arrays, axis, dim, along):
    ends, at = ([], 0)
    for a in arrays[:-1]:
        at += a.shape[along]
        ends.append(at)
    both = jnp.concatenate(arrays, axis=along)
    return tuple(jnp.split(gathered_copies(both, axis, dim), ends, axis=along))


def rotate(first_real, first_imag, second_real, second_imag):
    return (
        first_real * second_real - first_imag * second_imag,
        first_real * second_imag + first_imag * second_real,
    )


def power_table(base_real, base_imag, exponent, largest):
    result_real = jnp.ones((exponent.shape[0], base_real.shape[0]), jnp.float32)
    result_imag = jnp.zeros((exponent.shape[0], base_real.shape[0]), jnp.float32)
    square_real, square_imag = (base_real, base_imag)
    for place in range(max(largest, 1).bit_length()):
        chosen = (exponent >> place & 1 == 1)[:, None]
        next_real, next_imag = rotate(result_real, result_imag, square_real, square_imag)
        result_real = jnp.where(chosen, next_real, result_real)
        result_imag = jnp.where(chosen, next_imag, result_imag)
        square_real, square_imag = rotate(square_real, square_imag, square_real, square_imag)
    return (result_real, result_imag)


def local(
    tokens,
    norm_gain,
    conv_value,
    conv_gate,
    state_feed,
    conv_taps,
    chan_gain,
    chan_shift,
    conv_project,
    decay_rate,
    frequency,
    input_real,
    input_imag,
    output_real,
    output_imag,
    skip_gain,
    state_value,
    state_gate,
    initial_state,
):
    floats = tokens.astype(jnp.float32)
    normed = (
        floats * lax.rsqrt(jnp.mean(floats * floats, axis=1, keepdims=True) + 1e-06) * norm_gain
    ).astype(jnp.bfloat16)
    length = tokens.shape[0]
    width = conv_value.shape[1]
    in_block = jnp.concatenate([conv_value, conv_gate, state_feed], axis=1)
    projected = jnp.dot(
        normed,
        lax.all_gather(in_block, "sp", axis=0, tiled=True),
        preferred_element_type=jnp.float32,
    )
    gated_linear = (projected[:, :width] * jax.nn.sigmoid(projected[:, width : 2 * width])).astype(
        jnp.bfloat16
    )
    state_drive = projected[:, 2 * width :].astype(jnp.bfloat16)
    kernel = conv_taps.shape[0]
    before = passed_along(gated_linear[length - (kernel - 1) :], "sp", 1)
    padded = jnp.concatenate([before, gated_linear], axis=0).astype(jnp.float32)
    conv_sum = jnp.zeros((length, width), jnp.float32)
    for offset in range(kernel):
        conv_sum = conv_sum + conv_taps[offset] * padded[offset : offset + length]
    conv_out = conv_sum.astype(jnp.bfloat16)
    seq_devices = lax.axis_size("sp")
    total_tokens = length * seq_devices
    groups, state_size, group_size = input_real.shape
    flat = groups * state_size
    rate_real = -decay_rate / total_tokens
    magnitude = jnp.exp(rate_real)
    step_real = magnitude * jnp.cos(frequency)
    step_imag = magnitude * jnp.sin(frequency)
    modulus = rate_real * rate_real + frequency * frequency
    lift_real = step_real - 1.0
    factor_real = (lift_real * rate_real + step_imag * frequency) / modulus
    factor_imag = (step_imag * rate_real - lift_real * frequency) / modulus
    drive_real = factor_real[..., None] * input_real - factor_imag[..., None] * input_imag
    drive_imag = factor_real[..., None] * input_imag + factor_imag[..., None] * input_real
    grouped = state_drive.astype(jnp.float32).reshape(length, groups, group_size)
    pushed_real = jnp.einsum("gph,tgh->tgp", drive_real, grouped).reshape(length, flat)
    pushed_imag = jnp.einsum("gph,tgh->tgp", drive_imag, grouped).reshape(length, flat)
    base_real = step_real.reshape(flat)
    base_imag = step_imag.reshape(flat)
    square_size = base_real * base_real + base_imag * base_imag
    back_real = base_real / square_size
    back_imag = -base_imag / square_size
    positions = lax.iota(jnp.int32, length)
    counted = positions + 1
    power_real, power_imag = power_table(base_real, base_imag, counted, length)
    undo_real, undo_imag = power_table(back_real, back_imag, counted, length)
    scaled_real, scaled_imag = rotate(undo_real, undo_imag, pushed_real, pushed_imag)
    lower = (positions[:, None] >= positions[None, :]).astype(jnp.float32)
    summed_real = jnp.dot(lower, scaled_real)
    summed_imag = jnp.dot(lower, scaled_imag)
    local_real, local_imag = rotate(power_real, power_imag, summed_real, summed_imag)
    span_real, span_imag = (power_real[-1], power_imag[-1])
    last_real, last_imag = (local_real[-1], local_imag[-1])
    start_real = initial_state[0].reshape(flat)
    start_imag = initial_state[1].reshape(flat)
    finals = gathered_copies(jnp.stack([last_real, last_imag])[None], "sp", 0)
    position = lax.axis_index("sp")
    device_ids = lax.iota(jnp.int32, seq_devices)
    lag = jnp.maximum(position - 1 - device_ids, 0)
    weight_real, weight_imag = power_table(span_real, span_imag, lag, seq_devices)
    before_mask = (device_ids < position).astype(jnp.float32)[:, None]
    moved_real, moved_imag = rotate(weight_real, weight_imag, finals[:, 0], finals[:, 1])
    lead_real, lead_imag = power_table(
        span_real, span_imag, jnp.stack([position, jnp.int32(seq_devices)]), seq_devices
    )
    opening_real, opening_imag = rotate(lead_real[0], lead_imag[0], start_real, start_imag)
    entry_real = opening_real + jnp.sum(moved_real * before_mask, axis=0)
    entry_imag = opening_imag + jnp.sum(moved_imag * before_mask, axis=0)
    tail_real, tail_imag = power_table(
        span_real, span_imag, seq_devices - 1 - device_ids, seq_devices
    )
    carried_real, carried_imag = rotate(tail_real, tail_imag, finals[:, 0], finals[:, 1])
    closing_real, closing_imag = rotate(lead_real[1], lead_imag[1], start_real, start_imag)
    final_real = closing_real + jnp.sum(carried_real, axis=0)
    final_imag = closing_imag + jnp.sum(carried_imag, axis=0)
    final_state = jnp.stack([final_real, final_imag]).reshape(2, groups, state_size)
    state_real = (power_real * entry_real - power_imag * entry_imag + local_real).reshape(
        length, groups, state_size
    )
    state_imag = (power_real * entry_imag + power_imag * entry_real + local_imag).reshape(
        length, groups, state_size
    )
    response = jnp.einsum("ghp,tgp->tgh", output_real, state_real) - jnp.einsum(
        "ghp,tgp->tgh", output_imag, state_imag
    )
    response = response.reshape(length, groups * group_size) + skip_gain * state_drive.astype(
        jnp.float32
    )
    activated = jax.nn.gelu(response).astype(jnp.bfloat16)
    conv_rows, activated_rows = sent_together((conv_out, activated), "tp", 1, 0)
    conv_full = conv_rows.astype(jnp.float32)
    row_mean = jnp.mean(conv_full, axis=1, keepdims=True)
    centred = conv_full - row_mean
    variance = jnp.mean(centred * centred, axis=1, keepdims=True)
    conv_act = jax.nn.silu(centred * lax.rsqrt(variance + 1e-05) * chan_gain + chan_shift).astype(
        jnp.bfloat16
    )
    columns = conv_project.shape[1]
    out_block = jnp.concatenate([conv_project, state_value, state_gate], axis=1)
    piece = lax.all_gather(out_block, "sp", axis=0, tiled=True)
    conv_branch = jnp.dot(conv_act, piece[:, :columns], preferred_element_type=jnp.float32)
    state_both = jnp.dot(activated_rows, piece[:, columns:], preferred_element_type=jnp.float32)
    mixer_out = (
        conv_branch + state_both[:, :columns] * jax.nn.sigmoid(state_both[:, columns:])
    ).astype(jnp.bfloat16)
    return (mixer_out, final_state)


def solution(mesh):
    in_specs = (
        P("sp", None),
        P(),
        P("sp", "tp"),
        P("sp", "tp"),
        P("sp", "tp"),
        P(None, "tp"),
        P(),
        P(),
        P("sp", "tp"),
        P("tp", None),
        P("tp", None),
        P("tp", None, None),
        P("tp", None, None),
        P("tp", None, None),
        P("tp", None, None),
        P("tp"),
        P("sp", "tp"),
        P("sp", "tp"),
        P(None, "tp", None),
    )
    out_specs = (P("sp", "tp"), P(None, "tp", None))
    return jax.shard_map(local, mesh=mesh, in_specs=in_specs, out_specs=out_specs, check_vma=False)
```

profile of v0, /device:TPU:1, one launch (start us, length us, event | category | flops | bytes accessed | tf_op | source)
XLA Modules:
  0.0 217.5 jit_solution(8492768212598717211)
XLA Ops:
  7.2 1.6 pad_maximum_fusion.1
  8.9 1.4 pad_maximum_fusion.2
  12.8 3.0 %add_select_fusion.5 = f32[192,1024]{1,0:T(8,128)S(1)} fusion(f32[1024]{0:T(1024)S(1)} %get-tuple-element.130, f32[1024]{0:T(1024)S(1)} %get-tuple-element.129, pred[192]{0:T(512)(128)(4,1)S(1)} %get-tuple-element.142, f32[1024]{0:T(1024)S(1)} %get-tuple-element.132, f32[1024]{0:T(1024)S(1)} %get-tuple-element.131, f32[1024]{0:T(1024)S(1)} %get-tuple-element.133, ...), kind=kLoop, calls=%fused_computation.81 | loop fusion | flops 10616832 | bytes 853504 | tf_op jit(solution)/shard_map/jit(_where)/select_n | solution.py:54
  15.8 3.0 %subtract_select_fusion.5 = f32[192,1024]{1,0:T(8,128)S(1)} fusion(f32[1024]{0:T(1024)S(1)} %get-tuple-element.130, f32[1024]{0:T(1024)S(1)} %get-tuple-element.129, pred[192]{0:T(512)(128)(4,1)S(1)} %get-tuple-element.142, f32[1024]{0:T(1024)S(1)} %get-tuple-element.132, f32[1024]{0:T(1024)S(1)} %get-tuple-element.131, f32[1024]{0:T(1024)S(1)} %get-tuple-element.133, ...), kind=kLoop, calls=%fused_computation.82 | loop fusion | flops 10616832 | bytes 853504 | tf_op jit(solution)/shard_map/jit(_where)/select_n | solution.py:53
  27.9 78.0 %all-gather.3.cloned.1.call-done = bf16[4096,768]{1,0:T(8,128)(2,1)} async-done(((bf16[64,768]{1,0:T(8,128)(2,1)}), bf16[4096,768]{1,0:T(8,128)(2,1)}) %all-gather.3.cloned.1.call-update) | async-done | bytes 6291472 | tf_op jit(solution)/shard_map/all_gather | solution.py:89
  105.9 4.2 %fusion.9 = f32[192,768]{1,0:T(8,128)S(1)} fusion(bf16[4096,768]{1,0:T(8,128)(2,1)} %all-gather.3.cloned.1.call-done, bf16[192,4096]{1,0:T(8,128)(2,1)S(1)} %copy-done.1, f32[4096]{0:T(1024)S(1)} %copy-done.140, f32[192]{0:T(256)S(1)} %add_rsqrt_fusion.1), kind=kOutput, calls=%fused_computation.14 | convolution fusion | flops 1211105280 | bytes 8471296 | tf_op jit(solution)/shard_map/dot_general | solution.py:87
  113.8 2.7 %fusion.48 = f32[192,1024]{1,0:T(8,128)S(1)} fusion(f32[192,1024]{1,0:T(8,128)S(1)} %copy.40, f32[192,1024]{1,0:T(8,128)S(1)} %copy.39, f32[1024]{0:T(1024)} %get-tuple-element.115, f32[1024]{0:T(1024)} %get-tuple-element.114, pred[192]{0:T(512)(128)(4,1)S(1)} %copy-done.99, f32[1024]{0:T(1024)} %get-tuple-element.117, f32[1024]{0:T(1024)} %get-tuple-element.116, ...), kind=kOutput, calls=%fused_computation.67 | convolution fusion | flops 87527424 | bytes 2426368 | tf_op jit(solution)/shard_map/dot_general | solution.py:131
  116.8 4.6 %multiply_subtract_fusion = (f32[192,1024]{1,0:T(8,128)S(1)}, f32[192,1024]{1,0:T(8,128)S(1)}) fusion(f32[192,1024]{1,0:T(8,128)S(1)} %fusion.48, f32[1024]{0:T(1024)S(1)} %copy-done.33, f32[1024]{0:T(1024)S(1)} %copy-done.31, f32[1024]{0:T(1024)S(1)} %copy-done.37, f32[1024]{0:T(1024)S(1)} %copy-done.35, f32[1024]{0:T(1024)S(1)} %copy-done.39, ...), kind=kOutput, calls=%fused_computation.62 | convolution fusion | flops 99520512 | bytes 4064768 | tf_op jit(solution)/shard_map/dot_general | solution.py:132
  121.4 6.8 %multiply_add_fusion = f32[192,1024]{1,0:T(8,128)S(1)} fusion(f32[192,1024]{1,0:T(8,128)S(1)} %fusion.48, f32[192,1024]{1,0:T(8,128)S(1)} %get-tuple-element.126, f32[1024]{0:T(1024)S(1)} %copy-done.33, f32[1024]{0:T(1024)S(1)} %copy-done.31, f32[1024]{0:T(1024)S(1)} %copy-done.37, f32[1024]{0:T(1024)S(1)} %copy-done.35, f32[1024]{0:T(1024)S(1)} %copy-done.39, ...), kind=kLoop, calls=%fused_computation.61 | loop fusion | flops 11993088 | bytes 2426368 | tf_op jit(solution)/shard_map/add | solution.py:42
  129.4 9.2 %all-to-all-start = ((f32[64,1,2,1024]{3,2,1,0:T(2,128)}), f32[64,1,2,1024]{3,2,1,0:T(2,128)S(1)}, u32[]{:S(2)}, u32[]{:S(2)}) async-start(f32[64,1,2,1024]{3,2,1,0:T(2,128)} %broadcast_in_dim.579), calls=%async_computation | async-start | bytes 1048576 | tf_op jit(solution)/shard_map/all_to_all | solution.py:21
  139.7 3.1 %collective-permute-start = (bf16[30,256]{1,0:T(8,128)(2,1)S(1)}, bf16[30,256]{1,0:T(8,128)(2,1)S(1)}, u32[]{:S(2)}, u32[]{:S(2)}) collective-permute-start(bf16[30,256]{1,0:T(8,128)(2,1)S(1)} %slice.335), channel_id=1, source_target_pairs={{0,8},{8,16},{16,24},{24,32},{32,40},{40,48},{48,56},{56,64},{64,7... | collective-permute-start | bytes 46088 | tf_op jit(solution)/shard_map/ppermute | solution.py:10
  143.0 4.1 %collective-permute-done = bf16[30,256]{1,0:T(8,128)(2,1)S(1)} collective-permute-done((bf16[30,256]{1,0:T(8,128)(2,1)S(1)}, bf16[30,256]{1,0:T(8,128)(2,1)S(1)}, u32[]{:S(2)}, u32[]{:S(2)}) %collective-permute-start) | collective-permute-done | bytes 15392 | tf_op jit(solution)/shard_map/ppermute | solution.py:10
  148.1 8.0 %all-to-all-done = f32[64,1,2,1024]{3,2,1,0:T(2,128)S(1)} async-done(((f32[64,1,2,1024]{3,2,1,0:T(2,128)}), f32[64,1,2,1024]{3,2,1,0:T(2,128)S(1)}, u32[]{:S(2)}, u32[]{:S(2)}) %all-to-all-start) | async-done | bytes 524320 | tf_op jit(solution)/shard_map/all_to_all | solution.py:21
  156.7 1.7 fusion.85
  158.4 1.1 fusion.83
  160.9 4.5 %add_add_fusion = bf16[192,1024]{1,0:T(8,128)(2,1)S(1)} fusion(f32[192,1024]{1,0:T(8,128)S(1)} %multiply_add_fusion, f32[1024]{0:T(1024)S(1)} %bitcast.192, f32[1024]{0:T(1024)S(1)} %bitcast.194, f32[1024]{0:T(1024)S(1)} %copy-done.33, f32[1024]{0:T(1024)S(1)} %copy-done.31, f32[1024]{0:T(1024)S(1)} %copy-done.37, f32[1024]{0:T(1024)S(1)} %copy-done.35, ...), kind=kLoop, calls=%fused_computation.59 | loop fusion | flops 12386304 | bytes 1254912 | tf_op jit(solution)/shard_map/add | solution.py:162
  165.6 4.5 %subtract_add_fusion = bf16[192,1024]{1,0:T(8,128)(2,1)S(1)} fusion(f32[192,1024]{1,0:T(8,128)S(1)} %get-tuple-element.125, f32[1024]{0:T(1024)S(1)} %bitcast.193, f32[1024]{0:T(1024)S(1)} %bitcast.195, f32[1024]{0:T(1024)S(1)} %copy-done.33, f32[1024]{0:T(1024)S(1)} %copy-done.31, f32[1024]{0:T(1024)S(1)} %copy-done.37, f32[1024]{0:T(1024)S(1)} %copy-done.35, ...), kind=kLoop, calls=%fused_computation.60 | loop fusion | flops 12386304 | bytes 1254912 | tf_op jit(solution)/shard_map/add | solution.py:159
  170.9 1.3 broadcast_in_dim.580
  172.2 7.6 %all-to-all-start.1 = ((bf16[8,384,256]{2,1,0:T(8,128)(2,1)}), bf16[8,384,256]{2,1,0:T(8,128)(2,1)S(1)}, u32[]{:S(2)}, u32[]{:S(2)}) async-start(bf16[8,384,256]{2,1,0:T(8,128)(2,1)} %broadcast_in_dim.580), calls=%async_computation.1 | async-start | bytes 3145728 | tf_op jit(solution)/shard_map/all_to_all | solution.py:21
  180.5 19.8 %all-to-all-done.1 = bf16[8,384,256]{2,1,0:T(8,128)(2,1)S(1)} async-done(((bf16[8,384,256]{2,1,0:T(8,128)(2,1)}), bf16[8,384,256]{2,1,0:T(8,128)(2,1)S(1)}, u32[]{:S(2)}, u32[]{:S(2)}) %all-to-all-start.1) | async-done | bytes 1572896 | tf_op jit(solution)/shard_map/all_to_all | solution.py:21
  200.6 1.1 copy.52
  202.4 1.8 all-gather.5.cloned.1.call-done
  204.2 3.4 %fusion = f32[192,1024]{1,0:T(8,128)S(1)} fusion(bf16[192,2048]{1,0:T(8,128)(2,1)} %bitcast.127, bf16[2048,1536]{1,0:T(8,128)(2,1)} %all-gather.5.cloned.1.call-done), kind=kOutput, calls=%fused_computation | convolution fusion | flops 805306368 | bytes 5767168 | tf_op jit(solution)/shard_map/dot_general | solution.py:184
  207.6 3.0 %fusion.16 = bf16[192,512]{1,0:T(8,128)(2,1)} fusion(bf16[2048,1536]{1,0:T(8,128)(2,1)} %all-gather.5.cloned.1.call-done, f32[192,2048]{1,0:T(8,128)S(1)} %bitcast.123, f32[2048]{0:T(1024)S(1)} %copy-done.141, f32[2048]{0:T(1024)S(1)} %copy-done.142, f32[192]{0:T(256)S(1)} %add_rsqrt_fusion, f32[192]{0:T(256)S(1)} %broadcast_multiply_fusion, ...), kind=kOutput, calls=%fused_computation.31 | convolution fusion | flops 406781952 | bytes 4670976 | tf_op jit(solution)/shard_map/dot_general | solution.py:183
  (360 shorter events, 21.5 us)
Async XLA Ops:
  7.2 163.1 %copy-start = (f32[16,16,64]{2,1,0:T(8,128)S(1)}, f32[16,16,64]{2,1,0:T(8,128)}, u32[]{:S(2)}) copy-start(f32[16,16,64]{2,1,0:T(8,128)} %param.32) | copy-start | bytes 196612
  7.2 98.7 %all-gather.3.cloned.1.call-start = ((), (), s32[]{:S(2)}) async-start(), calls=%async_computation.2 | async-start | bytes 6389760 | tf_op jit(solution)/shard_map/all_gather | solution.py:89
  8.8 195.4 %all-gather.5.cloned.1.call-start = ((), (), s32[]{:S(2)}) async-start(), calls=%async_computation.3 | async-start | bytes 6389760 | tf_op jit(solution)/shard_map/all_gather | solution.py:182
  11.2 100.0 %copy-start.61 = (f32[16,64]{1,0:T(8,128)}, f32[16,64]{1,0:T(8,128)S(1)}, u32[]{:S(2)}) copy-start(f32[16,64]{1,0:T(8,128)S(1)} %get-tuple-element.85) | copy-start | bytes 12292
  11.2 100.0 %copy-start.63 = (f32[16,64]{1,0:T(8,128)}, f32[16,64]{1,0:T(8,128)S(1)}, u32[]{:S(2)}) copy-start(f32[16,64]{1,0:T(8,128)S(1)} %get-tuple-element.86) | copy-start | bytes 12292
  15.8 90.1 %copy-start.140 = (f32[4096]{0:T(1024)S(1)}, f32[4096]{0:T(1024)}, u32[]{:S(2)}) copy-start(f32[4096]{0:T(1024)} %param.20) | copy-start | bytes 49156
  22.5 87.6 %copy-start.10 = (f32[1,1024]{1,0:T(1,128)}, f32[1,1024]{1,0:T(1,128)S(1)}, u32[]{:S(2)}) copy-start(f32[1,1024]{1,0:T(1,128)S(1)} %get-tuple-element.13) | copy-start | bytes 12292
  22.5 87.6 %copy-start.12 = (f32[1,1024]{1,0:T(1,128)}, f32[1,1024]{1,0:T(1,128)S(1)}, u32[]{:S(2)}) copy-start(f32[1,1024]{1,0:T(1,128)S(1)} %get-tuple-element.14) | copy-start | bytes 12292
  22.5 87.6 %copy-start.14 = (f32[1,1024]{1,0:T(1,128)}, f32[1,1024]{1,0:T(1,128)S(1)}, u32[]{:S(2)}) copy-start(f32[1,1024]{1,0:T(1,128)S(1)} %get-tuple-element.12) | copy-start | bytes 12292
  22.5 87.6 %copy-start.44 = (f32[1,1024]{1,0:T(1,128)}, f32[1,1024]{1,0:T(1,128)S(1)}, u32[]{:S(2)}) copy-start(f32[1,1024]{1,0:T(1,128)S(1)} %get-tuple-element.17) | copy-start | bytes 12292
  22.6 87.6 %copy-start.46 = (f32[1,1024]{1,0:T(1,128)}, f32[1,1024]{1,0:T(1,128)S(1)}, u32[]{:S(2)}) copy-start(f32[1,1024]{1,0:T(1,128)S(1)} %get-tuple-element.18) | copy-start | bytes 12292
  22.6 87.6 %copy-start.52 = (f32[1,1024]{1,0:T(1,128)}, f32[1,1024]{1,0:T(1,128)S(1)}, u32[]{:S(2)}) copy-start(f32[1,1024]{1,0:T(1,128)S(1)} %get-tuple-element.19) | copy-start | bytes 12292
  22.6 87.6 %copy-start.54 = (f32[1,1024]{1,0:T(1,128)}, f32[1,1024]{1,0:T(1,128)S(1)}, u32[]{:S(2)}) copy-start(f32[1,1024]{1,0:T(1,128)S(1)} %get-tuple-element.20) | copy-start | bytes 12292
  22.6 87.6 %copy-start.56 = (f32[1,1024]{1,0:T(1,128)}, f32[1,1024]{1,0:T(1,128)S(1)}, u32[]{:S(2)}) copy-start(f32[1,1024]{1,0:T(1,128)S(1)} %get-tuple-element.21) | copy-start | bytes 12292
  22.6 87.6 %copy-start.58 = (f32[1,1024]{1,0:T(1,128)}, f32[1,1024]{1,0:T(1,128)S(1)}, u32[]{:S(2)}) copy-start(f32[1,1024]{1,0:T(1,128)S(1)} %get-tuple-element.22) | copy-start | bytes 12292
  23.8 86.4 %copy-start.8 = (f32[1,1024]{1,0:T(1,128)}, f32[1,1024]{1,0:T(1,128)S(1)}, u32[]{:S(2)}) copy-start(f32[1,1024]{1,0:T(1,128)S(1)} %add_multiply_fusion.7) | copy-start | bytes 12292
  23.8 86.4 %copy-start.48 = (f32[1024]{0:T(1024)}, f32[1024]{0:T(1024)S(1)}, u32[]{:S(2)}) copy-start(f32[1024]{0:T(1024)S(1)} %get-tuple-element.99) | copy-start | bytes 12292
  23.8 86.4 %copy-start.50 = (f32[1024]{0:T(1024)}, f32[1024]{0:T(1024)S(1)}, u32[]{:S(2)}) copy-start(f32[1024]{0:T(1024)S(1)} %get-tuple-element.100) | copy-start | bytes 12292
  27.9 83.4 %copy-start.4 = (f32[16,64,16]{1,2,0:T(8,128)S(1)}, f32[16,64,16]{1,2,0:T(8,128)}, u32[]{:S(2)}) copy-start(f32[16,64,16]{1,2,0:T(8,128)} %param.30) | copy-start | bytes 196612
  27.9 83.4 %copy-start.6 = (f32[16,64,16]{1,2,0:T(8,128)S(1)}, f32[16,64,16]{1,2,0:T(8,128)}, u32[]{:S(2)}) copy-start(f32[16,64,16]{1,2,0:T(8,128)} %param.31) | copy-start | bytes 196612
  128.2 19.0 %copy-start.108 = (f32[1,256]{1,0:T(1,128)S(1)}, f32[1,256]{1,0:T(1,128)}, u32[]{:S(2)}) copy-start(f32[1,256]{1,0:T(1,128)} %get-tuple-element.46) | copy-start | bytes 3076
  129.4 26.7 %all-to-all-start = ((f32[64,1,2,1024]{3,2,1,0:T(2,128)}), f32[64,1,2,1024]{3,2,1,0:T(2,128)S(1)}, u32[]{:S(2)}, u32[]{:S(2)}) async-start(f32[64,1,2,1024]{3,2,1,0:T(2,128)} %broadcast_in_dim.579), calls=%async_computation | async-start | bytes 1048576 | tf_op jit(solution)/shard_map/all_to_all | solution.py:21
  139.7 7.4 %collective-permute-start = (bf16[30,256]{1,0:T(8,128)(2,1)S(1)}, bf16[30,256]{1,0:T(8,128)(2,1)S(1)}, u32[]{:S(2)}, u32[]{:S(2)}) collective-permute-start(bf16[30,256]{1,0:T(8,128)(2,1)S(1)} %slice.335), channel_id=1, source_target_pairs={{0,8},{8,16},{16,24},{24,32},{32,40},{40,48},{48,56},{56,64},{64,7... | collective-permute-start | bytes 46088 | tf_op jit(solution)/shard_map/ppermute | solution.py:10
  172.2 28.1 %all-to-all-start.1 = ((bf16[8,384,256]{2,1,0:T(8,128)(2,1)}), bf16[8,384,256]{2,1,0:T(8,128)(2,1)S(1)}, u32[]{:S(2)}, u32[]{:S(2)}) async-start(bf16[8,384,256]{2,1,0:T(8,128)(2,1)} %broadcast_in_dim.580), calls=%async_computation.1 | async-start | bytes 3145728 | tf_op jit(solution)/shard_map/all_to_all | solution.py:21
  (124 other events, 1004.1 us)
Sparse Core Ops, SparseCore 0:
  11.0 94.8 all-gather.2
  109.4 94.6 all-gather.4
where the time goes:
time: 218 us; the launch traced here: 217 us
  waiting for transfers between devices  112 us (51%)
  other arithmetic  40.3 us (18%)
  starting transfers between devices  20 us (9%)
  matrix products  19 us (9%)
  between operations  16.4 us (8%)
  local copies, waits for them, and re-layouts  9.94 us (5%)
    all_gather x1, waiting for transfers between devices, local(): lax.all_gather(in_block, 'sp', axis=0, tiled=True)  78 us
    all_to_all x2, waiting for transfers between devices, copy_for_each(): lax.all_to_all(jnp.broadcast_to(shard[None], (length, *shard.shape)), axi...  27.8 us
    all_to_all x2, starting transfers between devices, copy_for_each(): lax.all_to_all(jnp.broadcast_to(shard[None], (length, *shard.shape)), axi...  16.8 us
    add x3, other arithmetic, rotate(): first_real * second_imag + first_imag * second_real  7.44 us
    dot_general x1, matrix products, local(): summed_imag = jnp.dot(lower, scaled_imag)  4.6 us
    add x1, other arithmetic, local(): power_real * entry_real - power_imag * entry_imag + local_real  4.47 us
    add x1, other arithmetic, local(): power_real * entry_imag + power_imag * entry_real + local_imag  4.46 us
  transfers between devices with their start and end apart: 5, of which 5 were waited for; matrix products, arithmetic and copies ran while one was open for 27% of the time, Pallas kernels for 0%

commit v1 on v0

v1 whole, which is shorter than its diff:
```python
import functools

import jax
import jax.numpy as jnp
from jax import lax
from jax.experimental import pallas as pl
from jax.experimental.pallas import tpu as pltpu
from jax.sharding import Mesh, PartitionSpec as P

BF = jnp.bfloat16
F32 = jnp.float32
LANES = 128


def rotate(first_real, first_imag, second_real, second_imag):
    return (
        first_real * second_real - first_imag * second_imag,
        first_real * second_imag + first_imag * second_real,
    )


def power_table(base_real, base_imag, exponent, largest):
    result_real = jnp.ones((exponent.shape[0], base_real.shape[0]), F32)
    result_imag = jnp.zeros((exponent.shape[0], base_real.shape[0]), F32)
    square_real, square_imag = (base_real, base_imag)
    for place in range(max(largest, 1).bit_length()):
        chosen = (exponent >> place & 1 == 1)[:, None]
        next_real, next_imag = rotate(result_real, result_imag, square_real, square_imag)
        result_real = jnp.where(chosen, next_real, result_real)
        result_imag = jnp.where(chosen, next_imag, result_imag)
        square_real, square_imag = rotate(square_real, square_imag, square_real, square_imag)
    return (result_real, result_imag)


def first_kernel(
    normed_ref, weights_ref, drive_ref, undo_ref, gated_ref, feed_ref, sums_ref, total_ref, acc_ref, last_ref
):
    step = pl.program_id(0)
    devices, _, width = weights_ref.shape
    rows = 64

    @pl.when(step == 0)
    def _():
        acc_ref[...] = jnp.zeros_like(acc_ref)

    for kind in range(3):
        block = weights_ref[:, kind * rows : (kind + 1) * rows, :].reshape(devices * rows, width)
        acc_ref[:, kind * width : (kind + 1) * width] += jnp.dot(
            normed_ref[...], block, preferred_element_type=F32
        )

    @pl.when(step == pl.num_programs(0) - 1)
    def _():
        length = acc_ref.shape[0]
        gated_ref[...] = (acc_ref[:, :width] * jax.nn.sigmoid(acc_ref[:, width : 2 * width])).astype(BF)
        feed = acc_ref[:, 2 * width :].astype(BF)
        feed_ref[...] = feed
        lower = (
            lax.broadcasted_iota(jnp.int32, (length, length), 0)
            >= lax.broadcasted_iota(jnp.int32, (length, length), 1)
        ).astype(BF)
        chunks = sums_ref.shape[1] // (2 * LANES)
        for at in range(chunks):
            real = slice(2 * at * LANES, (2 * at + 1) * LANES)
            imag = slice((2 * at + 1) * LANES, (2 * at + 2) * LANES)
            both = slice(2 * at * LANES, (2 * at + 2) * LANES)
            pushed = jnp.dot(feed, drive_ref[:, both], preferred_element_type=F32)
            scaled_real, scaled_imag = rotate(
                undo_ref[:, real], undo_ref[:, imag], pushed[:, :LANES], pushed[:, LANES:]
            )
            scaled = jnp.concatenate([scaled_real, scaled_imag], axis=1).astype(BF)
            sums = jnp.dot(lower, scaled, preferred_element_type=F32)
            sums_ref[:, both] = sums
            last_ref[at : at + 1, :] = sums[length - 1 :, :LANES]
            last_ref[chunks + at : chunks + at + 1, :] = sums[length - 1 :, LANES:]
        total_ref[...] = jnp.broadcast_to(last_ref[...][None], total_ref.shape)


def conv_kernel(before_ref, gated_ref, taps_ref, out_ref, pad_ref):
    length, width = gated_ref.shape
    lead = before_ref.shape[0]
    taps = taps_ref.shape[0]
    pad_ref[:lead] = before_ref[...].astype(F32)
    pad_ref[lead:] = gated_ref[...].astype(F32)
    for col in range(width // LANES):
        cols = slice(col * LANES, (col + 1) * LANES)
        acc = jnp.zeros((length, LANES), F32)
        for tap in range(taps):
            start = lead - (taps - 1) + tap
            acc = acc + taps_ref[tap : tap + 1, cols] * pad_ref[start : start + length, cols]
        rounded = acc.astype(BF)
        for copy in range(out_ref.shape[0]):
            out_ref[copy, :, cols] = rounded


def second_kernel(
    totals_ref, lead_ref, tail_ref, ends_ref, power_ref, sums_ref, mix_ref, feed_ref, skip_ref, out_ref, final_ref
):
    chunks = final_ref.shape[0] // 2
    total_real, total_imag = (totals_ref[:, :chunks, :], totals_ref[:, chunks:, :])
    lead_real, lead_imag = rotate(lead_ref[:, :chunks, :], lead_ref[:, chunks:, :], total_real, total_imag)
    entry_real = ends_ref[0, :chunks] + jnp.sum(lead_real, axis=0)
    entry_imag = ends_ref[0, chunks:] + jnp.sum(lead_imag, axis=0)
    tail_real, tail_imag = rotate(tail_ref[:, :chunks, :], tail_ref[:, chunks:, :], total_real, total_imag)
    final_ref[:chunks] = ends_ref[1, :chunks] + jnp.sum(tail_real, axis=0)
    final_ref[chunks:] = ends_ref[1, chunks:] + jnp.sum(tail_imag, axis=0)
    feed = feed_ref[...].astype(F32)
    response = skip_ref[...] * feed
    for at in range(chunks):
        real = slice(2 * at * LANES, (2 * at + 1) * LANES)
        imag = slice((2 * at + 1) * LANES, (2 * at + 2) * LANES)
        both = slice(2 * at * LANES, (2 * at + 2) * LANES)
        state_real, state_imag = rotate(
            power_ref[:, real],
            power_ref[:, imag],
            sums_ref[:, real] + entry_real[at : at + 1],
            sums_ref[:, imag] + entry_imag[at : at + 1],
        )
        states = jnp.concatenate([state_real, state_imag], axis=1).astype(BF)
        response = response + jnp.dot(states, mix_ref[both, :], preferred_element_type=F32)
    activated = jax.nn.gelu(response).astype(BF)
    for copy in range(out_ref.shape[0]):
        out_ref[copy] = activated


def last_kernel(conv_ref, act_ref, weights_ref, gain_ref, shift_ref, out_ref, acc_ref, mean_ref, scale_ref):
    step = pl.program_id(0)
    blocks, length, width = conv_ref.shape
    devices = weights_ref.shape[0]
    rows = 32

    @pl.when(step == 0)
    def _():
        acc_ref[...] = jnp.zeros_like(acc_ref)
        channels = blocks * width
        total = jnp.zeros((length, width), F32)
        for at in range(blocks):
            total = total + conv_ref[at].astype(F32)
        mean = jnp.sum(total, axis=1, keepdims=True) / channels
        spread = jnp.zeros((length, width), F32)
        for at in range(blocks):
            centred = conv_ref[at].astype(F32) - mean
            spread = spread + centred * centred
        variance = jnp.sum(spread, axis=1, keepdims=True) / channels
        mean_ref[...] = jnp.broadcast_to(mean, mean_ref.shape)
        scale_ref[...] = jnp.broadcast_to(lax.rsqrt(variance + 1e-05), scale_ref.shape)

    centred = conv_ref[step].astype(F32) - mean_ref[...]
    conv_act = jax.nn.silu(centred * scale_ref[...] * gain_ref[0] + shift_ref[0]).astype(BF)
    activated = act_ref[0]
    for part in range(6):
        block = weights_ref[:, part * rows : (part + 1) * rows, :].reshape(devices * rows, width)
        acc_ref[:, part * width : (part + 1) * width] += jnp.dot(
            conv_act if part < 2 else activated, block, preferred_element_type=F32
        )

    @pl.when(step == pl.num_programs(0) - 1)
    def _():
        columns = 2 * width
        out_ref[...] = (
            acc_ref[:, :columns]
            + acc_ref[:, columns : 2 * columns] * jax.nn.sigmoid(acc_ref[:, 2 * columns :])
        ).astype(BF)


def whole(shape):
    return pl.BlockSpec(shape, lambda *_: (0,) * len(shape))


def packed(real, imag):
    n, s = real.shape
    both = jnp.stack([real.reshape(n, s // LANES, LANES), imag.reshape(n, s // LANES, LANES)], axis=2)
    return both.reshape(n, 2 * s)


def rows_of(real, imag):
    n, s = real.shape
    return jnp.concatenate([real.reshape(n, s // LANES, LANES), imag.reshape(n, s // LANES, LANES)], axis=1)


def local(
    tokens,
    norm_gain,
    conv_value,
    conv_gate,
    state_feed,
    conv_taps,
    chan_gain,
    chan_shift,
    conv_project,
    decay_rate,
    frequency,
    input_real,
    input_imag,
    output_real,
    output_imag,
    skip_gain,
    state_value,
    state_gate,
    initial_state,
):
    seq_devices = lax.axis_size("sp")
    tp_devices = lax.axis_size("tp")
    position = lax.axis_index("sp")
    length, model = tokens.shape
    rows_in, width = conv_value.shape
    rows_out, columns = conv_project.shape
    shard = jnp.concatenate(
        [conv_value, conv_gate, state_feed]
        + [w[:, at : at + width] for w in (conv_project, state_value, state_gate) for at in (0, width)],
        axis=0,
    )
    gathered = lax.all_gather(shard, "sp", axis=0, tiled=False)

    floats = tokens.astype(F32)
    normed = (
        floats * lax.rsqrt(jnp.mean(floats * floats, axis=1, keepdims=True) + 1e-06) * norm_gain
    ).astype(BF)

    groups, state_size, group_size = input_real.shape
    flat = groups * state_size
    total_tokens = length * seq_devices
    rate_real = -decay_rate / total_tokens
    magnitude = jnp.exp(rate_real)
    step_real = magnitude * jnp.cos(frequency)
    step_imag = magnitude * jnp.sin(frequency)
    modulus = rate_real * rate_real + frequency * frequency
    lift_real = step_real - 1.0
    factor_real = (lift_real * rate_real + step_imag * frequency) / modulus
    factor_imag = (step_imag * rate_real - lift_real * frequency) / modulus
    drive_real = factor_real[..., None] * input_real - factor_imag[..., None] * input_imag
    drive_imag = factor_real[..., None] * input_imag + factor_imag[..., None] * input_real

    def spread(blocks):
        g, a, b = blocks.shape
        row = lax.broadcasted_iota(jnp.int32, (g * a, g * b), 0) // a
        col = lax.broadcasted_iota(jnp.int32, (g * a, g * b), 1) // b
        return jnp.where(row == col, jnp.tile(blocks.reshape(g * a, b), (1, g)), 0.0)

    drive = packed(
        spread(jnp.swapaxes(drive_real, 1, 2)), spread(jnp.swapaxes(drive_imag, 1, 2))
    ).astype(BF)
    mix = jnp.swapaxes(packed(
        spread(output_real), -spread(output_imag)
    ), 0, 1).astype(BF)

    base_real = step_real.reshape(flat)
    base_imag = step_imag.reshape(flat)
    square_size = base_real * base_real + base_imag * base_imag
    counted = lax.iota(jnp.int32, length) + 1
    power_real, power_imag = power_table(base_real, base_imag, counted, length)
    undo_real, undo_imag = power_table(base_real / square_size, -base_imag / square_size, counted, length)
    span_real, span_imag = (power_real[-1], power_imag[-1])
    device_ids = lax.iota(jnp.int32, seq_devices)
    lag = position - device_ids
    lead_real, lead_imag = power_table(span_real, span_imag, jnp.maximum(lag, 0), seq_devices)
    earlier = (lag > 0).astype(F32)[:, None]
    lead = rows_of(lead_real * earlier, lead_imag * earlier)
    tail = rows_of(*power_table(span_real, span_imag, seq_devices - device_ids, seq_devices))
    ends = rows_of(
        *rotate(
            *power_table(span_real, span_imag, jnp.stack([position, jnp.int32(seq_devices)]), seq_devices),
            initial_state[0].reshape(1, flat),
            initial_state[1].reshape(1, flat),
        )
    )
    power = packed(power_real, power_imag)
    undo = packed(undo_real, undo_imag)
    chunks = flat // LANES

    steps = 8
    per_step = seq_devices // steps
    gated, feed, sums, total = pl.pallas_call(
        first_kernel,
        grid=(steps,),
        in_specs=[
            pl.BlockSpec((length, model // steps), lambda k: (0, k)),
            pl.BlockSpec((per_step, 3 * rows_in, width), lambda k: (k, 0, 0)),
            whole(drive.shape),
            whole(undo.shape),
        ],
        out_specs=[
            whole((length, width)),
            whole((length, width)),
            whole((length, 2 * flat)),
            whole((seq_devices, 2 * chunks, LANES)),
        ],
        out_shape=[
            jax.ShapeDtypeStruct((length, width), BF),
            jax.ShapeDtypeStruct((length, width), BF),
            jax.ShapeDtypeStruct((length, 2 * flat), F32),
            jax.ShapeDtypeStruct((seq_devices, 2 * chunks, LANES), F32),
        ],
        scratch_shapes=[pltpu.VMEM((length, 3 * width), F32), pltpu.VMEM((2 * chunks, LANES), F32)],
        name="first",
    )(normed, gathered, drive, undo)

    taps = conv_taps.shape[0]
    halo = (taps - 1 + 15) // 16 * 16
    before = lax.ppermute(
        gated[length - halo :], "sp", [(source, source + 1) for source in range(seq_devices - 1)]
    )
    totals = lax.all_to_all(total, "sp", 0, 0, tiled=True)
    conv_copies = pl.pallas_call(
        conv_kernel,
        out_shape=jax.ShapeDtypeStruct((tp_devices, length, width), BF),
        scratch_shapes=[pltpu.VMEM((halo + length, width), F32)],
        name="conv",
    )(before, gated, conv_taps)
    conv_rows = lax.all_to_all(conv_copies, "tp", 0, 0, tiled=True)

    act_copies, final = pl.pallas_call(
        second_kernel,
        out_shape=[
            jax.ShapeDtypeStruct((tp_devices, length, width), BF),
            jax.ShapeDtypeStruct((2 * chunks, LANES), F32),
        ],
        name="second",
    )(totals, lead, tail, ends, power, sums, mix, feed, skip_gain.reshape(1, width))
    final_state = final.reshape(2, groups, state_size)
    act_rows = lax.all_to_all(act_copies, "tp", 0, 0, tiled=True)

    mixer_out = pl.pallas_call(
        last_kernel,
        grid=(tp_devices,),
        in_specs=[
            whole((tp_devices, length, width)),
            pl.BlockSpec((1, length, width), lambda k: (k, 0, 0)),
            pl.BlockSpec((seq_devices // tp_devices, 3 * rows_in, width), lambda k: (k, 1, 0)),
            pl.BlockSpec((1, 1, width), lambda k: (k, 0, 0)),
            pl.BlockSpec((1, 1, width), lambda k: (k, 0, 0)),
        ],
        out_specs=whole((length, columns)),
        out_shape=jax.ShapeDtypeStruct((length, columns), BF),
        scratch_shapes=[
            pltpu.VMEM((length, 6 * width), F32),
            pltpu.VMEM((length, width), F32),
            pltpu.VMEM((length, width), F32),
        ],
        name="last",
    )(
        conv_rows,
        act_rows,
        gathered,
        chan_gain.reshape(tp_devices, 1, width),
        chan_shift.reshape(tp_devices, 1, width),
    )
    return (mixer_out, final_state)


def solution(mesh):
    in_specs = (
        P("sp", None),
        P(),
        P("sp", "tp"),
        P("sp", "tp"),
        P("sp", "tp"),
        P(None, "tp"),
        P(),
        P(),
        P("sp", "tp"),
        P("tp", None),
        P("tp", None),
        P("tp", None, None),
        P("tp", None, None),
        P("tp", None, None),
        P("tp", None, None),
        P("tp"),
        P("sp", "tp"),
        P("sp", "tp"),
        P(None, "tp", None),
    )
    out_specs = (P("sp", "tp"), P(None, "tp", None))
    return jax.shard_map(local, mesh=mesh, in_specs=in_specs, out_specs=out_specs, check_vma=False)
```

time: 218 us -> 230 us (1.055)
  waiting for transfers between devices: 112 us -> 60.2 us
  other arithmetic: 40.3 us -> 85 us
  Pallas kernels: 0 us -> 24.8 us
  matrix products: 19 us -> 0 us
  local copies, waits for them, and re-layouts: 9.94 us -> 19.1 us
  starting transfers between devices: 20 us -> 25 us
    select_n x3 -> x8, other arithmetic: 3.8 us -> 55.2 us  [power_table(): result_real = jnp.where(chosen, next_real, result_real)]
    all_gather x2 -> x1, waiting for transfers between devices: 79.8 us -> 43.3 us  [local(): gathered = lax.all_gather(shard, 'sp', axis=0, tiled=False)]
    pallas_call x0 -> x4, Pallas kernels: none -> 24.8 us  [the longest x1 9.96 us: local(): pl.pallas_call(first_kernel, grid=(steps,), in_specs=[pl.BlockSpec((lengt...]
    dot_general x9 -> x0, matrix products: 19 us -> none  [the longest x1 4.6 us: local(): summed_imag = jnp.dot(lower, scaled_imag)]
    all_to_all x2 -> x3, waiting for transfers between devices: 27.8 us -> 16.8 us  [the longest x1 11.5 us: local(): act_rows = lax.all_to_all(act_copies, 'tp', 0, 0, tiled=True)]
    select_n x3 -> x5, other arithmetic: 3.79 us -> 14.8 us  [power_table(): result_imag = jnp.where(chosen, next_imag, result_imag)]
    add x3 -> x0, other arithmetic: 8.97 us -> none  [the longest x1 4.47 us: local(): power_real * entry_real - power_imag * entry_imag + local_real]
    add x3, other arithmetic: 7.44 us -> 0.02 us  [rotate(): first_real * second_imag + first_imag * second_real]
  transfers between devices with their start and end apart: 5 -> 5, of which waited for: 5 -> 4; matrix products, arithmetic and copies ran while one was open for 27% -> 42% of each run, Pallas kernels for 0% -> 3%
where the time goes in v1:
time: 230 us; the launch traced here: 229 us
  other arithmetic  85 us (37%)
  waiting for transfers between devices  60.2 us (26%)
  starting transfers between devices  25 us (11%)
  Pallas kernels  24.8 us (11%)
  local copies, waits for them, and re-layouts  19.1 us (8%)
  between operations  14.5 us (6%)
    select_n x8, other arithmetic, power_table(): result_real = jnp.where(chosen, next_real, result_real)  55.2 us
    all_gather x1, waiting for transfers between devices, local(): gathered = lax.all_gather(shard, 'sp', axis=0, tiled=False)  43.3 us
    select_n x5, other arithmetic, power_table(): result_imag = jnp.where(chosen, next_imag, result_imag)  14.8 us
    all_to_all x1, waiting for transfers between devices, local(): act_rows = lax.all_to_all(act_copies, 'tp', 0, 0, tiled=True)  11.5 us
    all_to_all x1, starting transfers between devices, local(): totals = lax.all_to_all(total, 'sp', 0, 0, tiled=True)  10.2 us
    pallas_call x1, Pallas kernels, local(): pl.pallas_call(first_kernel, grid=(steps,), in_specs=[pl.BlockSpec((lengt...  9.96 us
    unnamed x48, local copies, waits for them, and re-layouts  8.44 us
    pallas_call x1, Pallas kernels, local(): pl.pallas_call(last_kernel, grid=(tp_devices,), in_specs=[whole((tp_devic...  8.06 us
  transfers between devices with their start and end apart: 5, of which 4 were waited for; matrix products, arithmetic and copies ran while one was open for 42% of the time, Pallas kernels for 3%

profile of v1, /device:TPU:1, one launch (start us, length us, event | category | flops | bytes accessed | tf_op | source)
XLA Modules:
  0.0 228.7 jit_solution(8383327456887300911)
XLA Ops:
  17.2 19.0 %broadcast_select_fusion.11 = (f32[192,8,1,128]{3,2,1,0:T(1,128)S(1)}, f32[192,8,1,128]{3,2,1,0:T(1,128)S(1)}, f32[192,8,1,128]{3,2,1,0:T(1,128)S(1)}) fusion(pred[192]{0:T(512)(128)(4,1)S(1)} %get-tuple-element.182, f32[8,128]{1,0:T(8,128)S(1)} %get-tuple-element.118, f32[8,128]{1,0:T(8,128)S(1)} %get-tuple-element.119, ...), kind=kLoop, calls=%fused_computation.18 | loop fusion | flops 4325376 | bytes 2392832 | tf_op jit(solution)/shard_map/jit(_where)/select_n | solution.py:29
  36.2 19.0 %broadcast_select_fusion.9 = (f32[192,8,1,128]{3,2,1,0:T(1,128)S(1)}, f32[192,8,1,128]{3,2,1,0:T(1,128)S(1)}, f32[192,8,1,128]{3,2,1,0:T(1,128)S(1)}) fusion(pred[192]{0:T(512)(128)(4,1)S(1)} %get-tuple-element.182, f32[8,128]{1,0:T(8,128)S(1)} %get-tuple-element.133, f32[8,128]{1,0:T(8,128)S(1)} %get-tuple-element.134, f32[8,128]{1,0:T(8,128)S(1)} %get-tuple-element.135, ...), kind=kLoop, calls=%fused_computation.16 | loop fusion | flops 4325376 | bytes 2392832 | tf_op jit(solution)/shard_map/jit(_where)/select_n | solution.py:29
  55.2 3.1 %broadcast_select_fusion.8 = (f32[192,8,1,128]{3,2,1,0:T(1,128)S(1)}, f32[192,8,1,128]{3,2,1,0:T(1,128)S(1)}) fusion(f32[192,8,1,128]{3,2,1,0:T(1,128)S(1)} %get-tuple-element.35, pred[192]{0:T(512)(128)(4,1)S(1)} %get-tuple-element.182, f32[192,8,1,128]{3,2,1,0:T(1,128)S(1)} %get-tuple-element.34, f32[8,128]{1,0:T(8,128)S(1)} %get-tuple-element.133, ...), kind=kLoop, calls=%fused_computation.15 | loop fusion | flops 1572864 | bytes 4735168 | tf_op jit(solution)/shard_map/jit(_where)/select_n | solution.py:30
  58.4 6.9 %broadcast_select_fusion.17 = (f32[192,8,1,128]{3,2,1,0:T(1,128)S(1)}, f32[192,8,1,128]{3,2,1,0:T(1,128)S(1)}, f32[192,8,1,128]{3,2,1,0:T(1,128)S(1)}, f32[192,8...) fusion(pred[192]{0:T(512)(128)(4,1)S(1)} %get-tuple-element.184, ...), kind=kLoop, calls=%fused_computation.24 | loop fusion | flops 4718592 | bytes 7897472 | tf_op jit(solution)/shard_map/jit(_where)/select_n | solution.py:29
  65.3 3.1 %broadcast_select_fusion.16 = (f32[192,8,1,128]{3,2,1,0:T(1,128)S(1)}, f32[192,8,1,128]{3,2,1,0:T(1,128)S(1)}) fusion(f32[192,8,1,128]{3,2,1,0:T(1,128)S(1)} %get-tuple-element.32, pred[192]{0:T(512)(128)(4,1)S(1)} %get-tuple-element.184, f32[192,8,1,128]{3,2,1,0:T(1,128)S(1)} %get-tuple-element.31, f32[8,128]{1,0:T(8,128)S(1)} %get-tuple-element.129, ...), kind=kLoop, calls=%fused_computation.23 | loop fusion | flops 1572864 | bytes 4735168 | tf_op jit(solution)/shard_map/jit(_where)/select_n | solution.py:30
  68.4 6.9 %broadcast_select_fusion.25 = (f32[192,8,1,128]{3,2,1,0:T(1,128)S(1)}, f32[192,8,1,128]{3,2,1,0:T(1,128)S(1)}, f32[192,8,1,128]{3,2,1,0:T(1,128)S(1)}, f32[192,8...) fusion(pred[192]{0:T(512)(128)(4,1)S(1)} %get-tuple-element.186, ...), kind=kLoop, calls=%fused_computation.32 | loop fusion | flops 4718592 | bytes 7897472 | tf_op jit(solution)/shard_map/jit(_where)/select_n | solution.py:29
  75.3 4.1 %broadcast_select_fusion.24 = (f32[192,8,1,128]{3,2,1,0:T(1,128)}, f32[192,8,1,128]{3,2,1,0:T(1,128)S(1)}) fusion(f32[192,8,1,128]{3,2,1,0:T(1,128)S(1)} %get-tuple-element.16, pred[192]{0:T(512)(128)(4,1)S(1)} %get-tuple-element.186, f32[192,8,1,128]{3,2,1,0:T(1,128)S(1)} %get-tuple-element.15, f32[8,128]{1,0:T(8,128)S(1)} %get-tuple-element.177, ...), kind=kLoop, calls=%fused_computation.31 | loop fusion | flops 1572864 | bytes 4735168 | tf_op jit(solution)/shard_map/jit(_where)/select_n | solution.py:30
  80.9 2.4 %reshape.3647.undo_ref = f32[192,2048]{1,0:T(8,128)} reshape(f32[192,8,2,128]{3,2,1,0:T(2,128)S(1)} %pad_maximum_fusion) | data formatting | bytes 3145728 | tf_op jit(solution)/shard_map/reshape | solution.py:173
  87.3 2.7 %add_select_fusion = f32[192,1024]{1,0:T(8,128)S(1)} fusion(f32[1024]{0:T(1024)S(1)} %get-tuple-element.99, f32[1024]{0:T(1024)S(1)} %get-tuple-element.97, pred[192]{0:T(512)(128)(4,1)S(1)} %get-tuple-element.185, f32[1024]{0:T(1024)S(1)} %get-tuple-element.104, f32[1024]{0:T(1024)S(1)} %get-tuple-element.108, f32[1024]{0:T(1024)S(1)} %get-tuple-element.144, ...), kind=kLoop, calls=%fused_computation.62 | loop fusion | flops 9043968 | bytes 845120 | tf_op jit(solution)/shard_map/jit(_where)/select_n | solution.py:30
  90.1 2.7 %subtract_select_fusion = f32[192,1024]{1,0:T(8,128)S(1)} fusion(f32[1024]{0:T(1024)S(1)} %get-tuple-element.99, f32[1024]{0:T(1024)S(1)} %get-tuple-element.97, pred[192]{0:T(512)(128)(4,1)S(1)} %get-tuple-element.185, f32[1024]{0:T(1024)S(1)} %get-tuple-element.104, f32[1024]{0:T(1024)S(1)} %get-tuple-element.108, f32[1024]{0:T(1024)S(1)} %get-tuple-element.144, ...), kind=kLoop, calls=%fused_computation.63 | loop fusion | flops 9043968 | bytes 845120 | tf_op jit(solution)/shard_map/jit(_where)/select_n | solution.py:29
  94.4 1.6 fusion.2.normed_ref
  96.0 43.3 %all-gather.3.cloned.1.call-done = bf16[24576,256]{1,0:T(8,128)(2,1)} async-done(((bf16[384,256]{1,0:T(8,128)(2,1)}), bf16[24576,256]{1,0:T(8,128)(2,1)}) %all-gather.3.cloned.1.call-update) | async-done | bytes 12582928 | tf_op jit(solution)/shard_map/all_gather | solution.py:213
  139.3 10.0 %first.1 = (bf16[192,256]{1,0:T(8,128)(2,1)}, bf16[192,256]{1,0:T(8,128)(2,1)}, f32[192,2048]{1,0:T(8,128)}, f32[64,16,128]{2,1,0:T(8,128)}) custom-call(bf16[192,4096]{1,0:T(8,128)(2,1)} %fusion.2.normed_ref, bf16[64,384,256]{2,1,0:T(8,128)(2,1)} %bitcast.35, bf16[256,2048]{1,0:T(8,128)(2,1)} %copy.26.drive_ref, f32[192,2048]{1,0:T(8,128)} %reshape.3647.undo_ref), custom_call_target="tpu_custom_call" | custom-call | tf_op jit(solution)/shard_map/first/pallas_call | solution.py:273
  149.3 10.2 %all-to-all-start.1 = ((f32[64,16,128]{2,1,0:T(8,128)}), f32[64,16,128]{2,1,0:T(8,128)}, u32[]{:S(2)}, u32[]{:S(2)}) async-start(f32[64,16,128]{2,1,0:T(8,128)} %get-tuple-element.9), calls=%async_computation.1 | async-start | bytes 1048576 | tf_op jit(solution)/shard_map/all_to_all | solution.py:303
  159.5 1.6 add_select_fusion.4
  164.7 3.0 %collective-permute-start = (bf16[32,256]{1,0:T(8,128)(2,1)S(1)}, bf16[32,256]{1,0:T(8,128)(2,1)S(1)}, u32[]{:S(2)}, u32[]{:S(2)}) collective-permute-start(bf16[32,256]{1,0:T(8,128)(2,1)S(1)} %slice.39), channel_id=1, source_target_pairs={{0,8},{8,16},{16,24},{24,32},{32,40},{40,48},{48,56},{56,64},{64,7... | collective-permute-start | bytes 49160 | tf_op jit(solution)/shard_map/ppermute | solution.py:300
  169.8 2.7 %conv.1 = bf16[8,192,256]{2,1,0:T(8,128)(2,1)} custom-call(bf16[32,256]{1,0:T(8,128)(2,1)} %copy-done.14, bf16[192,256]{1,0:T(8,128)(2,1)} %get-tuple-element.8.gated_ref, f32[31,256]{1,0:T(8,128)} %taps_ref.1), custom_call_target="tpu_custom_call" | custom-call | tf_op jit(solution)/shard_map/conv/pallas_call | solution.py:304
  172.5 4.2 %all-to-all-done.1.totals_ref = f32[64,16,128]{2,1,0:T(8,128)} async-done(((f32[64,16,128]{2,1,0:T(8,128)}), f32[64,16,128]{2,1,0:T(8,128)}, u32[]{:S(2)}, u32[]{:S(2)}) %all-to-all-start.1) | async-done | bytes 524320 | tf_op jit(solution)/shard_map/all_to_all | solution.py:303
  176.7 7.3 %all-to-all-start = ((bf16[8,192,256]{2,1,0:T(8,128)(2,1)}), bf16[8,192,256]{2,1,0:T(8,128)(2,1)S(1)}, u32[]{:S(2)}, u32[]{:S(2)}) async-start(bf16[8,192,256]{2,1,0:T(8,128)(2,1)} %conv.1), calls=%async_computation | async-start | bytes 1572864 | tf_op jit(solution)/shard_map/all_to_all | solution.py:310
  184.7 2.4 %reshape.3648.power_ref = f32[192,2048]{1,0:T(8,128)} reshape(f32[192,8,2,128]{3,2,1,0:T(2,128)S(1)} %pad_maximum_fusion.1) | data formatting | bytes 3145728 | tf_op jit(solution)/shard_map/reshape | solution.py:173
  191.0 4.1 %second.1 = (bf16[8,192,256]{2,1,0:T(8,128)(2,1)}, f32[16,128]{1,0:T(8,128)}) custom-call(f32[64,16,128]{2,1,0:T(8,128)} %all-to-all-done.1.totals_ref, f32[64,16,128]{2,1,0:T(8,128)} %pad_maximum_fusion.4.lead_ref, f32[64,16,128]{2,1,0:T(8,128)} %pad_maximum_fusion.5.tail_ref, f32[2,16,128]{2,1,0:T(8,128)} %pad_maximum_fusion.6.ends_ref, ...), custom_call_target="tpu_custom_call" | custom-call | tf_op jit(solution)/shard_map/second/pallas_call | solution.py:312
  196.2 4.4 %all-to-all-start.2 = ((bf16[8,192,256]{2,1,0:T(8,128)(2,1)}), bf16[8,192,256]{2,1,0:T(8,128)(2,1)S(1)}, u32[]{:S(2)}, u32[]{:S(2)}) async-start(bf16[8,192,256]{2,1,0:T(8,128)(2,1)} %get-tuple-element.12), calls=%async_computation.2 | async-start | bytes 1572864 | tf_op jit(solution)/shard_map/all_to_all | solution.py:321
  201.3 11.5 %all-to-all-done.2.act_ref = bf16[8,192,256]{2,1,0:T(8,128)(2,1)S(1)} async-done(((bf16[8,192,256]{2,1,0:T(8,128)(2,1)}), bf16[8,192,256]{2,1,0:T(8,128)(2,1)S(1)}, u32[]{:S(2)}, u32[]{:S(2)}) %all-to-all-start.2) | async-done | bytes 786464 | tf_op jit(solution)/shard_map/all_to_all | solution.py:321
  213.8 8.1 %last.1 = bf16[192,512]{1,0:T(8,128)(2,1)} custom-call(bf16[8,192,256]{2,1,0:T(8,128)(2,1)} %copy-done.2, bf16[8,192,256]{2,1,0:T(8,128)(2,1)} %copy-done.3, bf16[64,384,256]{2,1,0:T(8,128)(2,1)} %bitcast.36, f32[8,1,256]{2,1,0:T(1,128)} %bitcast.113, f32[8,1,256]{2,1,0:T(1,128)} %bitcast.114), custom_call_target="tpu_custom_call" | custom-call | tf_op jit(solution)/shard_map/last/pallas_call | solution.py:323
  (118 shorter events, 29.5 us)
Async XLA Ops:
  7.2 132.2 %all-gather.3.cloned.1.call-start = ((), (), s32[]{:S(2)}) async-start(), calls=%async_computation.3 | async-start | bytes 12779520 | tf_op jit(solution)/shard_map/all_gather | solution.py:213
  13.8 0.7 copy-start.8
  80.8 2.5 %copy-start.9 = (f32[16,64,16]{1,2,0:T(8,128)S(1)}, f32[16,64,16]{1,2,0:T(8,128)}, u32[]{:S(2)}) copy-start(f32[16,64,16]{1,2,0:T(8,128)} %param.31) | copy-start | bytes 196612
  80.8 2.5 %copy-start.10 = (f32[16,64,16]{1,2,0:T(8,128)S(1)}, f32[16,64,16]{1,2,0:T(8,128)}, u32[]{:S(2)}) copy-start(f32[16,64,16]{1,2,0:T(8,128)} %param.30) | copy-start | bytes 196612
  80.8 2.7 %copy-start.11 = (f32[16,16,64]{2,1,0:T(8,128)S(1)}, f32[16,16,64]{2,1,0:T(8,128)}, u32[]{:S(2)}) copy-start(f32[16,16,64]{2,1,0:T(8,128)} %param.32) | copy-start | bytes 196612
  83.6 1.5 copy-start.18
  83.7 1.5 copy-start.16
  85.2 1.6 copy-start
  87.3 7.1 %copy-start.13 = (f32[4096]{0:T(1024)S(1)}, f32[4096]{0:T(1024)}, u32[]{:S(2)}) copy-start(f32[4096]{0:T(1024)} %param.20) | copy-start | bytes 49156
  149.3 18.5 %copy-start.1 = (f32[192,8,1,128]{3,2,1,0:T(1,128)S(1)}, f32[192,8,1,128]{3,2,1,0:T(1,128)}, u32[]{:S(2)}) copy-start(f32[192,8,1,128]{3,2,1,0:T(1,128)} %get-tuple-element.161) | copy-start | bytes 2359300
  149.3 27.4 %all-to-all-start.1 = ((f32[64,16,128]{2,1,0:T(8,128)}), f32[64,16,128]{2,1,0:T(8,128)}, u32[]{:S(2)}, u32[]{:S(2)}) async-start(f32[64,16,128]{2,1,0:T(8,128)} %get-tuple-element.9), calls=%async_computation.1 | async-start | bytes 1048576 | tf_op jit(solution)/shard_map/all_to_all | solution.py:303
  164.7 4.5 %collective-permute-start = (bf16[32,256]{1,0:T(8,128)(2,1)S(1)}, bf16[32,256]{1,0:T(8,128)(2,1)S(1)}, u32[]{:S(2)}, u32[]{:S(2)}) collective-permute-start(bf16[32,256]{1,0:T(8,128)(2,1)S(1)} %slice.39), channel_id=1, source_target_pairs={{0,8},{8,16},{16,24},{24,32},{32,40},{40,48},{48,56},{56,64},{64,7... | collective-permute-start | bytes 49160 | tf_op jit(solution)/shard_map/ppermute | solution.py:300
  176.7 19.5 %all-to-all-start = ((bf16[8,192,256]{2,1,0:T(8,128)(2,1)}), bf16[8,192,256]{2,1,0:T(8,128)(2,1)S(1)}, u32[]{:S(2)}, u32[]{:S(2)}) async-start(bf16[8,192,256]{2,1,0:T(8,128)(2,1)} %conv.1), calls=%async_computation | async-start | bytes 1572864 | tf_op jit(solution)/shard_map/all_to_all | solution.py:310
  184.7 2.4 %copy-start.12 = (f32[16,16,64]{2,1,0:T(8,128)S(1)}, f32[16,16,64]{2,1,0:T(8,128)}, u32[]{:S(2)}) copy-start(f32[16,16,64]{2,1,0:T(8,128)} %param.33) | copy-start | bytes 196612
  184.7 2.5 %copy-start.5 = (f32[64,8,128]{2,1,0:T(8,128)S(1)}, f32[64,8,128]{2,1,0:T(8,128)}, u32[]{:S(2)}) copy-start(f32[64,8,128]{2,1,0:T(8,128)} %add_select_fusion.4) | copy-start | bytes 786436
  184.7 3.4 %copy-start.6 = (f32[64,8,128]{2,1,0:T(8,128)S(1)}, f32[64,8,128]{2,1,0:T(8,128)}, u32[]{:S(2)}) copy-start(f32[64,8,128]{2,1,0:T(8,128)} %select_multiply_fusion.13) | copy-start | bytes 786436
  184.7 3.4 %copy-start.7 = (f32[64,8,128]{2,1,0:T(8,128)S(1)}, f32[64,8,128]{2,1,0:T(8,128)}, u32[]{:S(2)}) copy-start(f32[64,8,128]{2,1,0:T(8,128)} %select_multiply_fusion.12) | copy-start | bytes 786436
  187.2 1.8 copy-start.17
  187.2 1.8 copy-start.19
  188.9 1.0 copy-start.4
  195.1 5.5 %copy-start.15 = (f32[16,128]{1,0:T(8,128)S(1)}, f32[16,128]{1,0:T(8,128)}, u32[]{:S(2)}) copy-start(f32[16,128]{1,0:T(8,128)} %get-tuple-element.13) | copy-start | bytes 24580
  196.2 16.6 %copy-start.2 = (bf16[8,192,256]{2,1,0:T(8,128)(2,1)}, bf16[8,192,256]{2,1,0:T(8,128)(2,1)S(1)}, u32[]{:S(2)}) copy-start(bf16[8,192,256]{2,1,0:T(8,128)(2,1)S(1)} %all-to-all-done.conv_ref) | copy-start | bytes 2359300
  196.2 16.6 %all-to-all-start.2 = ((bf16[8,192,256]{2,1,0:T(8,128)(2,1)}), bf16[8,192,256]{2,1,0:T(8,128)(2,1)S(1)}, u32[]{:S(2)}, u32[]{:S(2)}) async-start(bf16[8,192,256]{2,1,0:T(8,128)(2,1)} %get-tuple-element.12), calls=%async_computation.2 | async-start | bytes 1572864 | tf_op jit(solution)/shard_map/all_to_all | solution.py:321
  212.8 0.9 copy-start.3
  (1 other events, 0.6 us)
Sparse Core Ops, SparseCore 0:
  14.6 124.6 all-gather.2

commit v2 on v1

--- a/solution.py
+++ b/solution.py
@@ -10,6 +10,7 @@
 BF = jnp.bfloat16
 F32 = jnp.float32
 LANES = 128
+CHUNK = 256
 
 
 def rotate(first_real, first_imag, second_real, second_imag):
@@ -32,12 +33,34 @@
     return (result_real, result_imag)
 
 
+def pack_kernel(*refs):
+    out_ref = refs[-1]
+    width = out_ref.shape[1]
+    at = 0
+    for ref in refs[:-1]:
+        for col in range(0, ref.shape[1], width):
+            out_ref[at : at + ref.shape[0]] = ref[:, col : col + width]
+            at += ref.shape[0]
+
+
 def first_kernel(
-    normed_ref, weights_ref, drive_ref, undo_ref, gated_ref, feed_ref, sums_ref, total_ref, acc_ref, last_ref
+    normed_ref,
+    weights_ref,
+    drive_real_ref,
+    drive_imag_ref,
+    undo_real_ref,
+    undo_imag_ref,
+    gated_ref,
+    feed_ref,
+    sums_real_ref,
+    sums_imag_ref,
+    total_ref,
+    acc_ref,
+    last_ref,
 ):
     step = pl.program_id(0)
     devices, _, width = weights_ref.shape
-    rows = 64
+    rows = weights_ref.shape[1] // 3
 
     @pl.when(step == 0)
     def _():
@@ -59,20 +82,19 @@
             lax.broadcasted_iota(jnp.int32, (length, length), 0)
             >= lax.broadcasted_iota(jnp.int32, (length, length), 1)
         ).astype(BF)
-        chunks = sums_ref.shape[1] // (2 * LANES)
-        for at in range(chunks):
-            real = slice(2 * at * LANES, (2 * at + 1) * LANES)
-            imag = slice((2 * at + 1) * LANES, (2 * at + 2) * LANES)
-            both = slice(2 * at * LANES, (2 * at + 2) * LANES)
-            pushed = jnp.dot(feed, drive_ref[:, both], preferred_element_type=F32)
-            scaled_real, scaled_imag = rotate(
-                undo_ref[:, real], undo_ref[:, imag], pushed[:, :LANES], pushed[:, LANES:]
-            )
-            scaled = jnp.concatenate([scaled_real, scaled_imag], axis=1).astype(BF)
-            sums = jnp.dot(lower, scaled, preferred_element_type=F32)
-            sums_ref[:, both] = sums
-            last_ref[at : at + 1, :] = sums[length - 1 :, :LANES]
-            last_ref[chunks + at : chunks + at + 1, :] = sums[length - 1 :, LANES:]
+        flat = sums_real_ref.shape[1]
+        half = last_ref.shape[0] // 2
+        for at in range(0, flat, CHUNK):
+            cols = slice(at, at + CHUNK)
+            pushed_real = jnp.dot(feed, drive_real_ref[:, cols], preferred_element_type=F32)
+            pushed_imag = jnp.dot(feed, drive_imag_ref[:, cols], preferred_element_type=F32)
+            scaled = rotate(undo_real_ref[:, cols], undo_imag_ref[:, cols], pushed_real, pushed_imag)
+            for part, ref in enumerate((sums_real_ref, sums_imag_ref)):
+                sums = jnp.dot(lower, scaled[part].astype(BF), preferred_element_type=F32)
+                ref[:, cols] = sums
+                for lane in range(0, CHUNK, LANES):
+                    row = part * half + (at + lane) // LANES
+                    last_ref[row : row + 1, :] = sums[length - 1 :, lane : lane + LANES]
         total_ref[...] = jnp.broadcast_to(last_ref[...][None], total_ref.shape)
 
 
@@ -94,44 +116,58 @@
 
 
 def second_kernel(
-    totals_ref, lead_ref, tail_ref, ends_ref, power_ref, sums_ref, mix_ref, feed_ref, skip_ref, out_ref, final_ref
+    totals_ref,
+    lead_ref,
+    tail_ref,
+    ends_ref,
+    power_real_ref,
+    power_imag_ref,
+    sums_real_ref,
+    sums_imag_ref,
+    mix_real_ref,
+    mix_imag_ref,
+    feed_ref,
+    skip_ref,
+    out_ref,
+    final_ref,
+    entry_ref,
 ):
-    chunks = final_ref.shape[0] // 2
-    total_real, total_imag = (totals_ref[:, :chunks, :], totals_ref[:, chunks:, :])
-    lead_real, lead_imag = rotate(lead_ref[:, :chunks, :], lead_ref[:, chunks:, :], total_real, total_imag)
-    entry_real = ends_ref[0, :chunks] + jnp.sum(lead_real, axis=0)
-    entry_imag = ends_ref[0, chunks:] + jnp.sum(lead_imag, axis=0)
-    tail_real, tail_imag = rotate(tail_ref[:, :chunks, :], tail_ref[:, chunks:, :], total_real, total_imag)
-    final_ref[:chunks] = ends_ref[1, :chunks] + jnp.sum(tail_real, axis=0)
-    final_ref[chunks:] = ends_ref[1, chunks:] + jnp.sum(tail_imag, axis=0)
-    feed = feed_ref[...].astype(F32)
-    response = skip_ref[...] * feed
-    for at in range(chunks):
-        real = slice(2 * at * LANES, (2 * at + 1) * LANES)
-        imag = slice((2 * at + 1) * LANES, (2 * at + 2) * LANES)
-        both = slice(2 * at * LANES, (2 * at + 2) * LANES)
+    half = final_ref.shape[0] // 2
+    total_real, total_imag = (totals_ref[:, :half, :], totals_ref[:, half:, :])
+    lead_real, lead_imag = rotate(lead_ref[:, :half, :], lead_ref[:, half:, :], total_real, total_imag)
+    entry_ref[:half] = ends_ref[0, :half] + jnp.sum(lead_real, axis=0)
+    entry_ref[half:] = ends_ref[0, half:] + jnp.sum(lead_imag, axis=0)
+    tail_real, tail_imag = rotate(tail_ref[:, :half, :], tail_ref[:, half:, :], total_real, total_imag)
+    final_ref[:half] = ends_ref[1, :half] + jnp.sum(tail_real, axis=0)
+    final_ref[half:] = ends_ref[1, half:] + jnp.sum(tail_imag, axis=0)
+    response = skip_ref[...] * feed_ref[...].astype(F32)
+    for at in range(0, sums_real_ref.shape[1], CHUNK):
+        cols = slice(at, at + CHUNK)
+        rows = range(at // LANES, (at + CHUNK) // LANES)
+        entry_real = jnp.concatenate([entry_ref[row : row + 1] for row in rows], axis=1)
+        entry_imag = jnp.concatenate([entry_ref[half + row : half + row + 1] for row in rows], axis=1)
         state_real, state_imag = rotate(
-            power_ref[:, real],
-            power_ref[:, imag],
-            sums_ref[:, real] + entry_real[at : at + 1],
-            sums_ref[:, imag] + entry_imag[at : at + 1],
+            power_real_ref[:, cols],
+            power_imag_ref[:, cols],
+            sums_real_ref[:, cols] + entry_real,
+            sums_imag_ref[:, cols] + entry_imag,
         )
-        states = jnp.concatenate([state_real, state_imag], axis=1).astype(BF)
-        response = response + jnp.dot(states, mix_ref[both, :], preferred_element_type=F32)
+        response = response + jnp.dot(state_real.astype(BF), mix_real_ref[cols, :], preferred_element_type=F32)
+        response = response + jnp.dot(state_imag.astype(BF), mix_imag_ref[cols, :], preferred_element_type=F32)
     activated = jax.nn.gelu(response).astype(BF)
     for copy in range(out_ref.shape[0]):
         out_ref[copy] = activated
 
 
-def last_kernel(conv_ref, act_ref, weights_ref, gain_ref, shift_ref, out_ref, acc_ref, mean_ref, scale_ref):
+def branch_kernel(conv_ref, weights_ref, gain_ref, shift_ref, out_ref, mean_ref, scale_ref):
     step = pl.program_id(0)
     blocks, length, width = conv_ref.shape
     devices = weights_ref.shape[0]
-    rows = 32
+    rows = weights_ref.shape[1] // 2
 
     @pl.when(step == 0)
     def _():
-        acc_ref[...] = jnp.zeros_like(acc_ref)
+        out_ref[...] = jnp.zeros_like(out_ref)
         channels = blocks * width
         total = jnp.zeros((length, width), F32)
         for at in range(blocks):
@@ -147,19 +183,35 @@
 
     centred = conv_ref[step].astype(F32) - mean_ref[...]
     conv_act = jax.nn.silu(centred * scale_ref[...] * gain_ref[0] + shift_ref[0]).astype(BF)
+    for part in range(2):
+        block = weights_ref[:, part * rows : (part + 1) * rows, :].reshape(devices * rows, width)
+        out_ref[:, part * width : (part + 1) * width] += jnp.dot(conv_act, block, preferred_element_type=F32)
+
+
+def last_kernel(act_ref, value_ref, gate_ref, branch_ref, out_ref, acc_ref):
+    step = pl.program_id(0)
+    width = act_ref.shape[2]
+    devices = value_ref.shape[0]
+    rows = value_ref.shape[1] // 2
+
+    @pl.when(step == 0)
+    def _():
+        acc_ref[...] = jnp.zeros_like(acc_ref)
+
     activated = act_ref[0]
-    for part in range(6):
-        block = weights_ref[:, part * rows : (part + 1) * rows, :].reshape(devices * rows, width)
+    for part in range(4):
+        ref = (value_ref, value_ref, gate_ref, gate_ref)[part]
+        at = part % 2 * rows
+        block = ref[:, at : at + rows, :].reshape(devices * rows, width)
         acc_ref[:, part * width : (part + 1) * width] += jnp.dot(
-            conv_act if part < 2 else activated, block, preferred_element_type=F32
+            activated, block, preferred_element_type=F32
         )
 
     @pl.when(step == pl.num_programs(0) - 1)
     def _():
         columns = 2 * width
         out_ref[...] = (
-            acc_ref[:, :columns]
-            + acc_ref[:, columns : 2 * columns] * jax.nn.sigmoid(acc_ref[:, 2 * columns :])
+            branch_ref[...] + acc_ref[:, :columns] * jax.nn.sigmoid(acc_ref[:, columns:])
         ).astype(BF)
 
 
@@ -167,10 +219,14 @@
     return pl.BlockSpec(shape, lambda *_: (0,) * len(shape))
 
 
-def packed(real, imag):
-    n, s = real.shape
-    both = jnp.stack([real.reshape(n, s // LANES, LANES), imag.reshape(n, s // LANES, LANES)], axis=2)
-    return both.reshape(n, 2 * s)
+def spread(blocks, size):
+    total, b = blocks.shape
+    wide = total // size * b
+    pick = lax.broadcasted_iota(jnp.int32, (b, wide), 1) % b == lax.broadcasted_iota(jnp.int32, (b, wide), 0)
+    tiled = jnp.dot(blocks.astype(BF), pick.astype(BF), preferred_element_type=F32)
+    row = lax.broadcasted_iota(jnp.int32, tiled.shape, 0) // size
+    col = lax.broadcasted_iota(jnp.int32, tiled.shape, 1) // b
+    return jnp.where(row == col, tiled, 0.0).astype(BF)
 
 
 def rows_of(real, imag):
@@ -205,11 +261,11 @@
     length, model = tokens.shape
     rows_in, width = conv_value.shape
     rows_out, columns = conv_project.shape
-    shard = jnp.concatenate(
-        [conv_value, conv_gate, state_feed]
-        + [w[:, at : at + width] for w in (conv_project, state_value, state_gate) for at in (0, width)],
-        axis=0,
-    )
+    shard = pl.pallas_call(
+        pack_kernel,
+        out_shape=jax.ShapeDtypeStruct((3 * rows_in + 3 * rows_out * (columns // width), width), BF),
+        name="pack",
+    )(conv_value, conv_gate, state_feed, conv_project, state_value, state_gate)
     gathered = lax.all_gather(shard, "sp", axis=0, tiled=False)
 
     floats = tokens.astype(F32)
@@ -231,25 +287,23 @@
     drive_real = factor_real[..., None] * input_real - factor_imag[..., None] * input_imag
     drive_imag = factor_real[..., None] * input_imag + factor_imag[..., None] * input_real
 
-    def spread(blocks):
-        g, a, b = blocks.shape
-        row = lax.broadcasted_iota(jnp.int32, (g * a, g * b), 0) // a
-        col = lax.broadcasted_iota(jnp.int32, (g * a, g * b), 1) // b
-        return jnp.where(row == col, jnp.tile(blocks.reshape(g * a, b), (1, g)), 0.0)
-
-    drive = packed(
-        spread(jnp.swapaxes(drive_real, 1, 2)), spread(jnp.swapaxes(drive_imag, 1, 2))
-    ).astype(BF)
-    mix = jnp.swapaxes(packed(
-        spread(output_real), -spread(output_imag)
-    ), 0, 1).astype(BF)
+    drive_real = spread(jnp.swapaxes(drive_real, 1, 2).reshape(groups * group_size, state_size), group_size)
+    drive_imag = spread(jnp.swapaxes(drive_imag, 1, 2).reshape(groups * group_size, state_size), group_size)
+    mix_real = spread(jnp.swapaxes(output_real, 1, 2).reshape(flat, group_size), state_size)
+    mix_imag = spread(jnp.swapaxes(-output_imag, 1, 2).reshape(flat, group_size), state_size)
 
     base_real = step_real.reshape(flat)
     base_imag = step_imag.reshape(flat)
     square_size = base_real * base_real + base_imag * base_imag
-    counted = lax.iota(jnp.int32, length) + 1
-    power_real, power_imag = power_table(base_real, base_imag, counted, length)
-    undo_real, undo_imag = power_table(base_real / square_size, -base_imag / square_size, counted, length)
+
+    def powers(real, imag):
+        low = power_table(real, imag, lax.iota(jnp.int32, 8) + 1, 8)
+        high = power_table(real, imag, lax.iota(jnp.int32, length // 8) * 8, length)
+        table = rotate(high[0][:, None], high[1][:, None], low[0][None], low[1][None])
+        return tuple(part.reshape(length, flat) for part in table)
+
+    power_real, power_imag = powers(base_real, base_imag)
+    undo_real, undo_imag = powers(base_real / square_size, -base_imag / square_size)
     span_real, span_imag = (power_real[-1], power_imag[-1])
     device_ids = lax.iota(jnp.int32, seq_devices)
     lag = position - device_ids
@@ -264,36 +318,43 @@
             initial_state[1].reshape(1, flat),
         )
     )
-    power = packed(power_real, power_imag)
-    undo = packed(undo_real, undo_imag)
+    (
+        normed, drive_real, drive_imag, mix_real, mix_imag, power_real, power_imag, undo_real, undo_imag, lead, tail, ends
+    ) = lax.optimization_barrier((
+        normed, drive_real, drive_imag, mix_real, mix_imag, power_real, power_imag, undo_real, undo_imag, lead, tail, ends
+    ))
     chunks = flat // LANES
 
     steps = 8
     per_step = seq_devices // steps
-    gated, feed, sums, total = pl.pallas_call(
+    gated, feed, sums_real, sums_imag, total = pl.pallas_call(
         first_kernel,
         grid=(steps,),
         in_specs=[
             pl.BlockSpec((length, model // steps), lambda k: (0, k)),
             pl.BlockSpec((per_step, 3 * rows_in, width), lambda k: (k, 0, 0)),
-            whole(drive.shape),
-            whole(undo.shape),
+            whole(drive_real.shape),
+            whole(drive_imag.shape),
+            whole(undo_real.shape),
+            whole(undo_imag.shape),
         ],
         out_specs=[
             whole((length, width)),
             whole((length, width)),
-            whole((length, 2 * flat)),
+            whole((length, flat)),
+            whole((length, flat)),
             whole((seq_devices, 2 * chunks, LANES)),
         ],
         out_shape=[
             jax.ShapeDtypeStruct((length, width), BF),
             jax.ShapeDtypeStruct((length, width), BF),
-            jax.ShapeDtypeStruct((length, 2 * flat), F32),
+            jax.ShapeDtypeStruct((length, flat), F32),
+            jax.ShapeDtypeStruct((length, flat), F32),
             jax.ShapeDtypeStruct((seq_devices, 2 * chunks, LANES), F32),
         ],
         scratch_shapes=[pltpu.VMEM((length, 3 * width), F32), pltpu.VMEM((2 * chunks, LANES), F32)],
         name="first",
-    )(normed, gathered, drive, undo)
+    )(normed, gathered, drive_real, drive_imag, undo_real, undo_imag)
 
     taps = conv_taps.shape[0]
     halo = (taps - 1 + 15) // 16 * 16
@@ -315,36 +376,50 @@
             jax.ShapeDtypeStruct((tp_devices, length, width), BF),
             jax.ShapeDtypeStruct((2 * chunks, LANES), F32),
         ],
+        scratch_shapes=[pltpu.VMEM((2 * chunks, LANES), F32)],
         name="second",
-    )(totals, lead, tail, ends, power, sums, mix, feed, skip_gain.reshape(1, width))
+    )(
+        totals, lead, tail, ends, power_real, power_imag, sums_real, sums_imag, mix_real, mix_imag, feed,
+        skip_gain.reshape(1, width),
+    )
     final_state = final.reshape(2, groups, state_size)
     act_rows = lax.all_to_all(act_copies, "tp", 0, 0, tiled=True)
 
+    per_block = seq_devices // tp_devices
+    first_out = 3 * rows_in // (2 * rows_out)
+    branch = pl.pallas_call(
+        branch_kernel,
+        grid=(tp_devices,),
+        in_specs=[
+            whole((tp_devices, length, width)),
+            pl.BlockSpec((per_block, 2 * rows_out, width), lambda k: (k, first_out, 0)),
+            pl.BlockSpec((1, 1, width), lambda k: (k, 0, 0)),
+            pl.BlockSpec((1, 1, width), lambda k: (k, 0, 0)),
+        ],
+        out_specs=whole((length, columns)),
+        out_shape=jax.ShapeDtypeStruct((length, columns), F32),
+        scratch_shapes=[pltpu.VMEM((length, width), F32), pltpu.VMEM((length, width), F32)],
+        name="branch",
+    )(
+        conv_rows,
+        gathered,
+        chan_gain.reshape(tp_devices, 1, width),
+        chan_shift.reshape(tp_devices, 1, width),
+    )
     mixer_out = pl.pallas_call(
         last_kernel,
         grid=(tp_devices,),
         in_specs=[
-            whole((tp_devices, length, width)),
             pl.BlockSpec((1, length, width), lambda k: (k, 0, 0)),
-            pl.BlockSpec((seq_devices // tp_devices, 3 * rows_in, width), lambda k: (k, 1, 0)),
-            pl.BlockSpec((1, 1, width), lambda k: (k, 0, 0)),
-            pl.BlockSpec((1, 1, width), lambda k: (k, 0, 0)),
+            pl.BlockSpec((per_block, 2 * rows_out, width), lambda k: (k, first_out + 1, 0)),
+            pl.BlockSpec((per_block, 2 * rows_out, width), lambda k: (k, first_out + 2, 0)),
+            whole((length, columns)),
         ],
         out_specs=whole((length, columns)),
         out_shape=jax.ShapeDtypeStruct((length, columns), BF),
-        scratch_shapes=[
-            pltpu.VMEM((length, 6 * width), F32),
-            pltpu.VMEM((length, width), F32),
-            pltpu.VMEM((length, width), F32),
-        ],
+        scratch_shapes=[pltpu.VMEM((length, 4 * width), F32)],
         name="last",
-    )(
-        conv_rows,
-        act_rows,
-        gathered,
-        chan_gain.reshape(tp_devices, 1, width),
-        chan_shift.reshape(tp_devices, 1, width),
-    )
+    )(act_rows, gathered, gathered, branch)
     return (mixer_out, final_state)
 
 

time: 230 us -> 225 us (0.978)
  other arithmetic: 85 us -> 12.8 us
  waiting for transfers between devices: 60.2 us -> 131 us
  local copies, waits for them, and re-layouts: 19.1 us -> 4.21 us
  Pallas kernels: 24.8 us -> 31.9 us
  matrix products: 0 us -> 5.52 us
    all_gather x1, waiting for transfers between devices: 43.3 us -> 107 us  [local(): gathered = lax.all_gather(shard, 'sp', axis=0, tiled=False)]
    select_n x8 -> x7, other arithmetic: 55.2 us -> 1.44 us  [power_table(): result_real = jnp.where(chosen, next_real, result_real)]
    select_n x5 -> x3, other arithmetic: 14.8 us -> 1.06 us  [power_table(): result_imag = jnp.where(chosen, next_imag, result_imag)]
    unnamed x48 -> x22, local copies, waits for them, and re-layouts: 8.44 us -> 1.54 us
    all_to_all x1, waiting for transfers between devices: 1.1 us -> 7.97 us  [local(): conv_rows = lax.all_to_all(conv_copies, 'tp', 0, 0, tiled=True)]
    pallas_call x1 -> x3, Pallas kernels: 8.06 us -> 14.8 us  [the longest x1 6.76 us: local(): pl.pallas_call(last_kernel, grid=(tp_devices,), in_specs=[pl.BlockSpec((1...]
    all_to_all x1, waiting for transfers between devices: 11.5 us -> 4.99 us  [local(): act_rows = lax.all_to_all(act_copies, 'tp', 0, 0, tiled=True)]
    another operation x6 -> x0, other arithmetic: 5.9 us -> none  [the longest x4 4.01 us: packed(): jnp.stack([real.reshape(n, s // LANES, LANES), imag.reshape(n, s // LANES...]
  transfers between devices with their start and end apart: 5 -> 5, of which waited for: 4 -> 5; matrix products, arithmetic and copies ran while one was open for 42% -> 9% of each run, Pallas kernels for 3% -> 6%
where the time goes in v2:
time: 225 us; the launch traced here: 224 us
  waiting for transfers between devices  131 us (58%)
  Pallas kernels  31.9 us (14%)
  starting transfers between devices  24.4 us (11%)
  between operations  14.4 us (6%)
  other arithmetic  12.8 us (6%)
  matrix products  5.52 us (2%)
  local copies, waits for them, and re-layouts  4.21 us (2%)
    all_gather x1, waiting for transfers between devices, local(): gathered = lax.all_gather(shard, 'sp', axis=0, tiled=False)  107 us
    pallas_call x1, Pallas kernels, local(): pl.pallas_call(first_kernel, grid=(steps,), in_specs=[pl.BlockSpec((lengt...  10.2 us
    all_to_all x1, starting transfers between devices, local(): totals = lax.all_to_all(total, 'sp', 0, 0, tiled=True)  9.79 us
    all_to_all x1, waiting for transfers between devices, local(): conv_rows = lax.all_to_all(conv_copies, 'tp', 0, 0, tiled=True)  7.97 us
    all_to_all x1, starting transfers between devices, local(): conv_rows = lax.all_to_all(conv_copies, 'tp', 0, 0, tiled=True)  7.28 us
    pallas_call x1, Pallas kernels, local(): pl.pallas_call(last_kernel, grid=(tp_devices,), in_specs=[pl.BlockSpec((1...  6.76 us
    pallas_call x1, Pallas kernels, local(): pl.pallas_call(branch_kernel, grid=(tp_devices,), in_specs=[whole((tp_dev...  6.52 us
    all_to_all x1, waiting for transfers between devices, local(): totals = lax.all_to_all(total, 'sp', 0, 0, tiled=True)  6.46 us
  transfers between devices with their start and end apart: 5, of which 5 were waited for; matrix products, arithmetic and copies ran while one was open for 9% of the time, Pallas kernels for 6%

profile of v2, /device:TPU:1, one launch (start us, length us, event | category | flops | bytes accessed | tf_op | source)
XLA Modules:
  0.0 224.3 jit_solution(17744355127922881419)
XLA Ops:
  7.2 1.5 pack.1
  10.5 0.9 convert_bitcast_fusion
  11.6 0.9 fusion.55
  20.3 1.7 fusion.7.mix_imag_ref
  22.0 1.6 fusion.8.mix_real_ref
  23.6 1.1 fusion.5.drive_real_ref
  24.7 1.1 fusion.6.drive_imag_ref
  25.8 1.4 add_bitcast_fusion
  27.2 1.6 fusion.2.normed_ref
  28.8 107.5 %all-gather.3.cloned.1.call-done = bf16[24576,256]{1,0:T(8,128)(2,1)} async-done(((bf16[384,256]{1,0:T(8,128)(2,1)}), bf16[24576,256]{1,0:T(8,128)(2,1)}) %all-gather.3.cloned.1.call-update) | async-done | bytes 12582928 | tf_op jit(solution)/shard_map/all_gather | solution.py:269
  136.3 10.2 %first.1 = (bf16[192,256]{1,0:T(8,128)(2,1)}, bf16[192,256]{1,0:T(8,128)(2,1)}, f32[192,1024]{1,0:T(8,128)}, f32[192,1024]{1,0:T(8,128)}, f32[64,16,128]{2,1,0:T(8,128)}) custom-call(bf16[192,4096]{1,0:T(8,128)(2,1)} %fusion.2.normed_ref, bf16[64,384,256]{2,1,0:T(8,128)(2,1)} %bitcast.57, bf16[256,1024]{1,0:T(8,128)(2,1)} %fusion.5.drive_real_ref, ...), custom_call_target="tpu_custom_call" | custom-call | tf_op jit(solution)/shard_map/first/pallas_call | solution.py:330
  146.5 9.8 %all-to-all-start = ((f32[64,16,128]{2,1,0:T(8,128)}), f32[64,16,128]{2,1,0:T(8,128)S(1)}, u32[]{:S(2)}, u32[]{:S(2)}) async-start(f32[64,16,128]{2,1,0:T(8,128)} %get-tuple-element.26), calls=%async_computation | async-start | bytes 1048576 | tf_op jit(solution)/shard_map/all_to_all | solution.py:364
  157.0 2.9 %collective-permute-start = (bf16[32,256]{1,0:T(8,128)(2,1)S(1)}, bf16[32,256]{1,0:T(8,128)(2,1)S(1)}, u32[]{:S(2)}, u32[]{:S(2)}) collective-permute-start(bf16[32,256]{1,0:T(8,128)(2,1)S(1)} %slice.19), channel_id=1, source_target_pairs={{0,8},{8,16},{16,24},{24,32},{32,40},{40,48},{48,56},{56,64},{64,7... | collective-permute-start | bytes 49160 | tf_op jit(solution)/shard_map/ppermute | solution.py:361
  159.9 4.1 %collective-permute-done.before_ref = bf16[32,256]{1,0:T(8,128)(2,1)S(1)} collective-permute-done((bf16[32,256]{1,0:T(8,128)(2,1)S(1)}, bf16[32,256]{1,0:T(8,128)(2,1)S(1)}, u32[]{:S(2)}, u32[]{:S(2)}) %collective-permute-start) | collective-permute-done | bytes 16416 | tf_op jit(solution)/shard_map/ppermute | solution.py:361
  164.6 2.7 %conv.1 = bf16[8,192,256]{2,1,0:T(8,128)(2,1)} custom-call(bf16[32,256]{1,0:T(8,128)(2,1)} %copy-done.9, bf16[192,256]{1,0:T(8,128)(2,1)} %get-tuple-element.38.gated_ref, f32[31,256]{1,0:T(8,128)} %taps_ref.1), custom_call_target="tpu_custom_call" | custom-call | tf_op jit(solution)/shard_map/conv/pallas_call | solution.py:365
  167.3 6.5 %all-to-all-done.totals_ref = f32[64,16,128]{2,1,0:T(8,128)S(1)} async-done(((f32[64,16,128]{2,1,0:T(8,128)}), f32[64,16,128]{2,1,0:T(8,128)S(1)}, u32[]{:S(2)}, u32[]{:S(2)}) %all-to-all-start) | async-done | bytes 524320 | tf_op jit(solution)/shard_map/all_to_all | solution.py:364
  173.7 7.3 %all-to-all-start.2 = ((bf16[8,192,256]{2,1,0:T(8,128)(2,1)}), bf16[8,192,256]{2,1,0:T(8,128)(2,1)S(1)}, u32[]{:S(2)}, u32[]{:S(2)}) async-start(bf16[8,192,256]{2,1,0:T(8,128)(2,1)} %conv.1), calls=%async_computation.2 | async-start | bytes 1572864 | tf_op jit(solution)/shard_map/all_to_all | solution.py:371
  181.0 4.2 %second.1 = (bf16[8,192,256]{2,1,0:T(8,128)(2,1)}, f32[16,128]{1,0:T(8,128)}) custom-call(f32[64,16,128]{2,1,0:T(8,128)} %copy-done.5, f32[64,16,128]{2,1,0:T(8,128)} %pad_maximum_fusion.lead_ref, f32[64,16,128]{2,1,0:T(8,128)} %pad_maximum_fusion.1.tail_ref, f32[2,16,128]{2,1,0:T(8,128)} %pad_maximum_fusion.2.ends_ref, f32[192,1024]{1,0:T(8,128)} %copy-done.2, ...), custom_call_target="tpu_custom_call" | custom-call | tf_op jit(solution)/shard_map/second/pallas_call | solution.py:373
  185.2 8.0 %all-to-all-done.2.conv_ref = bf16[8,192,256]{2,1,0:T(8,128)(2,1)S(1)} async-done(((bf16[8,192,256]{2,1,0:T(8,128)(2,1)}), bf16[8,192,256]{2,1,0:T(8,128)(2,1)S(1)}, u32[]{:S(2)}, u32[]{:S(2)}) %all-to-all-start.2) | async-done | bytes 786464 | tf_op jit(solution)/shard_map/all_to_all | solution.py:371
  193.2 4.4 %all-to-all-start.1 = ((bf16[8,192,256]{2,1,0:T(8,128)(2,1)}), bf16[8,192,256]{2,1,0:T(8,128)(2,1)S(1)}, u32[]{:S(2)}, u32[]{:S(2)}) async-start(bf16[8,192,256]{2,1,0:T(8,128)(2,1)} %get-tuple-element.37), calls=%async_computation.1 | async-start | bytes 1572864 | tf_op jit(solution)/shard_map/all_to_all | solution.py:386
  197.6 6.5 %branch.1.branch_ref = f32[192,512]{1,0:T(8,128)} custom-call(bf16[8,192,256]{2,1,0:T(8,128)(2,1)} %copy-done.4, bf16[64,384,256]{2,1,0:T(8,128)(2,1)} %bitcast.58, f32[8,1,256]{2,1,0:T(1,128)} %bitcast.129, f32[8,1,256]{2,1,0:T(1,128)} %bitcast.130), custom_call_target="tpu_custom_call" | custom-call | tf_op jit(solution)/shard_map/branch/pallas_call | solution.py:390
  204.8 5.0 %all-to-all-done.1.act_ref = bf16[8,192,256]{2,1,0:T(8,128)(2,1)S(1)} async-done(((bf16[8,192,256]{2,1,0:T(8,128)(2,1)}), bf16[8,192,256]{2,1,0:T(8,128)(2,1)S(1)}, u32[]{:S(2)}, u32[]{:S(2)}) %all-to-all-start.1) | async-done | bytes 786464 | tf_op jit(solution)/shard_map/all_to_all | solution.py:386
  209.8 0.9 copy-done.3
  210.7 6.8 %last.1 = bf16[192,512]{1,0:T(8,128)(2,1)} custom-call(bf16[8,192,256]{2,1,0:T(8,128)(2,1)} %copy-done.3, bf16[64,384,256]{2,1,0:T(8,128)(2,1)} %bitcast.59, bf16[64,384,256]{2,1,0:T(8,128)(2,1)} %bitcast.60, f32[192,512]{1,0:T(8,128)} %branch.1.branch_ref), custom_call_target="tpu_custom_call" | custom-call | tf_op jit(solution)/shard_map/last/pallas_call | solution.py:409
  (86 shorter events, 11.4 us)
Async XLA Ops:
  7.2 129.1 %all-gather.3.cloned.1.call-start = ((), (), s32[]{:S(2)}) async-start(), calls=%async_computation.3 | async-start | bytes 12779520 | tf_op jit(solution)/shard_map/all_gather | solution.py:269
  13.0 6.1 %copy-start = (bf16[192,4096]{1,0:T(8,128)(2,1)S(1)}, bf16[192,4096]{1,0:T(8,128)(2,1)}, u32[]{:S(2)}) copy-start(bf16[192,4096]{1,0:T(8,128)(2,1)} %param.19) | copy-start | bytes 4718596
  14.0 6.3 %copy-start.1 = (f32[192,1024]{1,0:T(8,128)}, f32[192,1024]{1,0:T(8,128)S(1)}, u32[]{:S(2)}) copy-start(f32[192,1024]{1,0:T(8,128)S(1)} %get-tuple-element.31.power_imag_ref) | copy-start | bytes 2359300
  14.0 6.3 %copy-start.2 = (f32[192,1024]{1,0:T(8,128)}, f32[192,1024]{1,0:T(8,128)S(1)}, u32[]{:S(2)}) copy-start(f32[192,1024]{1,0:T(8,128)S(1)} %get-tuple-element.30.power_real_ref) | copy-start | bytes 2359300
  14.0 6.2 %copy-start.6 = (f32[16,64,16]{1,2,0:T(8,128)S(1)}, f32[16,64,16]{1,2,0:T(8,128)}, u32[]{:S(2)}) copy-start(f32[16,64,16]{1,2,0:T(8,128)} %param.30) | copy-start | bytes 196612
  14.0 6.2 %copy-start.7 = (f32[16,64,16]{1,2,0:T(8,128)S(1)}, f32[16,64,16]{1,2,0:T(8,128)}, u32[]{:S(2)}) copy-start(f32[16,64,16]{1,2,0:T(8,128)} %param.31) | copy-start | bytes 196612
  23.6 3.6 %copy-start.8 = (f32[4096]{0:T(1024)S(1)}, f32[4096]{0:T(1024)}, u32[]{:S(2)}) copy-start(f32[4096]{0:T(1024)} %param.20) | copy-start | bytes 49156
  146.5 27.2 %all-to-all-start = ((f32[64,16,128]{2,1,0:T(8,128)}), f32[64,16,128]{2,1,0:T(8,128)S(1)}, u32[]{:S(2)}, u32[]{:S(2)}) async-start(f32[64,16,128]{2,1,0:T(8,128)} %get-tuple-element.26), calls=%async_computation | async-start | bytes 1048576 | tf_op jit(solution)/shard_map/all_to_all | solution.py:364
  157.0 7.0 %collective-permute-start = (bf16[32,256]{1,0:T(8,128)(2,1)S(1)}, bf16[32,256]{1,0:T(8,128)(2,1)S(1)}, u32[]{:S(2)}, u32[]{:S(2)}) collective-permute-start(bf16[32,256]{1,0:T(8,128)(2,1)S(1)} %slice.19), channel_id=1, source_target_pairs={{0,8},{8,16},{16,24},{24,32},{32,40},{40,48},{48,56},{56,64},{64,7... | collective-permute-start | bytes 49160 | tf_op jit(solution)/shard_map/ppermute | solution.py:361
  164.0 0.6 copy-start.9
  173.7 7.3 %copy-start.5 = (f32[64,16,128]{2,1,0:T(8,128)}, f32[64,16,128]{2,1,0:T(8,128)S(1)}, u32[]{:S(2)}) copy-start(f32[64,16,128]{2,1,0:T(8,128)S(1)} %all-to-all-done.totals_ref) | copy-start | bytes 1572868
  173.7 19.4 %all-to-all-start.2 = ((bf16[8,192,256]{2,1,0:T(8,128)(2,1)}), bf16[8,192,256]{2,1,0:T(8,128)(2,1)S(1)}, u32[]{:S(2)}, u32[]{:S(2)}) async-start(bf16[8,192,256]{2,1,0:T(8,128)(2,1)} %conv.1), calls=%async_computation.2 | async-start | bytes 1572864 | tf_op jit(solution)/shard_map/all_to_all | solution.py:371
  193.2 4.4 %copy-start.4 = (bf16[8,192,256]{2,1,0:T(8,128)(2,1)}, bf16[8,192,256]{2,1,0:T(8,128)(2,1)S(1)}, u32[]{:S(2)}) copy-start(bf16[8,192,256]{2,1,0:T(8,128)(2,1)S(1)} %all-to-all-done.2.conv_ref) | copy-start | bytes 2359300
  193.2 16.6 %all-to-all-start.1 = ((bf16[8,192,256]{2,1,0:T(8,128)(2,1)}), bf16[8,192,256]{2,1,0:T(8,128)(2,1)S(1)}, u32[]{:S(2)}, u32[]{:S(2)}) async-start(bf16[8,192,256]{2,1,0:T(8,128)(2,1)} %get-tuple-element.37), calls=%async_computation.1 | async-start | bytes 1572864 | tf_op jit(solution)/shard_map/all_to_all | solution.py:386
  197.6 6.5 %copy-start.10 = (f32[16,128]{1,0:T(8,128)S(1)}, f32[16,128]{1,0:T(8,128)}, u32[]{:S(2)}) copy-start(f32[16,128]{1,0:T(8,128)} %get-tuple-element.39) | copy-start | bytes 24580
  209.8 0.9 copy-start.3
Sparse Core Ops, SparseCore 0:
  11.6 124.6 all-gather.2

commit v3 on v2

--- a/solution.py
+++ b/solution.py
@@ -1,11 +1,9 @@
-import functools
-
 import jax
 import jax.numpy as jnp
 from jax import lax
 from jax.experimental import pallas as pl
 from jax.experimental.pallas import tpu as pltpu
-from jax.sharding import Mesh, PartitionSpec as P
+from jax.sharding import PartitionSpec as P
 
 BF = jnp.bfloat16
 F32 = jnp.float32
@@ -55,47 +53,57 @@
     sums_real_ref,
     sums_imag_ref,
     total_ref,
+    buffer_ref,
     acc_ref,
     last_ref,
+    sems,
 ):
-    step = pl.program_id(0)
-    devices, _, width = weights_ref.shape
-    rows = weights_ref.shape[1] // 3
-
-    @pl.when(step == 0)
-    def _():
-        acc_ref[...] = jnp.zeros_like(acc_ref)
-
-    for kind in range(3):
-        block = weights_ref[:, kind * rows : (kind + 1) * rows, :].reshape(devices * rows, width)
-        acc_ref[:, kind * width : (kind + 1) * width] += jnp.dot(
-            normed_ref[...], block, preferred_element_type=F32
-        )
-
-    @pl.when(step == pl.num_programs(0) - 1)
-    def _():
-        length = acc_ref.shape[0]
-        gated_ref[...] = (acc_ref[:, :width] * jax.nn.sigmoid(acc_ref[:, width : 2 * width])).astype(BF)
-        feed = acc_ref[:, 2 * width :].astype(BF)
-        feed_ref[...] = feed
-        lower = (
-            lax.broadcasted_iota(jnp.int32, (length, length), 0)
-            >= lax.broadcasted_iota(jnp.int32, (length, length), 1)
-        ).astype(BF)
-        flat = sums_real_ref.shape[1]
-        half = last_ref.shape[0] // 2
-        for at in range(0, flat, CHUNK):
-            cols = slice(at, at + CHUNK)
-            pushed_real = jnp.dot(feed, drive_real_ref[:, cols], preferred_element_type=F32)
-            pushed_imag = jnp.dot(feed, drive_imag_ref[:, cols], preferred_element_type=F32)
-            scaled = rotate(undo_real_ref[:, cols], undo_imag_ref[:, cols], pushed_real, pushed_imag)
-            for part, ref in enumerate((sums_real_ref, sums_imag_ref)):
-                sums = jnp.dot(lower, scaled[part].astype(BF), preferred_element_type=F32)
-                ref[:, cols] = sums
-                for lane in range(0, CHUNK, LANES):
-                    row = part * half + (at + lane) // LANES
-                    last_ref[row : row + 1, :] = sums[length - 1 :, lane : lane + LANES]
-        total_ref[...] = jnp.broadcast_to(last_ref[...][None], total_ref.shape)
+    devices, rows, width = buffer_ref.shape
+    rows //= 3
+    parts = sems.shape[0]
+    per_part = devices // parts
+
+    def fetch(part):
+        at = pl.ds(part * per_part, per_part)
+        return pltpu.make_async_copy(weights_ref.at[at, pl.ds(0, 3 * rows)], buffer_ref.at[at], sems.at[part])
+
+    for part in range(parts):
+        fetch(part).start()
+    span = per_part * rows
+    for part in range(parts):
+        fetch(part).wait()
+        for kind in range(3):
+            block = buffer_ref[
+                part * per_part : (part + 1) * per_part, kind * rows : (kind + 1) * rows, :
+            ].reshape(span, width)
+            product = jnp.dot(
+                normed_ref[:, part * span : (part + 1) * span], block, preferred_element_type=F32
+            )
+            cols = slice(kind * width, (kind + 1) * width)
+            acc_ref[:, cols] = product if part == 0 else acc_ref[:, cols] + product
+
+    length = acc_ref.shape[0]
+    feed = acc_ref[:, 2 * width :].astype(BF)
+    feed_ref[...] = feed
+    lower = (
+        lax.broadcasted_iota(jnp.int32, (length, length), 0)
+        >= lax.broadcasted_iota(jnp.int32, (length, length), 1)
+    ).astype(BF)
+    flat = sums_real_ref.shape[1]
+    half = last_ref.shape[0] // 2
+    for at in range(0, flat, CHUNK):
+        cols = slice(at, at + CHUNK)
+        pushed_real = jnp.dot(feed, drive_real_ref[:, cols], preferred_element_type=F32)
+        pushed_imag = jnp.dot(feed, drive_imag_ref[:, cols], preferred_element_type=F32)
+        scaled = rotate(undo_real_ref[:, cols], undo_imag_ref[:, cols], pushed_real, pushed_imag)
+        for part, ref in enumerate((sums_real_ref, sums_imag_ref)):
+            sums = jnp.dot(lower, scaled[part].astype(BF), preferred_element_type=F32)
+            ref[:, cols] = sums
+            for lane in range(0, CHUNK, LANES):
+                row = part * half + (at + lane) // LANES
+                last_ref[row : row + 1, :] = sums[length - 1 :, lane : lane + LANES]
+    total_ref[...] = jnp.broadcast_to(last_ref[...][None], total_ref.shape)
+    gated_ref[...] = (acc_ref[:, :width] * jax.nn.sigmoid(acc_ref[:, width : 2 * width])).astype(BF)
 
 
 def conv_kernel(before_ref, gated_ref, taps_ref, out_ref, pad_ref):
@@ -110,9 +118,7 @@
         for tap in range(taps):
             start = lead - (taps - 1) + tap
             acc = acc + taps_ref[tap : tap + 1, cols] * pad_ref[start : start + length, cols]
-        rounded = acc.astype(BF)
-        for copy in range(out_ref.shape[0]):
-            out_ref[copy, :, cols] = rounded
+        out_ref[:, cols] = acc.astype(BF)
 
 
 def second_kernel(
@@ -128,6 +134,7 @@
     mix_imag_ref,
     feed_ref,
     skip_ref,
+    conv_ref,
     out_ref,
     final_ref,
     entry_ref,
@@ -155,64 +162,67 @@
         response = response + jnp.dot(state_real.astype(BF), mix_real_ref[cols, :], preferred_element_type=F32)
         response = response + jnp.dot(state_imag.astype(BF), mix_imag_ref[cols, :], preferred_element_type=F32)
     activated = jax.nn.gelu(response).astype(BF)
+    length = activated.shape[0]
+    conv = conv_ref[...]
     for copy in range(out_ref.shape[0]):
-        out_ref[copy] = activated
-
-
-def branch_kernel(conv_ref, weights_ref, gain_ref, shift_ref, out_ref, mean_ref, scale_ref):
-    step = pl.program_id(0)
-    blocks, length, width = conv_ref.shape
-    devices = weights_ref.shape[0]
-    rows = weights_ref.shape[1] // 2
-
-    @pl.when(step == 0)
-    def _():
-        out_ref[...] = jnp.zeros_like(out_ref)
-        channels = blocks * width
-        total = jnp.zeros((length, width), F32)
-        for at in range(blocks):
-            total = total + conv_ref[at].astype(F32)
-        mean = jnp.sum(total, axis=1, keepdims=True) / channels
-        spread = jnp.zeros((length, width), F32)
-        for at in range(blocks):
-            centred = conv_ref[at].astype(F32) - mean
-            spread = spread + centred * centred
-        variance = jnp.sum(spread, axis=1, keepdims=True) / channels
-        mean_ref[...] = jnp.broadcast_to(mean, mean_ref.shape)
-        scale_ref[...] = jnp.broadcast_to(lax.rsqrt(variance + 1e-05), scale_ref.shape)
-
-    centred = conv_ref[step].astype(F32) - mean_ref[...]
-    conv_act = jax.nn.silu(centred * scale_ref[...] * gain_ref[0] + shift_ref[0]).astype(BF)
-    for part in range(2):
-        block = weights_ref[:, part * rows : (part + 1) * rows, :].reshape(devices * rows, width)
-        out_ref[:, part * width : (part + 1) * width] += jnp.dot(conv_act, block, preferred_element_type=F32)
-
-
-def last_kernel(act_ref, value_ref, gate_ref, branch_ref, out_ref, acc_ref):
-    step = pl.program_id(0)
-    width = act_ref.shape[2]
-    devices = value_ref.shape[0]
-    rows = value_ref.shape[1] // 2
-
-    @pl.when(step == 0)
-    def _():
-        acc_ref[...] = jnp.zeros_like(acc_ref)
-
-    activated = act_ref[0]
-    for part in range(4):
-        ref = (value_ref, value_ref, gate_ref, gate_ref)[part]
-        at = part % 2 * rows
-        block = ref[:, at : at + rows, :].reshape(devices * rows, width)
-        acc_ref[:, part * width : (part + 1) * width] += jnp.dot(
-            activated, block, preferred_element_type=F32
+        out_ref[copy, :length] = conv
+        out_ref[copy, length:] = activated
+
+
+def last_kernel(rows_ref, weights_ref, gain_ref, shift_ref, out_ref, buffer_ref, act_ref, acc_ref, sems):
+    blocks, length, width = rows_ref.shape
+    length //= 2
+    devices, rows, _ = buffer_ref.shape
+    rows //= 6
+    parts = sems.shape[0]
+    per_part = devices // parts
+    per_block = blocks // parts
+
+    def fetch(part):
+        at = pl.ds(part * per_part, per_part)
+        return pltpu.make_async_copy(
+            weights_ref.at[at, pl.ds(6 * rows, 6 * rows)], buffer_ref.at[at], sems.at[part]
         )
 
-    @pl.when(step == pl.num_programs(0) - 1)
-    def _():
-        columns = 2 * width
-        out_ref[...] = (
-            branch_ref[...] + acc_ref[:, :columns] * jax.nn.sigmoid(acc_ref[:, columns:])
-        ).astype(BF)
+    for part in range(parts):
+        fetch(part).start()
+    channels = blocks * width
+    total = jnp.zeros((length, width), F32)
+    squares = jnp.zeros((length, width), F32)
+    for at in range(blocks):
+        total = total + rows_ref[at, :length, :].astype(F32)
+    mean = jnp.sum(total, axis=1, keepdims=True) / channels
+    for at in range(blocks):
+        centred = rows_ref[at, :length, :].astype(F32) - mean
+        squares = squares + centred * centred
+    scale = lax.rsqrt(jnp.sum(squares, axis=1, keepdims=True) / channels + 1e-05)
+    for at in range(blocks):
+        centred = rows_ref[at, :length, :].astype(F32) - mean
+        cols = slice(at * width, (at + 1) * width)
+        act_ref[:, cols] = jax.nn.silu(centred * scale * gain_ref[:, cols] + shift_ref[:, cols]).astype(BF)
+    span = per_part * rows
+    for part in range(parts):
+        fetch(part).wait()
+        conv_act = act_ref[:, part * span : (part + 1) * span]
+        activated = jnp.concatenate(
+            [rows_ref[part * per_block + at, length:, :] for at in range(per_block)], axis=1
+        )
+        for kind in range(6):
+            block = buffer_ref[
+                part * per_part : (part + 1) * per_part, kind * rows : (kind + 1) * rows, :
+            ].reshape(span, width)
+            product = jnp.dot(conv_act if kind < 2 else activated, block, preferred_element_type=F32)
+            cols = slice(kind * width, (kind + 1) * width)
+            acc_ref[:, cols] = product if part == 0 else acc_ref[:, cols] + product
+    columns = 2 * width
+    out_ref[...] = (
+        acc_ref[:, :columns]
+        + acc_ref[:, columns : 2 * columns] * jax.nn.sigmoid(acc_ref[:, 2 * columns :])
+    ).astype(BF)
+
+
+def grant(mib):
+    return pltpu.CompilerParams(vmem_limit_bytes=mib << 20)
 
 
 def whole(shape):
@@ -325,25 +335,17 @@
     ))
     chunks = flat // LANES
 
-    steps = 8
-    per_step = seq_devices // steps
+    parts = 4
+    hbm = pl.BlockSpec(memory_space=pltpu.HBM)
     gated, feed, sums_real, sums_imag, total = pl.pallas_call(
         first_kernel,
-        grid=(steps,),
         in_specs=[
-            pl.BlockSpec((length, model // steps), lambda k: (0, k)),
-            pl.BlockSpec((per_step, 3 * rows_in, width), lambda k: (k, 0, 0)),
+            whole(normed.shape),
+            hbm,
             whole(drive_real.shape),
             whole(drive_imag.shape),
             whole(undo_real.shape),
             whole(undo_imag.shape),
-        ],
-        out_specs=[
-            whole((length, width)),
-            whole((length, width)),
-            whole((length, flat)),
-            whole((length, flat)),
-            whole((seq_devices, 2 * chunks, LANES)),
         ],
         out_shape=[
             jax.ShapeDtypeStruct((length, width), BF),
@@ -352,7 +354,13 @@
             jax.ShapeDtypeStruct((length, flat), F32),
             jax.ShapeDtypeStruct((seq_devices, 2 * chunks, LANES), F32),
         ],
-        scratch_shapes=[pltpu.VMEM((length, 3 * width), F32), pltpu.VMEM((2 * chunks, LANES), F32)],
+        scratch_shapes=[
+            pltpu.VMEM((seq_devices, 3 * rows_in, width), BF),
+            pltpu.VMEM((length, 3 * width), F32),
+            pltpu.VMEM((2 * chunks, LANES), F32),
+            pltpu.SemaphoreType.DMA((parts,)),
+        ],
+        compiler_params=grant(24),
         name="first",
     )(normed, gathered, drive_real, drive_imag, undo_real, undo_imag)
 
@@ -362,64 +370,48 @@
         gated[length - halo :], "sp", [(source, source + 1) for source in range(seq_devices - 1)]
     )
     totals = lax.all_to_all(total, "sp", 0, 0, tiled=True)
-    conv_copies = pl.pallas_call(
+    conv_out = pl.pallas_call(
         conv_kernel,
-        out_shape=jax.ShapeDtypeStruct((tp_devices, length, width), BF),
+        out_shape=jax.ShapeDtypeStruct((length, width), BF),
         scratch_shapes=[pltpu.VMEM((halo + length, width), F32)],
+        compiler_params=grant(4),
         name="conv",
     )(before, gated, conv_taps)
-    conv_rows = lax.all_to_all(conv_copies, "tp", 0, 0, tiled=True)
-
-    act_copies, final = pl.pallas_call(
+
+    copies, final = pl.pallas_call(
         second_kernel,
         out_shape=[
-            jax.ShapeDtypeStruct((tp_devices, length, width), BF),
+            jax.ShapeDtypeStruct((tp_devices, 2 * length, width), BF),
             jax.ShapeDtypeStruct((2 * chunks, LANES), F32),
         ],
         scratch_shapes=[pltpu.VMEM((2 * chunks, LANES), F32)],
+        compiler_params=grant(16),
         name="second",
     )(
         totals, lead, tail, ends, power_real, power_imag, sums_real, sums_imag, mix_real, mix_imag, feed,
-        skip_gain.reshape(1, width),
+        skip_gain.reshape(1, width), conv_out,
     )
     final_state = final.reshape(2, groups, state_size)
-    act_rows = lax.all_to_all(act_copies, "tp", 0, 0, tiled=True)
-
-    per_block = seq_devices // tp_devices
-    first_out = 3 * rows_in // (2 * rows_out)
-    branch = pl.pallas_call(
-        branch_kernel,
-        grid=(tp_devices,),
-        in_specs=[
-            whole((tp_devices, length, width)),
-            pl.BlockSpec((per_block, 2 * rows_out, width), lambda k: (k, first_out, 0)),
-            pl.BlockSpec((1, 1, width), lambda k: (k, 0, 0)),
-            pl.BlockSpec((1, 1, width), lambda k: (k, 0, 0)),
-        ],
-        out_specs=whole((length, columns)),
-        out_shape=jax.ShapeDtypeStruct((length, columns), F32),
-        scratch_shapes=[pltpu.VMEM((length, width), F32), pltpu.VMEM((length, width), F32)],
-        name="branch",
-    )(
-        conv_rows,
-        gathered,
-        chan_gain.reshape(tp_devices, 1, width),
-        chan_shift.reshape(tp_devices, 1, width),
-    )
+    exchanged = lax.all_to_all(copies, "tp", 0, 0, tiled=True)
+
     mixer_out = pl.pallas_call(
         last_kernel,
-        grid=(tp_devices,),
         in_specs=[
-            pl.BlockSpec((1, length, width), lambda k: (k, 0, 0)),
-            pl.BlockSpec((per_block, 2 * rows_out, width), lambda k: (k, first_out + 1, 0)),
-            pl.BlockSpec((per_block, 2 * rows_out, width), lambda k: (k, first_out + 2, 0)),
-            whole((length, columns)),
-        ],
-        out_specs=whole((length, columns)),
+            whole(exchanged.shape),
+            hbm,
+            whole((1, chan_gain.shape[0])),
+            whole((1, chan_gain.shape[0])),
+        ],
         out_shape=jax.ShapeDtypeStruct((length, columns), BF),
-        scratch_shapes=[pltpu.VMEM((length, 4 * width), F32)],
+        scratch_shapes=[
+            pltpu.VMEM((seq_devices, 6 * rows_out, width), BF),
+            pltpu.VMEM((length, tp_devices * width), BF),
+            pltpu.VMEM((length, 6 * width), F32),
+            pltpu.SemaphoreType.DMA((parts,)),
+        ],
+        compiler_params=grant(24),
         name="last",
-    )(act_rows, gathered, gathered, branch)
+    )(exchanged, gathered, chan_gain.reshape(1, -1), chan_shift.reshape(1, -1))
     return (mixer_out, final_state)
 
 

time: 225 us -> 231 us (1.027)
  local copies, waits for them, and re-layouts: 4.21 us -> 25.6 us
  Pallas kernels: 31.9 us -> 10.6 us
  waiting for transfers between devices: 131 us -> 143 us
  starting transfers between devices: 24.4 us -> 20.2 us
    unnamed x22 -> x48, local copies, waits for them, and re-layouts: 1.54 us -> 23.7 us
    pallas_call x4 -> x3, Pallas kernels: 26.2 us -> 8.09 us  [the longest x1 3.75 us: local(): pl.pallas_call(first_kernel, in_specs=[whole(normed.shape), hbm, whole(dr...]
    all_to_all x2 -> x1, waiting for transfers between devices: 13 us -> 19.9 us  [local(): exchanged = lax.all_to_all(copies, 'tp', 0, 0, tiled=True)]
    all_to_all x2 -> x1, starting transfers between devices: 11.7 us -> 7.27 us  [local(): exchanged = lax.all_to_all(copies, 'tp', 0, 0, tiled=True)]
    pallas_call x1, Pallas kernels: 4.18 us -> 0.97 us  [local(): pl.pallas_call(second_kernel, out_shape=[jax.ShapeDtypeStruct((tp_devices...]
    all_to_all x1, waiting for transfers between devices: 6.46 us -> 8.94 us  [local(): totals = lax.all_to_all(total, 'sp', 0, 0, tiled=True)]
  transfers between devices with their start and end apart: 5 -> 4, of which waited for: 5 -> 4; matrix products, arithmetic and copies ran while one was open for 9% -> 8% of each run, Pallas kernels for 6% -> 0%
where the time goes in v3:
time: 231 us; the launch traced here: 230 us
  waiting for transfers between devices  143 us (62%)
  local copies, waits for them, and re-layouts  25.6 us (11%)
  starting transfers between devices  20.2 us (9%)
  between operations  14.5 us (6%)
  other arithmetic  11 us (5%)
  Pallas kernels  10.6 us (5%)
  matrix products  5.5 us (2%)
    all_gather x1, waiting for transfers between devices, local(): gathered = lax.all_gather(shard, 'sp', axis=0, tiled=False)  109 us
    unnamed x48, local copies, waits for them, and re-layouts  23.7 us
    all_to_all x1, waiting for transfers between devices, local(): exchanged = lax.all_to_all(copies, 'tp', 0, 0, tiled=True)  19.9 us
    all_to_all x1, starting transfers between devices, local(): totals = lax.all_to_all(total, 'sp', 0, 0, tiled=True)  9.8 us
    all_to_all x1, waiting for transfers between devices, local(): totals = lax.all_to_all(total, 'sp', 0, 0, tiled=True)  8.94 us
    all_to_all x1, starting transfers between devices, local(): exchanged = lax.all_to_all(copies, 'tp', 0, 0, tiled=True)  7.27 us
    dot_general x4, matrix products, spread(): jnp.dot(blocks.astype(BF), pick.astype(BF), preferred_element_type=F32)  5.5 us
  transfers between devices with their start and end apart: 4, of which 4 were waited for; matrix products, arithmetic and copies ran while one was open for 8% of the time, Pallas kernels for 0%

profile of v3, /device:TPU:1, one launch (start us, length us, event | category | flops | bytes accessed | tf_op | source)
XLA Modules:
  0.0 230.2 jit_solution(18370837435736972892)
XLA Ops:
  7.2 1.5 pack.1
  19.5 1.7 fusion.7.mix_imag_ref
  21.2 1.7 fusion.8.mix_real_ref
  22.8 1.1 fusion.5.drive_real_ref
  23.9 1.1 fusion.6.drive_imag_ref
  25.0 1.4 add_bitcast_fusion
  26.9 109.4 %all-gather.3.cloned.1.call-done = bf16[24576,256]{1,0:T(8,128)(2,1)} async-done(((bf16[384,256]{1,0:T(8,128)(2,1)}), bf16[24576,256]{1,0:T(8,128)(2,1)}) %all-gather.3.cloned.1.call-update) | async-done | bytes 12582928 | tf_op jit(solution)/shard_map/all_gather | solution.py:279
  136.3 4.6 %copy-done = bf16[24576,256]{1,0:T(8,128)(2,1)S(1)} copy-done((bf16[24576,256]{1,0:T(8,128)(2,1)S(1)}, bf16[24576,256]{1,0:T(8,128)(2,1)}, u32[]{:S(2)}) %copy-start) | copy-done | bytes 12582936
  140.8 1.1 copy-done.2
  142.0 1.1 copy-done.3
  143.1 1.0 copy-done.13
  145.2 3.8 %first.1 = (bf16[192,256]{1,0:T(8,128)(2,1)S(1)}, bf16[192,256]{1,0:T(8,128)(2,1)S(1)}, f32[192,1024]{1,0:T(8,128)S(1)}, f32[192,1024]{1,0:T(8,128)S(1)}, f32[64,16,128]{2,1,0:T(8,128)S(1)}) custom-call(bf16[192,4096]{1,0:T(8,128)(2,1)S(1)} %fusion.2.normed_ref, bf16[64,384,256]{2,1,0:T(8,128)(2,1)S(1)} %bitcast.57, bf16[256,1024]{1,0:T(8,128)(2,1)S(1)} %copy-done.13, ...), custom_call_target="tpu_custom_call" | custom-call | tf_op jit(solution)/shard_map/first/pallas_call | solution.py:340
  151.5 9.8 %all-to-all-start = ((f32[64,16,128]{2,1,0:T(8,128)}), f32[64,16,128]{2,1,0:T(8,128)S(1)}, u32[]{:S(2)}, u32[]{:S(2)}) async-start(f32[64,16,128]{2,1,0:T(8,128)} %copy-done.15), calls=%async_computation | async-start | bytes 1048576 | tf_op jit(solution)/shard_map/all_to_all | solution.py:372
  161.4 3.1 %collective-permute-start = (bf16[32,256]{1,0:T(8,128)(2,1)S(1)}, bf16[32,256]{1,0:T(8,128)(2,1)S(1)}, u32[]{:S(2)}, u32[]{:S(2)}) collective-permute-start(bf16[32,256]{1,0:T(8,128)(2,1)S(1)} %slice.19), channel_id=1, source_target_pairs={{0,8},{8,16},{16,24},{24,32},{32,40},{40,48},{48,56},{56,64},{64,7... | collective-permute-start | bytes 49160 | tf_op jit(solution)/shard_map/ppermute | solution.py:369
  164.5 4.6 %collective-permute-done.before_ref = bf16[32,256]{1,0:T(8,128)(2,1)S(1)} collective-permute-done((bf16[32,256]{1,0:T(8,128)(2,1)S(1)}, bf16[32,256]{1,0:T(8,128)(2,1)S(1)}, u32[]{:S(2)}, u32[]{:S(2)}) %collective-permute-start) | collective-permute-done | bytes 16416 | tf_op jit(solution)/shard_map/ppermute | solution.py:369
  169.9 8.9 %all-to-all-done.totals_ref = f32[64,16,128]{2,1,0:T(8,128)S(1)} async-done(((f32[64,16,128]{2,1,0:T(8,128)}), f32[64,16,128]{2,1,0:T(8,128)S(1)}, u32[]{:S(2)}, u32[]{:S(2)}) %all-to-all-start) | async-done | bytes 524320 | tf_op jit(solution)/shard_map/all_to_all | solution.py:372
  178.8 1.0 copy-done.4
  180.9 1.1 copy-done.8
  182.0 1.1 copy-done.10
  186.2 1.1 copy-done.6
  187.4 7.3 %all-to-all-start.1 = ((bf16[8,384,256]{2,1,0:T(8,128)(2,1)}), bf16[8,384,256]{2,1,0:T(8,128)(2,1)S(1)}, u32[]{:S(2)}, u32[]{:S(2)}) async-start(bf16[8,384,256]{2,1,0:T(8,128)(2,1)} %copy-done.6), calls=%async_computation.1 | async-start | bytes 3145728 | tf_op jit(solution)/shard_map/all_to_all | solution.py:395
  195.3 19.9 %all-to-all-done.1.rows_ref = bf16[8,384,256]{2,1,0:T(8,128)(2,1)S(1)} async-done(((bf16[8,384,256]{2,1,0:T(8,128)(2,1)}), bf16[8,384,256]{2,1,0:T(8,128)(2,1)S(1)}, u32[]{:S(2)}, u32[]{:S(2)}) %all-to-all-start.1) | async-done | bytes 1572896 | tf_op jit(solution)/shard_map/all_to_all | solution.py:395
  215.2 4.6 %copy-done.1 = bf16[24576,256]{1,0:T(8,128)(2,1)S(1)} copy-done((bf16[24576,256]{1,0:T(8,128)(2,1)S(1)}, bf16[24576,256]{1,0:T(8,128)(2,1)}, u32[]{:S(2)}) %copy-start.1) | copy-done | bytes 12582936
  219.8 3.5 %last.1 = bf16[192,512]{1,0:T(8,128)(2,1)} custom-call(bf16[8,384,256]{2,1,0:T(8,128)(2,1)S(1)} %all-to-all-done.1.rows_ref, bf16[64,384,256]{2,1,0:T(8,128)(2,1)S(1)} %bitcast.58, f32[1,2048]{1,0:T(1,128)S(1)} %bitcast.59, f32[1,2048]{1,0:T(1,128)S(1)} %bitcast.60), custom_call_target="tpu_custom_call" | custom-call | tf_op jit(solution)/shard_map/last/pallas_call | solution.py:397
  (109 shorter events, 20.2 us)
Async XLA Ops:
  7.2 129.1 %all-gather.3.cloned.1.call-start = ((), (), s32[]{:S(2)}) async-start(), calls=%async_computation.2 | async-start | bytes 12779520 | tf_op jit(solution)/shard_map/all_gather | solution.py:279
  13.0 5.3 %copy-start.20 = (bf16[192,4096]{1,0:T(8,128)(2,1)S(1)}, bf16[192,4096]{1,0:T(8,128)(2,1)}, u32[]{:S(2)}) copy-start(bf16[192,4096]{1,0:T(8,128)(2,1)} %param.19) | copy-start | bytes 4718596
  14.0 5.5 %copy-start.21 = (f32[16,64,16]{1,2,0:T(8,128)S(1)}, f32[16,64,16]{1,2,0:T(8,128)}, u32[]{:S(2)}) copy-start(f32[16,64,16]{1,2,0:T(8,128)} %param.30) | copy-start | bytes 196612
  14.0 5.5 %copy-start.22 = (f32[16,64,16]{1,2,0:T(8,128)S(1)}, f32[16,64,16]{1,2,0:T(8,128)}, u32[]{:S(2)}) copy-start(f32[16,64,16]{1,2,0:T(8,128)} %param.31) | copy-start | bytes 196612
  22.8 3.6 %copy-start.23 = (f32[4096]{0:T(1024)S(1)}, f32[4096]{0:T(1024)}, u32[]{:S(2)}) copy-start(f32[4096]{0:T(1024)} %param.20) | copy-start | bytes 49156
  136.3 4.6 %copy-start = (bf16[24576,256]{1,0:T(8,128)(2,1)S(1)}, bf16[24576,256]{1,0:T(8,128)(2,1)}, u32[]{:S(2)}) copy-start(bf16[24576,256]{1,0:T(8,128)(2,1)} %all-gather.3.cloned.1.call-done) | copy-start | bytes 37748740
  140.8 1.1 copy-start.2
  142.0 1.1 copy-start.3
  143.1 1.0 copy-start.13
  144.1 1.0 copy-start.14
  145.2 23.9 %copy-start.16 = (f32[31,256]{1,0:T(8,128)S(1)}, f32[31,256]{1,0:T(8,128)}, u32[]{:S(2)}) copy-start(f32[31,256]{1,0:T(8,128)} %taps_ref.1) | copy-start | bytes 95236
  145.2 33.6 %copy-start.19 = (f32[256]{0:T(256)S(1)}, f32[256]{0:T(256)}, u32[]{:S(2)}) copy-start(f32[256]{0:T(256)} %param.34) | copy-start | bytes 3076
  151.5 27.2 %all-to-all-start = ((f32[64,16,128]{2,1,0:T(8,128)}), f32[64,16,128]{2,1,0:T(8,128)S(1)}, u32[]{:S(2)}, u32[]{:S(2)}) async-start(f32[64,16,128]{2,1,0:T(8,128)} %copy-done.15), calls=%async_computation | async-start | bytes 1048576 | tf_op jit(solution)/shard_map/all_to_all | solution.py:372
  161.4 7.7 %collective-permute-start = (bf16[32,256]{1,0:T(8,128)(2,1)S(1)}, bf16[32,256]{1,0:T(8,128)(2,1)S(1)}, u32[]{:S(2)}, u32[]{:S(2)}) collective-permute-start(bf16[32,256]{1,0:T(8,128)(2,1)S(1)} %slice.19), channel_id=1, source_target_pairs={{0,8},{8,16},{16,24},{24,32},{32,40},{40,48},{48,56},{56,64},{64,7... | collective-permute-start | bytes 49160 | tf_op jit(solution)/shard_map/ppermute | solution.py:369
  178.8 1.0 copy-start.4
  179.8 1.0 copy-start.5
  180.9 1.1 copy-start.8
  182.0 1.1 copy-start.10
  183.1 1.0 copy-start.11
  185.2 30.0 %copy-start.17 = (f32[2048]{0:T(1024)S(1)}, f32[2048]{0:T(1024)}, u32[]{:S(2)}) copy-start(f32[2048]{0:T(1024)} %param.25) | copy-start | bytes 24580
  185.2 30.0 %copy-start.18 = (f32[2048]{0:T(1024)S(1)}, f32[2048]{0:T(1024)}, u32[]{:S(2)}) copy-start(f32[2048]{0:T(1024)} %param.26) | copy-start | bytes 24580
  186.2 1.2 copy-start.6
  187.4 27.9 %all-to-all-start.1 = ((bf16[8,384,256]{2,1,0:T(8,128)(2,1)}), bf16[8,384,256]{2,1,0:T(8,128)(2,1)S(1)}, u32[]{:S(2)}, u32[]{:S(2)}) async-start(bf16[8,384,256]{2,1,0:T(8,128)(2,1)} %copy-done.6), calls=%async_computation.1 | async-start | bytes 3145728 | tf_op jit(solution)/shard_map/all_to_all | solution.py:395
  215.2 4.6 %copy-start.1 = (bf16[24576,256]{1,0:T(8,128)(2,1)S(1)}, bf16[24576,256]{1,0:T(8,128)(2,1)}, u32[]{:S(2)}) copy-start(bf16[24576,256]{1,0:T(8,128)(2,1)} %all-gather.3.cloned.1.call-done) | copy-start | bytes 37748740
  (4 other events, 3.6 us)
Sparse Core Ops, SparseCore 0:
  11.6 124.6 all-gather.2

commit v4 on v3

--- a/solution.py
+++ b/solution.py
@@ -3,12 +3,15 @@
 from jax import lax
 from jax.experimental import pallas as pl
 from jax.experimental.pallas import tpu as pltpu
-from jax.sharding import PartitionSpec as P
+from jax.sharding import Mesh, PartitionSpec as P
 
 BF = jnp.bfloat16
 F32 = jnp.float32
 LANES = 128
 CHUNK = 256
+SP = ("z", "yh", "yl")
+TP = ("x", "c")
+SEQUENCE = ("z", "yh", "c")
 
 
 def rotate(first_real, first_imag, second_real, second_imag):
@@ -41,9 +44,57 @@
             at += ref.shape[0]
 
 
+def norm_kernel(core_ref, tokens_ref, gain_ref, out_ref):
+    floats = tokens_ref[...].astype(F32)
+    model = floats.shape[1]
+    scale = lax.rsqrt(jnp.sum(floats * floats, axis=1, keepdims=True) / model + 1e-06)
+    first_core = core_ref[0] == 0
+    low = lax.broadcasted_iota(jnp.int32, (floats.shape[0], LANES), 1) < LANES // 2
+    for at in range(0, model, 2 * LANES):
+        left = tokens_ref[:, at : at + LANES].astype(F32) * scale * gain_ref[:, at : at + LANES]
+        right = (
+            tokens_ref[:, at + LANES : at + 2 * LANES].astype(F32)
+            * scale
+            * gain_ref[:, at + LANES : at + 2 * LANES]
+        )
+        taken = jnp.where(
+            low,
+            jnp.where(first_core, left, pltpu.roll(left, LANES // 2, 1)),
+            jnp.where(first_core, pltpu.roll(right, LANES // 2, 1), right),
+        )
+        out_ref[:, at // 2 : at // 2 + LANES] = taken.astype(BF)
+
+
+def project_kernel(keep_ref, send_ref, weights_ref, keep_out_ref, send_out_ref, buffer_ref, sems):
+    outer, inner, rows, width = buffer_ref.shape
+    rows //= 3
+    parts = sems.shape[0]
+    per_part = outer // parts
+
+    def fetch(part):
+        at = pl.ds(part * per_part, per_part)
+        return pltpu.make_async_copy(weights_ref.at[at], buffer_ref.at[at], sems.at[part])
+
+    for part in range(parts):
+        fetch(part).start()
+    span = per_part * inner * rows
+    for part in range(parts):
+        fetch(part).wait()
+        for kind in range(3):
+            block = buffer_ref[
+                part * per_part : (part + 1) * per_part, :, kind * rows : (kind + 1) * rows, :
+            ].reshape(span, width)
+            cols = slice(kind * width, (kind + 1) * width)
+            for lhs_ref, out_ref in ((send_ref, send_out_ref), (keep_ref, keep_out_ref)):
+                product = jnp.dot(
+                    lhs_ref[:, part * span : (part + 1) * span], block, preferred_element_type=F32
+                )
+                out_ref[:, cols] = product if part == 0 else out_ref[:, cols] + product
+
+
 def first_kernel(
-    normed_ref,
-    weights_ref,
+    kept_ref,
+    received_ref,
     drive_real_ref,
     drive_imag_ref,
     undo_real_ref,
@@ -53,37 +104,10 @@
     sums_real_ref,
     sums_imag_ref,
     total_ref,
-    buffer_ref,
-    acc_ref,
     last_ref,
-    sems,
 ):
-    devices, rows, width = buffer_ref.shape
-    rows //= 3
-    parts = sems.shape[0]
-    per_part = devices // parts
-
-    def fetch(part):
-        at = pl.ds(part * per_part, per_part)
-        return pltpu.make_async_copy(weights_ref.at[at, pl.ds(0, 3 * rows)], buffer_ref.at[at], sems.at[part])
-
-    for part in range(parts):
-        fetch(part).start()
-    span = per_part * rows
-    for part in range(parts):
-        fetch(part).wait()
-        for kind in range(3):
-            block = buffer_ref[
-                part * per_part : (part + 1) * per_part, kind * rows : (kind + 1) * rows, :
-            ].reshape(span, width)
-            product = jnp.dot(
-                normed_ref[:, part * span : (part + 1) * span], block, preferred_element_type=F32
-            )
-            cols = slice(kind * width, (kind + 1) * width)
-            acc_ref[:, cols] = product if part == 0 else acc_ref[:, cols] + product
-
-    length = acc_ref.shape[0]
-    feed = acc_ref[:, 2 * width :].astype(BF)
+    length, width = gated_ref.shape
+    feed = (kept_ref[:, 2 * width :] + received_ref[:, 2 * width :]).astype(BF)
     feed_ref[...] = feed
     lower = (
         lax.broadcasted_iota(jnp.int32, (length, length), 0)
@@ -103,7 +127,9 @@
                 row = part * half + (at + lane) // LANES
                 last_ref[row : row + 1, :] = sums[length - 1 :, lane : lane + LANES]
     total_ref[...] = jnp.broadcast_to(last_ref[...][None], total_ref.shape)
-    gated_ref[...] = (acc_ref[:, :width] * jax.nn.sigmoid(acc_ref[:, width : 2 * width])).astype(BF)
+    value = kept_ref[:, :width] + received_ref[:, :width]
+    gate = kept_ref[:, width : 2 * width] + received_ref[:, width : 2 * width]
+    gated_ref[...] = (value * jax.nn.sigmoid(gate)).astype(BF)
 
 
 def conv_kernel(before_ref, gated_ref, taps_ref, out_ref, pad_ref):
@@ -169,23 +195,26 @@
         out_ref[copy, length:] = activated
 
 
-def last_kernel(rows_ref, weights_ref, gain_ref, shift_ref, out_ref, buffer_ref, act_ref, acc_ref, sems):
+def last_kernel(
+    core_ref, rows_ref, own_ref, other_ref, gain_ref, shift_ref, out_ref, buffer_ref, act_ref, acc_ref, sems
+):
     blocks, length, width = rows_ref.shape
     length //= 2
-    devices, rows, _ = buffer_ref.shape
+    outer, inner, cores, rows, _ = buffer_ref.shape
     rows //= 6
     parts = sems.shape[0]
-    per_part = devices // parts
+    per_part = outer // parts
     per_block = blocks // parts
-
-    def fetch(part):
+    core = core_ref[0]
+
+    def fetch(part, half):
         at = pl.ds(part * per_part, per_part)
-        return pltpu.make_async_copy(
-            weights_ref.at[at, pl.ds(6 * rows, 6 * rows)], buffer_ref.at[at], sems.at[part]
-        )
+        slot, ref = ((core, own_ref), (1 - core, other_ref))[half]
+        return pltpu.make_async_copy(ref.at[at], buffer_ref.at[at, :, slot], sems.at[part, half])
 
     for part in range(parts):
-        fetch(part).start()
+        fetch(part, 0).start()
+        fetch(part, 1).start()
     channels = blocks * width
     total = jnp.zeros((length, width), F32)
     squares = jnp.zeros((length, width), F32)
@@ -200,16 +229,17 @@
         centred = rows_ref[at, :length, :].astype(F32) - mean
         cols = slice(at * width, (at + 1) * width)
         act_ref[:, cols] = jax.nn.silu(centred * scale * gain_ref[:, cols] + shift_ref[:, cols]).astype(BF)
-    span = per_part * rows
+    span = per_part * inner * cores * rows
     for part in range(parts):
-        fetch(part).wait()
+        fetch(part, 0).wait()
+        fetch(part, 1).wait()
         conv_act = act_ref[:, part * span : (part + 1) * span]
         activated = jnp.concatenate(
             [rows_ref[part * per_block + at, length:, :] for at in range(per_block)], axis=1
         )
         for kind in range(6):
             block = buffer_ref[
-                part * per_part : (part + 1) * per_part, kind * rows : (kind + 1) * rows, :
+                part * per_part : (part + 1) * per_part, :, :, kind * rows : (kind + 1) * rows, :
             ].reshape(span, width)
             product = jnp.dot(conv_act if kind < 2 else activated, block, preferred_element_type=F32)
             cols = slice(kind * width, (kind + 1) * width)
@@ -265,25 +295,83 @@
     state_gate,
     initial_state,
 ):
-    seq_devices = lax.axis_size("sp")
-    tp_devices = lax.axis_size("tp")
-    position = lax.axis_index("sp")
+    seq_devices = lax.axis_size("z") * lax.axis_size("yh") * lax.axis_size("c")
+    tp_devices = lax.axis_size("x") * lax.axis_size("yl")
+    core = lax.axis_index("c")
+    same = lax.axis_index("yl") == core
+    position = (lax.axis_index("z") * lax.axis_size("yh") + lax.axis_index("yh")) * 2 + core
     length, model = tokens.shape
     rows_in, width = conv_value.shape
     rows_out, columns = conv_project.shape
-    shard = pl.pallas_call(
-        pack_kernel,
-        out_shape=jax.ShapeDtypeStruct((3 * rows_in + 3 * rows_out * (columns // width), width), BF),
-        name="pack",
-    )(conv_value, conv_gate, state_feed, conv_project, state_value, state_gate)
-    gathered = lax.all_gather(shard, "sp", axis=0, tiled=False)
-
-    floats = tokens.astype(F32)
-    normed = (
-        floats * lax.rsqrt(jnp.mean(floats * floats, axis=1, keepdims=True) + 1e-06) * norm_gain
-    ).astype(BF)
+    inner = lax.axis_size("yh")
+
+    def swapped(value):
+        return lax.ppermute(value, ("yl", "c"), [(a * 2 + b, b * 2 + a) for a in range(2) for b in range(2)])
+
+    def packed(rows, *arrays):
+        return pl.pallas_call(
+            pack_kernel,
+            out_shape=jax.ShapeDtypeStruct((rows, width), BF),
+            compiler_params=grant(4),
+            name="pack",
+        )(*arrays)
+
+    def spread_y(shard):
+        return lax.all_to_all(
+            jnp.broadcast_to(shard[None], (inner, *shard.shape)), "yh", 0, 0, tiled=True
+        )
+
+    shard_first = swapped(packed(3 * rows_in, conv_value, conv_gate, state_feed))
+    rows_first = spread_y(shard_first)
+    weights_first = lax.all_gather(rows_first, "z", axis=0, tiled=False)
+    shard_last = packed(6 * rows_out, conv_project, state_value, state_gate)
+    shard_last, _ = lax.optimization_barrier((shard_last, rows_first))
+    rows_last = spread_y(swapped(shard_last))
+    weights_last = lax.all_gather(rows_last, "z", axis=0, tiled=False)
+
+    core_scalar = core.astype(jnp.int32).reshape(1)
+    smem = pl.BlockSpec(memory_space=pltpu.SMEM)
+    tokens, decay_rate, skip_gain, conv_taps, _ = lax.optimization_barrier(
+        (tokens, decay_rate, skip_gain, conv_taps, shard_first)
+    )
+    own_half = pl.pallas_call(
+        norm_kernel,
+        in_specs=[smem, whole(tokens.shape), whole((1, model))],
+        out_shape=jax.ShapeDtypeStruct((length, model // 2), BF),
+        name="norm",
+    )(core_scalar, tokens, norm_gain.reshape(1, model))
+    across = [(0, 1), (1, 0)]
+    other_half = lax.ppermute(own_half, "yl", across)
+    keep = jnp.where(same, own_half, other_half)
+    send = jnp.where(same, other_half, own_half)
 
     groups, state_size, group_size = input_real.shape
+    small = groups * group_size
+    parameters = [
+        jnp.concatenate([jnp.swapaxes(p, 1, 2).reshape(small, state_size) for p in (input_real, input_imag)], axis=1),
+        jnp.concatenate([p.reshape(small, state_size) for p in (output_real, output_imag)], axis=1),
+        jnp.concatenate([decay_rate, frequency], axis=1),
+        jnp.concatenate([initial_state[0], initial_state[1]], axis=1),
+        conv_taps[:, :LANES],
+        conv_taps[:, LANES:],
+        skip_gain.reshape(width // LANES, LANES),
+    ]
+    ends_at = []
+    for p in parameters:
+        ends_at.append((ends_at[-1] if ends_at else 0) + p.shape[0])
+    flat_parameters = jnp.concatenate(parameters, axis=0)
+    flat_parameters = jnp.where(same, flat_parameters, lax.ppermute(flat_parameters, "c", across))
+    inputs, outputs, rates, initial, taps_left, taps_right, skip = jnp.split(flat_parameters, ends_at[:-1], axis=0)
+    conv_taps = jnp.concatenate([taps_left, taps_right], axis=1)
+    input_real, input_imag = (
+        part.reshape(groups, group_size, state_size) for part in jnp.split(inputs, 2, axis=1)
+    )
+    output_real, output_imag = (
+        part.reshape(groups, group_size, state_size) for part in jnp.split(outputs, 2, axis=1)
+    )
+    decay_rate, frequency = jnp.split(rates, 2, axis=1)
+    initial_state = jnp.split(initial, 2, axis=1)
+
     flat = groups * state_size
     total_tokens = length * seq_devices
     rate_real = -decay_rate / total_tokens
@@ -294,11 +382,11 @@
     lift_real = step_real - 1.0
     factor_real = (lift_real * rate_real + step_imag * frequency) / modulus
     factor_imag = (step_imag * rate_real - lift_real * frequency) / modulus
-    drive_real = factor_real[..., None] * input_real - factor_imag[..., None] * input_imag
-    drive_imag = factor_real[..., None] * input_imag + factor_imag[..., None] * input_real
-
-    drive_real = spread(jnp.swapaxes(drive_real, 1, 2).reshape(groups * group_size, state_size), group_size)
-    drive_imag = spread(jnp.swapaxes(drive_imag, 1, 2).reshape(groups * group_size, state_size), group_size)
+    drive_real = factor_real[:, None] * input_real - factor_imag[:, None] * input_imag
+    drive_imag = factor_real[:, None] * input_imag + factor_imag[:, None] * input_real
+
+    drive_real = spread(drive_real.reshape(small, state_size), group_size)
+    drive_imag = spread(drive_imag.reshape(small, state_size), group_size)
     mix_real = spread(jnp.swapaxes(output_real, 1, 2).reshape(flat, group_size), state_size)
     mix_imag = spread(jnp.swapaxes(-output_imag, 1, 2).reshape(flat, group_size), state_size)
 
@@ -329,24 +417,24 @@
         )
     )
     (
-        normed, drive_real, drive_imag, mix_real, mix_imag, power_real, power_imag, undo_real, undo_imag, lead, tail, ends
+        keep, drive_real, drive_imag, mix_real, mix_imag, power_real, power_imag, undo_real, undo_imag, lead, tail, ends
     ) = lax.optimization_barrier((
-        normed, drive_real, drive_imag, mix_real, mix_imag, power_real, power_imag, undo_real, undo_imag, lead, tail, ends
+        keep, drive_real, drive_imag, mix_real, mix_imag, power_real, power_imag, undo_real, undo_imag, lead, tail, ends
     ))
     chunks = flat // LANES
 
     parts = 4
-    hbm = pl.BlockSpec(memory_space=pltpu.HBM)
+    hbm = pl.BlockSpec(memory_space=pl.ANY)
+    kept, sent = pl.pallas_call(
+        project_kernel,
+        in_specs=[whole(keep.shape), whole(send.shape), hbm],
+        out_shape=[jax.ShapeDtypeStruct((length, 3 * width), F32)] * 2,
+        scratch_shapes=[pltpu.VMEM(weights_first.shape, BF), pltpu.SemaphoreType.DMA((parts,))],
+        name="project",
+    )(keep, send, weights_first)
+    received = lax.ppermute(sent, "c", across)
     gated, feed, sums_real, sums_imag, total = pl.pallas_call(
         first_kernel,
-        in_specs=[
-            whole(normed.shape),
-            hbm,
-            whole(drive_real.shape),
-            whole(drive_imag.shape),
-            whole(undo_real.shape),
-            whole(undo_imag.shape),
-        ],
         out_shape=[
             jax.ShapeDtypeStruct((length, width), BF),
             jax.ShapeDtypeStruct((length, width), BF),
@@ -354,22 +442,16 @@
             jax.ShapeDtypeStruct((length, flat), F32),
             jax.ShapeDtypeStruct((seq_devices, 2 * chunks, LANES), F32),
         ],
-        scratch_shapes=[
-            pltpu.VMEM((seq_devices, 3 * rows_in, width), BF),
-            pltpu.VMEM((length, 3 * width), F32),
-            pltpu.VMEM((2 * chunks, LANES), F32),
-            pltpu.SemaphoreType.DMA((parts,)),
-        ],
-        compiler_params=grant(24),
+        scratch_shapes=[pltpu.VMEM((2 * chunks, LANES), F32)],
         name="first",
-    )(normed, gathered, drive_real, drive_imag, undo_real, undo_imag)
+    )(kept, received, drive_real, drive_imag, undo_real, undo_imag)
 
     taps = conv_taps.shape[0]
     halo = (taps - 1 + 15) // 16 * 16
     before = lax.ppermute(
-        gated[length - halo :], "sp", [(source, source + 1) for source in range(seq_devices - 1)]
-    )
-    totals = lax.all_to_all(total, "sp", 0, 0, tiled=True)
+        gated[length - halo :], SEQUENCE, [(source, source + 1) for source in range(seq_devices - 1)]
+    )
+    totals = lax.all_to_all(total, SEQUENCE, 0, 0, tiled=True)
     conv_out = pl.pallas_call(
         conv_kernel,
         out_shape=jax.ShapeDtypeStruct((length, width), BF),
@@ -385,57 +467,62 @@
             jax.ShapeDtypeStruct((2 * chunks, LANES), F32),
         ],
         scratch_shapes=[pltpu.VMEM((2 * chunks, LANES), F32)],
-        compiler_params=grant(16),
         name="second",
     )(
         totals, lead, tail, ends, power_real, power_imag, sums_real, sums_imag, mix_real, mix_imag, feed,
-        skip_gain.reshape(1, width), conv_out,
-    )
+        skip.reshape(1, width), conv_out,
+    )
+    final = swapped(final)
     final_state = final.reshape(2, groups, state_size)
-    exchanged = lax.all_to_all(copies, "tp", 0, 0, tiled=True)
-
-    mixer_out = pl.pallas_call(
+    exchanged = lax.all_to_all(copies, ("x", "yl"), 0, 0, tiled=True)
+
+    weights_sent, exchanged = lax.optimization_barrier((weights_last, exchanged))
+    weights_other = lax.ppermute(weights_sent, "c", across)
+    mixed = pl.pallas_call(
         last_kernel,
         in_specs=[
+            smem,
             whole(exchanged.shape),
+            hbm,
             hbm,
             whole((1, chan_gain.shape[0])),
             whole((1, chan_gain.shape[0])),
         ],
         out_shape=jax.ShapeDtypeStruct((length, columns), BF),
         scratch_shapes=[
-            pltpu.VMEM((seq_devices, 6 * rows_out, width), BF),
+            pltpu.VMEM((*weights_last.shape[:2], 2, *weights_last.shape[2:]), BF),
             pltpu.VMEM((length, tp_devices * width), BF),
             pltpu.VMEM((length, 6 * width), F32),
-            pltpu.SemaphoreType.DMA((parts,)),
+            pltpu.SemaphoreType.DMA((parts, 2)),
         ],
-        compiler_params=grant(24),
         name="last",
-    )(exchanged, gathered, chan_gain.reshape(1, -1), chan_shift.reshape(1, -1))
+    )(core_scalar, exchanged, weights_last, weights_other, chan_gain.reshape(1, -1), chan_shift.reshape(1, -1))
+    mixer_out = swapped(mixed)
     return (mixer_out, final_state)
 
 
 def solution(mesh):
+    mesh = Mesh(mesh.devices.reshape(8, 4, 2, 4, 2), ("z", "yh", "yl", "x", "c"))
     in_specs = (
-        P("sp", None),
+        P(SP, None),
         P(),
-        P("sp", "tp"),
-        P("sp", "tp"),
-        P("sp", "tp"),
-        P(None, "tp"),
+        P(SP, TP),
+        P(SP, TP),
+        P(SP, TP),
+        P(None, TP),
         P(),
         P(),
-        P("sp", "tp"),
-        P("tp", None),
-        P("tp", None),
-        P("tp", None, None),
-        P("tp", None, None),
-        P("tp", None, None),
-        P("tp", None, None),
-        P("tp"),
-        P("sp", "tp"),
-        P("sp", "tp"),
-        P(None, "tp", None),
-    )
-    out_specs = (P("sp", "tp"), P(None, "tp", None))
+        P(SP, TP),
+        P(TP, None),
+        P(TP, None),
+        P(TP, None, None),
+        P(TP, None, None),
+        P(TP, None, None),
+        P(TP, None, None),
+        P(TP),
+        P(SP, TP),
+        P(SP, TP),
+        P(None, TP, None),
+    )
+    out_specs = (P(SP, TP), P(None, TP, None))
     return jax.shard_map(local, mesh=mesh, in_specs=in_specs, out_specs=out_specs, check_vma=False)

time: 231 us -> 217 us (0.939)
  waiting for transfers between devices: 143 us -> 84.6 us
  starting transfers between devices: 20.2 us -> 53.4 us
  Pallas kernels: 10.6 us -> 24 us
  local copies, waits for them, and re-layouts: 25.6 us -> 16.4 us
  other arithmetic: 11 us -> 16.6 us
    all_gather x1 -> x2, waiting for transfers between devices: 109 us -> 16.6 us  [the longest x1 12.3 us: local(): weights_first = lax.all_gather(rows_first, 'z', axis=0, tiled=False)]
    ppermute x1 -> x9, starting transfers between devices: 3.1 us -> 31 us  [the longest x4 13.4 us: swapped(): lax.ppermute(value, ('yl', 'c'), [(a * 2 + b, b * 2 + a) for a in range(2...]
    all_to_all x2 -> x4, waiting for transfers between devices: 28.8 us -> 52 us  [the longest x2 27.6 us: spread_y(): lax.all_to_all(jnp.broadcast_to(shard[None], (inner, *shard.shape)), 'yh'...]
    unnamed x48 -> x55, local copies, waits for them, and re-layouts: 23.7 us -> 9.92 us
    ppermute x1 -> x9, waiting for transfers between devices: 4.58 us -> 16 us  [the longest x1 5.61 us: local(): weights_other = lax.ppermute(weights_sent, 'c', across)]
    pallas_call x3 -> x6, Pallas kernels: 8.82 us -> 18.6 us  [the longest x1 5.48 us: local(): pl.pallas_call(last_kernel, in_specs=[smem, whole(exchanged.shape), hbm,...]
    all_to_all x2 -> x4, starting transfers between devices: 17.1 us -> 22.4 us  [the longest x1 9.98 us: local(): totals = lax.all_to_all(total, SEQUENCE, 0, 0, tiled=True)]
    pallas_call x1, Pallas kernels: 0.97 us -> 4.6 us  [local(): pl.pallas_call(second_kernel, out_shape=[jax.ShapeDtypeStruct((tp_devices...]
  transfers between devices with their start and end apart: 4 -> 15, of which waited for: 4 -> 11; matrix products, arithmetic and copies ran while one was open for 8% -> 12% of each run, Pallas kernels for 0% -> 9%
where the time goes in v4:
time: 217 us; the launch traced here: 216 us
  waiting for transfers between devices  84.6 us (39%)
  starting transfers between devices  53.4 us (25%)
  Pallas kernels  24 us (11%)
  other arithmetic  16.6 us (8%)
  local copies, waits for them, and re-layouts  16.4 us (8%)
  between operations  14.6 us (7%)
  matrix products  6.36 us (3%)
    all_to_all x2, waiting for transfers between devices, spread_y(): lax.all_to_all(jnp.broadcast_to(shard[None], (inner, *shard.shape)), 'yh'...  27.6 us
    all_to_all x1, waiting for transfers between devices, local(): exchanged = lax.all_to_all(copies, ('x', 'yl'), 0, 0, tiled=True)  16.3 us
    ppermute x4, starting transfers between devices, swapped(): lax.ppermute(value, ('yl', 'c'), [(a * 2 + b, b * 2 + a) for a in range(2...  13.4 us
    all_gather x1, waiting for transfers between devices, local(): weights_first = lax.all_gather(rows_first, 'z', axis=0, tiled=False)  12.3 us
    all_to_all x1, starting transfers between devices, local(): totals = lax.all_to_all(total, SEQUENCE, 0, 0, tiled=True)  9.98 us
    unnamed x55, local copies, waits for them, and re-layouts  9.92 us
    all_to_all x2, starting transfers between devices, spread_y(): lax.all_to_all(jnp.broadcast_to(shard[None], (inner, *shard.shape)), 'yh'...  8.39 us
    all_to_all x1, waiting for transfers between devices, local(): totals = lax.all_to_all(total, SEQUENCE, 0, 0, tiled=True)  8.01 us
  transfers between devices with their start and end apart: 15, of which 11 were waited for; matrix products, arithmetic and copies ran while one was open for 12% of the time, Pallas kernels for 9%

profile of v4, /device:TPU:1, one launch (start us, length us, event | category | flops | bytes accessed | tf_op | source)
XLA Modules:
  0.0 215.9 jit_solution(17677313937835048117)
XLA Ops:
  9.4 4.6 %collective-permute-start = (bf16[192,256]{1,0:T(8,128)(2,1)S(1)}, bf16[192,256]{1,0:T(8,128)(2,1)S(1)}, u32[]{:S(2)}, u32[]{:S(2)}) collective-permute-start(bf16[192,256]{1,0:T(8,128)(2,1)S(1)} %pack.3), channel_id=1, source_target_pairs={{0,0},{1,8},{8,1},{9,9},{2,2},{3,10},{10,3},{11,11},{4,4},{5,12},{... | collective-permute-start | bytes 294920 | tf_op jit(solution)/shard_map/ppermute | solution.py:309
  21.2 4.8 %collective-permute-start.3 = (f32[608,128]{1,0:T(8,128)S(1)}, f32[608,128]{1,0:T(8,128)S(1)}, u32[]{:S(2)}, u32[]{:S(2)}) collective-permute-start(f32[608,128]{1,0:T(8,128)S(1)} %concatenate.59), channel_id=1, source_target_pairs={{0,1},{1,0},{2,3},{3,2},{4,5},{5,4},{6,7},{7,6},{8,9},{9,8},{10,11... | collective-permute-start | bytes 933896 | tf_op jit(solution)/shard_map/ppermute | solution.py:363
  26.1 3.3 %norm.1 = bf16[192,2048]{1,0:T(8,128)(2,1)} custom-call(s32[1]{0:T(128)} %bitcast.core_ref, bf16[192,4096]{1,0:T(8,128)(2,1)} %tokens_ref, f32[1,4096]{1,0:T(1,128)} %bitcast.154), custom_call_target="tpu_custom_call" | custom-call | tf_op jit(solution)/shard_map/norm/pallas_call | solution.py:337
  32.1 3.9 %all-to-all-start = ((bf16[4,192,256]{2,1,0:T(8,128)(2,1)}), bf16[4,192,256]{2,1,0:T(8,128)(2,1)S(1)}, u32[]{:S(2)}, u32[]{:S(2)}) async-start(bf16[4,192,256]{2,1,0:T(8,128)(2,1)} %broadcast_in_dim.680), calls=%async_computation | async-start | bytes 786432 | tf_op jit(solution)/shard_map/all_to_all | solution.py:320
  37.9 22.3 %all-to-all-done = bf16[4,192,256]{2,1,0:T(8,128)(2,1)S(1)} async-done(((bf16[4,192,256]{2,1,0:T(8,128)(2,1)}), bf16[4,192,256]{2,1,0:T(8,128)(2,1)S(1)}, u32[]{:S(2)}, u32[]{:S(2)}) %all-to-all-start) | async-done | bytes 393248 | tf_op jit(solution)/shard_map/all_to_all | solution.py:320
  69.6 3.2 %collective-permute-start.1 = (bf16[192,256]{1,0:T(8,128)(2,1)S(1)}, bf16[192,256]{1,0:T(8,128)(2,1)S(1)}, u32[]{:S(2)}, u32[]{:S(2)}) collective-permute-start(bf16[192,256]{1,0:T(8,128)(2,1)S(1)} %pack.2), channel_id=1, source_target_pairs={{0,0},{1,8},{8,1},{9,9},{2,2},{3,10},{10,3},{11,11},{4,4},{5,12},{... | collective-permute-start | bytes 294920 | tf_op jit(solution)/shard_map/ppermute | solution.py:309
  76.3 4.5 %all-to-all-start.1 = ((bf16[4,192,256]{2,1,0:T(8,128)(2,1)}), bf16[4,192,256]{2,1,0:T(8,128)(2,1)S(1)}, u32[]{:S(2)}, u32[]{:S(2)}) async-start(bf16[4,192,256]{2,1,0:T(8,128)(2,1)} %broadcast_in_dim.681), calls=%async_computation.1 | async-start | bytes 786432 | tf_op jit(solution)/shard_map/all_to_all | solution.py:320
  84.3 5.3 %all-to-all-done.1 = bf16[4,192,256]{2,1,0:T(8,128)(2,1)S(1)} async-done(((bf16[4,192,256]{2,1,0:T(8,128)(2,1)}), bf16[4,192,256]{2,1,0:T(8,128)(2,1)S(1)}, u32[]{:S(2)}, u32[]{:S(2)}) %all-to-all-start.1) | async-done | bytes 393248 | tf_op jit(solution)/shard_map/all_to_all | solution.py:320
  97.1 12.3 %all-gather.7.cloned.1.call-done = bf16[32,192,256]{2,1,0:T(8,128)(2,1)} async-done(((bf16[4,192,256]{2,1,0:T(8,128)(2,1)}), bf16[32,192,256]{2,1,0:T(8,128)(2,1)}) %all-gather.7.cloned.1.call-update) | async-done | bytes 3145744 | tf_op jit(solution)/shard_map/all_gather | solution.py:326
  109.4 5.2 %project.1 = (f32[192,768]{1,0:T(8,128)}, f32[192,768]{1,0:T(8,128)}) custom-call(bf16[192,2048]{1,0:T(8,128)(2,1)} %get-tuple-element.35.keep_ref, bf16[192,2048]{1,0:T(8,128)(2,1)} %get-tuple-element.101.send_ref, bf16[8,4,192,256]{3,2,1,0:T(8,128)(2,1)} %bitcast.77), custom_call_target="tpu_custom_call" | custom-call | tf_op jit(solution)/shard_map/project/pallas_call | solution.py:428
  114.6 2.8 %collective-permute-start.4 = (f32[192,768]{1,0:T(8,128)}, f32[192,768]{1,0:T(8,128)S(1)}, u32[]{:S(2)}, u32[]{:S(2)}) collective-permute-start(f32[192,768]{1,0:T(8,128)} %get-tuple-element.37), channel_id=1, source_target_pairs={{0,1},{1,0},{2,3},{3,2},{4,5},{5,4},{6,7},{7,6},{8,9},{9,8},{10,11... | collective-permute-start | bytes 1769480 | tf_op jit(solution)/shard_map/ppermute | solution.py:435
  120.0 4.5 %first.1 = (bf16[192,256]{1,0:T(8,128)(2,1)}, bf16[192,256]{1,0:T(8,128)(2,1)}, f32[192,1024]{1,0:T(8,128)}, f32[192,1024]{1,0:T(8,128)}, f32[64,16,128]{2,1,0:T(8,128)}) custom-call(f32[192,768]{1,0:T(8,128)} %get-tuple-element.36.kept_ref, f32[192,768]{1,0:T(8,128)} %copy-done.15, bf16[256,1024]{1,0:T(8,128)(2,1)} %fusion.drive_real_ref, ...), custom_call_target="tpu_custom_call" | custom-call | tf_op jit(solution)/shard_map/first/pallas_call | solution.py:436
  124.6 10.0 %all-to-all-start.2 = ((f32[64,16,128]{2,1,0:T(8,128)}), f32[64,16,128]{2,1,0:T(8,128)S(1)}, u32[]{:S(2)}, u32[]{:S(2)}) async-start(f32[64,16,128]{2,1,0:T(8,128)} %get-tuple-element.42), calls=%async_computation.2 | async-start | bytes 1048576 | tf_op jit(solution)/shard_map/all_to_all | solution.py:454
  135.3 4.6 %collective-permute-start.5 = (bf16[32,256]{1,0:T(8,128)(2,1)S(1)}, bf16[32,256]{1,0:T(8,128)(2,1)S(1)}, u32[]{:S(2)}, u32[]{:S(2)}) collective-permute-start(bf16[32,256]{1,0:T(8,128)(2,1)S(1)} %slice.35), channel_id=1, source_target_pairs={{0,1},{1,16},{16,17},{17,32},{32,33},{33,48},{48,49},{49,64},{64,6... | collective-permute-start | bytes 49160 | tf_op jit(solution)/shard_map/ppermute | solution.py:451
  140.5 4.5 %collective-permute-done.5.before_ref = bf16[32,256]{1,0:T(8,128)(2,1)S(1)} collective-permute-done((bf16[32,256]{1,0:T(8,128)(2,1)S(1)}, bf16[32,256]{1,0:T(8,128)(2,1)S(1)}, u32[]{:S(2)}, u32[]{:S(2)}) %collective-permute-start.5) | collective-permute-done | bytes 16416 | tf_op jit(solution)/shard_map/ppermute | solution.py:451
  147.3 8.0 %all-to-all-done.2.totals_ref = f32[64,16,128]{2,1,0:T(8,128)S(1)} async-done(((f32[64,16,128]{2,1,0:T(8,128)}), f32[64,16,128]{2,1,0:T(8,128)S(1)}, u32[]{:S(2)}, u32[]{:S(2)}) %all-to-all-start.2) | async-done | bytes 524320 | tf_op jit(solution)/shard_map/all_to_all | solution.py:454
  156.1 4.6 %second.1 = (bf16[8,384,256]{2,1,0:T(8,128)(2,1)}, f32[16,128]{1,0:T(8,128)}) custom-call(f32[64,16,128]{2,1,0:T(8,128)} %copy-done.12, f32[64,16,128]{2,1,0:T(8,128)} %pad_maximum_fusion.lead_ref, f32[64,16,128]{2,1,0:T(8,128)} %pad_maximum_fusion.1.tail_ref, f32[2,16,128]{2,1,0:T(8,128)} %pad_maximum_fusion.5.ends_ref, f32[192,1024]{1,0:T(8,128)} %copy-done.10, ...), custom_call_target="tpu_custom_call" | custom-call | tf_op jit(solution)/shard_map/second/pallas_call | solution.py:463
  160.7 4.0 %all-to-all-start.3 = ((bf16[8,384,256]{2,1,0:T(8,128)(2,1)}), bf16[8,384,256]{2,1,0:T(8,128)(2,1)S(1)}, u32[]{:S(2)}, u32[]{:S(2)}) async-start(bf16[8,384,256]{2,1,0:T(8,128)(2,1)} %get-tuple-element.54), calls=%async_computation.3 | async-start | bytes 3145728 | tf_op jit(solution)/shard_map/all_to_all | solution.py:477
  164.7 4.3 %all-gather.5.cloned.1.call-done = bf16[32,192,256]{2,1,0:T(8,128)(2,1)} async-done(((bf16[4,192,256]{2,1,0:T(8,128)(2,1)}), bf16[32,192,256]{2,1,0:T(8,128)(2,1)}) %all-gather.5.cloned.1.call-update) | async-done | bytes 3145744 | tf_op jit(solution)/shard_map/all_gather | solution.py:330
  169.0 16.3 %all-to-all-done.3.rows_ref = bf16[8,384,256]{2,1,0:T(8,128)(2,1)S(1)} async-done(((bf16[8,384,256]{2,1,0:T(8,128)(2,1)}), bf16[8,384,256]{2,1,0:T(8,128)(2,1)S(1)}, u32[]{:S(2)}, u32[]{:S(2)}) %all-to-all-start.3) | async-done | bytes 1572896 | tf_op jit(solution)/shard_map/all_to_all | solution.py:477
  185.3 3.6 %collective-permute-start.6 = (bf16[8,4,192,256]{3,2,1,0:T(8,128)(2,1)}, bf16[8,4,192,256]{3,2,1,0:T(8,128)(2,1)}, u32[]{:S(2)}, u32[]{:S(2)}) collective-permute-start(bf16[8,4,192,256]{3,2,1,0:T(8,128)(2,1)} %bitcast.78), channel_id=1, source_target_pairs={{0,1},{1,0},{2,3},{3,2},{4,5},{5,4},{6,7},{7,6},{8,9},{9,8},{10,11... | collective-permute-start | bytes 9437192 | tf_op jit(solution)/shard_map/ppermute | solution.py:480
  188.9 5.6 %collective-permute-done.6.other_ref = bf16[8,4,192,256]{3,2,1,0:T(8,128)(2,1)} collective-permute-done((bf16[8,4,192,256]{3,2,1,0:T(8,128)(2,1)}, bf16[8,4,192,256]{3,2,1,0:T(8,128)(2,1)}, u32[]{:S(2)}, u32[]{:S(2)}) %collective-permute-start.6) | collective-permute-done | bytes 3145760 | tf_op jit(solution)/shard_map/ppermute | solution.py:480
  194.5 5.5 %last.1 = bf16[192,512]{1,0:T(8,128)(2,1)} custom-call(s32[1]{0:T(128)} %bitcast.core_ref, bf16[8,384,256]{2,1,0:T(8,128)(2,1)} %copy-done.8, bf16[8,4,192,256]{3,2,1,0:T(8,128)(2,1)} %bitcast.79, bf16[8,4,192,256]{3,2,1,0:T(8,128)(2,1)} %collective-permute-done.6.other_ref, f32[1,2048]{1,0:T(1,128)} %bitcast.155, f32[1,2048]{1,0:T(1,128)} %bitcast.156), custom_call_target="tpu_custom_call" | custom-call | tf_op jit(solution)/shard_map/last/pallas_call | solution.py:481
  202.7 2.9 %collective-permute-start.8 = (f32[16,128]{1,0:T(8,128)S(1)}, f32[16,128]{1,0:T(8,128)S(1)}, u32[]{:S(2)}, u32[]{:S(2)}) collective-permute-start(f32[16,128]{1,0:T(8,128)S(1)} %copy-done.25), channel_id=1, source_target_pairs={{0,0},{1,8},{8,1},{9,9},{2,2},{3,10},{10,3},{11,11},{4,4},{5,12},{... | collective-permute-start | bytes 24584 | tf_op jit(solution)/shard_map/ppermute | solution.py:309
  (152 shorter events, 50.7 us)
Async XLA Ops:
  9.4 9.4 %collective-permute-start = (bf16[192,256]{1,0:T(8,128)(2,1)S(1)}, bf16[192,256]{1,0:T(8,128)(2,1)S(1)}, u32[]{:S(2)}, u32[]{:S(2)}) collective-permute-start(bf16[192,256]{1,0:T(8,128)(2,1)S(1)} %pack.3), channel_id=1, source_target_pairs={{0,0},{1,8},{8,1},{9,9},{2,2},{3,10},{10,3},{11,11},{4,4},{5,12},{... | collective-permute-start | bytes 294920 | tf_op jit(solution)/shard_map/ppermute | solution.py:309
  14.2 67.2 %copy-start.17 = (s32[1024]{0:T(1024)}, s32[1024]{0:T(1024)S(1)}, u32[]{:S(2)}) copy-start(s32[1024]{0:T(1024)S(1)} %get-tuple-element.160) | copy-start | bytes 12292
  14.3 67.2 %copy-start.18 = (s32[1024]{0:T(1024)}, s32[1024]{0:T(1024)S(1)}, u32[]{:S(2)}) copy-start(s32[1024]{0:T(1024)S(1)} %get-tuple-element.161) | copy-start | bytes 12292
  14.3 67.2 %copy-start.19 = (s32[1024]{0:T(1024)}, s32[1024]{0:T(1024)S(1)}, u32[]{:S(2)}) copy-start(s32[1024]{0:T(1024)S(1)} %get-tuple-element.162) | copy-start | bytes 12292
  14.3 67.2 %copy-start.20 = (s32[1024]{0:T(1024)}, s32[1024]{0:T(1024)S(1)}, u32[]{:S(2)}) copy-start(s32[1024]{0:T(1024)S(1)} %get-tuple-element.163) | copy-start | bytes 12292
  14.3 67.1 %copy-start.21 = (pred[1024]{0:T(1024)(128)(4,1)}, pred[1024]{0:T(1024)(128)(4,1)S(1)}, u32[]{:S(2)}) copy-start(pred[1024]{0:T(1024)(128)(4,1)S(1)} %get-tuple-element.164) | copy-start | bytes 3076
  14.3 67.1 %copy-start.22 = (pred[1024]{0:T(1024)(128)(4,1)}, pred[1024]{0:T(1024)(128)(4,1)S(1)}, u32[]{:S(2)}) copy-start(pred[1024]{0:T(1024)(128)(4,1)S(1)} %get-tuple-element.165) | copy-start | bytes 3076
  14.3 67.1 %copy-start.23 = (s32[256]{0:T(256)}, s32[256]{0:T(256)S(1)}, u32[]{:S(2)}) copy-start(s32[256]{0:T(256)S(1)} %get-tuple-element.166) | copy-start | bytes 3076
  14.4 67.1 %copy-start.24 = (s32[256]{0:T(256)}, s32[256]{0:T(256)S(1)}, u32[]{:S(2)}) copy-start(s32[256]{0:T(256)S(1)} %get-tuple-element.167) | copy-start | bytes 3076
  14.4 67.1 %copy-start.26 = (pred[256]{0:T(512)(128)(4,1)}, pred[256]{0:T(512)(128)(4,1)S(1)}, u32[]{:S(2)}) copy-start(pred[256]{0:T(512)(128)(4,1)S(1)} %get-tuple-element.171) | copy-start | bytes 772
  21.2 14.8 %collective-permute-start.3 = (f32[608,128]{1,0:T(8,128)S(1)}, f32[608,128]{1,0:T(8,128)S(1)}, u32[]{:S(2)}, u32[]{:S(2)}) collective-permute-start(f32[608,128]{1,0:T(8,128)S(1)} %concatenate.59), channel_id=1, source_target_pairs={{0,1},{1,0},{2,3},{3,2},{4,5},{5,4},{6,7},{7,6},{8,9},{9,8},{10,11... | collective-permute-start | bytes 933896 | tf_op jit(solution)/shard_map/ppermute | solution.py:363
  29.4 66.4 %collective-permute-start.2 = (bf16[192,2048]{1,0:T(8,128)(2,1)}, bf16[192,2048]{1,0:T(8,128)(2,1)S(1)}, u32[]{:S(2)}, u32[]{:S(2)}) collective-permute-start(bf16[192,2048]{1,0:T(8,128)(2,1)} %norm.1), channel_id=1, source_target_pairs={{0,8},{8,0},{1,9},{9,1},{2,10},{10,2},{3,11},{11,3},{4,12},{12,4},... | collective-permute-start | bytes 2359304 | tf_op jit(solution)/shard_map/ppermute | solution.py:344
  32.1 28.1 %all-to-all-start = ((bf16[4,192,256]{2,1,0:T(8,128)(2,1)}), bf16[4,192,256]{2,1,0:T(8,128)(2,1)S(1)}, u32[]{:S(2)}, u32[]{:S(2)}) async-start(bf16[4,192,256]{2,1,0:T(8,128)(2,1)} %broadcast_in_dim.680), calls=%async_computation | async-start | bytes 786432 | tf_op jit(solution)/shard_map/all_to_all | solution.py:320
  36.0 73.4 %all-gather.7.cloned.1.call-start = ((), (), s32[]{:S(2)}) async-start(), calls=%async_computation.5 | async-start | bytes 3538944 | tf_op jit(solution)/shard_map/all_gather | solution.py:326
  69.6 5.9 %collective-permute-start.1 = (bf16[192,256]{1,0:T(8,128)(2,1)S(1)}, bf16[192,256]{1,0:T(8,128)(2,1)S(1)}, u32[]{:S(2)}, u32[]{:S(2)}) collective-permute-start(bf16[192,256]{1,0:T(8,128)(2,1)S(1)} %pack.2), channel_id=1, source_target_pairs={{0,0},{1,8},{8,1},{9,9},{2,2},{3,10},{10,3},{11,11},{4,4},{5,12},{... | collective-permute-start | bytes 294920 | tf_op jit(solution)/shard_map/ppermute | solution.py:309
  76.3 13.3 %all-to-all-start.1 = ((bf16[4,192,256]{2,1,0:T(8,128)(2,1)}), bf16[4,192,256]{2,1,0:T(8,128)(2,1)S(1)}, u32[]{:S(2)}, u32[]{:S(2)}) async-start(bf16[4,192,256]{2,1,0:T(8,128)(2,1)} %broadcast_in_dim.681), calls=%async_computation.1 | async-start | bytes 786432 | tf_op jit(solution)/shard_map/all_to_all | solution.py:320
  80.8 88.2 %all-gather.5.cloned.1.call-start = ((), (), s32[]{:S(2)}) async-start(), calls=%async_computation.4 | async-start | bytes 3538944 | tf_op jit(solution)/shard_map/all_gather | solution.py:330
  114.6 4.6 %collective-permute-start.4 = (f32[192,768]{1,0:T(8,128)}, f32[192,768]{1,0:T(8,128)S(1)}, u32[]{:S(2)}, u32[]{:S(2)}) collective-permute-start(f32[192,768]{1,0:T(8,128)} %get-tuple-element.37), channel_id=1, source_target_pairs={{0,1},{1,0},{2,3},{3,2},{4,5},{5,4},{6,7},{7,6},{8,9},{9,8},{10,11... | collective-permute-start | bytes 1769480 | tf_op jit(solution)/shard_map/ppermute | solution.py:435
  124.6 30.8 %all-to-all-start.2 = ((f32[64,16,128]{2,1,0:T(8,128)}), f32[64,16,128]{2,1,0:T(8,128)S(1)}, u32[]{:S(2)}, u32[]{:S(2)}) async-start(f32[64,16,128]{2,1,0:T(8,128)} %get-tuple-element.42), calls=%async_computation.2 | async-start | bytes 1048576 | tf_op jit(solution)/shard_map/all_to_all | solution.py:454
  135.3 9.7 %collective-permute-start.5 = (bf16[32,256]{1,0:T(8,128)(2,1)S(1)}, bf16[32,256]{1,0:T(8,128)(2,1)S(1)}, u32[]{:S(2)}, u32[]{:S(2)}) collective-permute-start(bf16[32,256]{1,0:T(8,128)(2,1)S(1)} %slice.35), channel_id=1, source_target_pairs={{0,1},{1,16},{16,17},{17,32},{32,33},{33,48},{48,49},{49,64},{64,6... | collective-permute-start | bytes 49160 | tf_op jit(solution)/shard_map/ppermute | solution.py:451
  160.7 24.6 %all-to-all-start.3 = ((bf16[8,384,256]{2,1,0:T(8,128)(2,1)}), bf16[8,384,256]{2,1,0:T(8,128)(2,1)S(1)}, u32[]{:S(2)}, u32[]{:S(2)}) async-start(bf16[8,384,256]{2,1,0:T(8,128)(2,1)} %get-tuple-element.54), calls=%async_computation.3 | async-start | bytes 3145728 | tf_op jit(solution)/shard_map/all_to_all | solution.py:477
  185.3 9.2 %collective-permute-start.6 = (bf16[8,4,192,256]{3,2,1,0:T(8,128)(2,1)}, bf16[8,4,192,256]{3,2,1,0:T(8,128)(2,1)}, u32[]{:S(2)}, u32[]{:S(2)}) collective-permute-start(bf16[8,4,192,256]{3,2,1,0:T(8,128)(2,1)} %bitcast.78), channel_id=1, source_target_pairs={{0,1},{1,0},{2,3},{3,2},{4,5},{5,4},{6,7},{7,6},{8,9},{9,8},{10,11... | collective-permute-start | bytes 9437192 | tf_op jit(solution)/shard_map/ppermute | solution.py:480
  200.0 8.4 %collective-permute-start.7 = (bf16[192,512]{1,0:T(8,128)(2,1)}, bf16[192,512]{1,0:T(8,128)(2,1)S(1)}, u32[]{:S(2)}, u32[]{:S(2)}) collective-permute-start(bf16[192,512]{1,0:T(8,128)(2,1)} %last.1), channel_id=1, source_target_pairs={{0,0},{1,8},{8,1},{9,9},{2,2},{3,10},{10,3},{11,11},{4,4},{5,12},{... | collective-permute-start | bytes 589832 | tf_op jit(solution)/shard_map/ppermute | solution.py:309
  202.7 5.0 %collective-permute-start.8 = (f32[16,128]{1,0:T(8,128)S(1)}, f32[16,128]{1,0:T(8,128)S(1)}, u32[]{:S(2)}, u32[]{:S(2)}) collective-permute-start(f32[16,128]{1,0:T(8,128)S(1)} %copy-done.25), channel_id=1, source_target_pairs={{0,0},{1,8},{8,1},{9,9},{2,2},{3,10},{10,3},{11,11},{4,4},{5,12},{... | collective-permute-start | bytes 24584 | tf_op jit(solution)/shard_map/ppermute | solution.py:309
  (18 other events, 68.1 us)
Sparse Core Ops, SparseCore 0:
  61.1 48.2 all-gather.6
  111.5 57.4 all-gather.4

commit v5 on v4

--- a/solution.py
+++ b/solution.py
@@ -78,18 +78,19 @@
     for part in range(parts):
         fetch(part).start()
     span = per_part * inner * rows
+    length = keep_ref.shape[0]
     for part in range(parts):
         fetch(part).wait()
+        lhs = jnp.concatenate([ref[:, part * span : (part + 1) * span] for ref in (send_ref, keep_ref)], axis=0)
         for kind in range(3):
             block = buffer_ref[
                 part * per_part : (part + 1) * per_part, :, kind * rows : (kind + 1) * rows, :
             ].reshape(span, width)
             cols = slice(kind * width, (kind + 1) * width)
-            for lhs_ref, out_ref in ((send_ref, send_out_ref), (keep_ref, keep_out_ref)):
-                product = jnp.dot(
-                    lhs_ref[:, part * span : (part + 1) * span], block, preferred_element_type=F32
-                )
-                out_ref[:, cols] = product if part == 0 else out_ref[:, cols] + product
+            product = jnp.dot(lhs, block, preferred_element_type=F32)
+            for at, out_ref in ((0, send_out_ref), (length, keep_out_ref)):
+                rows_of_it = product[at : at + length]
+                out_ref[:, cols] = rows_of_it if part == 0 else out_ref[:, cols] + rows_of_it
 
 
 def first_kernel(
@@ -147,10 +148,28 @@
         out_ref[:, cols] = acc.astype(BF)
 
 
+def weighted(weights_ref, values_ref):
+    half = values_ref.shape[1] // 2
+    real, imag = rotate(
+        weights_ref[:, :half, :], weights_ref[:, half:, :], values_ref[:, :half, :], values_ref[:, half:, :]
+    )
+    return jnp.sum(real, axis=0), jnp.sum(imag, axis=0)
+
+
+def row_kernel(totals_ref, tail_ref, out_ref):
+    half = totals_ref.shape[1] // 2
+    real, imag = weighted(tail_ref, totals_ref)
+    for copy in range(out_ref.shape[0]):
+        out_ref[copy, :half] = real
+        out_ref[copy, half:] = imag
+
+
 def second_kernel(
     totals_ref,
     lead_ref,
-    tail_ref,
+    ends_of_rows_ref,
+    lead_rows_ref,
+    tail_rows_ref,
     ends_ref,
     power_real_ref,
     power_imag_ref,
@@ -166,13 +185,13 @@
     entry_ref,
 ):
     half = final_ref.shape[0] // 2
-    total_real, total_imag = (totals_ref[:, :half, :], totals_ref[:, half:, :])
-    lead_real, lead_imag = rotate(lead_ref[:, :half, :], lead_ref[:, half:, :], total_real, total_imag)
-    entry_ref[:half] = ends_ref[0, :half] + jnp.sum(lead_real, axis=0)
-    entry_ref[half:] = ends_ref[0, half:] + jnp.sum(lead_imag, axis=0)
-    tail_real, tail_imag = rotate(tail_ref[:, :half, :], tail_ref[:, half:, :], total_real, total_imag)
-    final_ref[:half] = ends_ref[1, :half] + jnp.sum(tail_real, axis=0)
-    final_ref[half:] = ends_ref[1, half:] + jnp.sum(tail_imag, axis=0)
+    lead = weighted(lead_ref, totals_ref)
+    lead_rows = weighted(lead_rows_ref, ends_of_rows_ref)
+    tail_rows = weighted(tail_rows_ref, ends_of_rows_ref)
+    for part in range(2):
+        rows = slice(part * half, (part + 1) * half)
+        entry_ref[rows] = ends_ref[0, rows] + lead[part] + lead_rows[part]
+        final_ref[rows] = ends_ref[1, rows] + tail_rows[part]
     response = skip_ref[...] * feed_ref[...].astype(F32)
     for at in range(0, sums_real_ref.shape[1], CHUNK):
         cols = slice(at, at + CHUNK)
@@ -312,28 +331,26 @@
         return pl.pallas_call(
             pack_kernel,
             out_shape=jax.ShapeDtypeStruct((rows, width), BF),
-            compiler_params=grant(4),
             name="pack",
         )(*arrays)
 
-    def spread_y(shard):
-        return lax.all_to_all(
-            jnp.broadcast_to(shard[None], (inner, *shard.shape)), "yh", 0, 0, tiled=True
+    def copies_of(shard):
+        return jnp.broadcast_to(shard[None], (inner, *shard.shape))
+
+    shard_first = swapped(packed(3 * rows_in, conv_value, conv_gate, state_feed))
+    wide_first = copies_of(shard_first)
+    wide_first, decay_rate, skip_gain, conv_taps, input_real, input_imag, output_real, output_imag = (
+        lax.optimization_barrier(
+            (wide_first, decay_rate, skip_gain, conv_taps, input_real, input_imag, output_real, output_imag)
         )
-
-    shard_first = swapped(packed(3 * rows_in, conv_value, conv_gate, state_feed))
-    rows_first = spread_y(shard_first)
+    )
+    rows_first = lax.all_to_all(wide_first, "yh", 0, 0, tiled=True)
     weights_first = lax.all_gather(rows_first, "z", axis=0, tiled=False)
     shard_last = packed(6 * rows_out, conv_project, state_value, state_gate)
-    shard_last, _ = lax.optimization_barrier((shard_last, rows_first))
-    rows_last = spread_y(swapped(shard_last))
-    weights_last = lax.all_gather(rows_last, "z", axis=0, tiled=False)
+    tokens, _ = lax.optimization_barrier((tokens, rows_first))
 
     core_scalar = core.astype(jnp.int32).reshape(1)
     smem = pl.BlockSpec(memory_space=pltpu.SMEM)
-    tokens, decay_rate, skip_gain, conv_taps, _ = lax.optimization_barrier(
-        (tokens, decay_rate, skip_gain, conv_taps, shard_first)
-    )
     own_half = pl.pallas_call(
         norm_kernel,
         in_specs=[smem, whole(tokens.shape), whole((1, model))],
@@ -342,6 +359,9 @@
     )(core_scalar, tokens, norm_gain.reshape(1, model))
     across = [(0, 1), (1, 0)]
     other_half = lax.ppermute(own_half, "yl", across)
+    shard_last, _ = lax.optimization_barrier((shard_last, own_half))
+    rows_last = lax.all_to_all(copies_of(swapped(shard_last)), "yh", 0, 0, tiled=True)
+    weights_last = lax.all_gather(rows_last, "z", axis=0, tiled=False)
     keep = jnp.where(same, own_half, other_half)
     send = jnp.where(same, other_half, own_half)
 
@@ -361,6 +381,7 @@
         ends_at.append((ends_at[-1] if ends_at else 0) + p.shape[0])
     flat_parameters = jnp.concatenate(parameters, axis=0)
     flat_parameters = jnp.where(same, flat_parameters, lax.ppermute(flat_parameters, "c", across))
+    flat_parameters, _ = lax.optimization_barrier((flat_parameters, own_half))
     inputs, outputs, rates, initial, taps_left, taps_right, skip = jnp.split(flat_parameters, ends_at[:-1], axis=0)
     conv_taps = jnp.concatenate([taps_left, taps_right], axis=1)
     input_real, input_imag = (
@@ -403,12 +424,23 @@
     power_real, power_imag = powers(base_real, base_imag)
     undo_real, undo_imag = powers(base_real / square_size, -base_imag / square_size)
     span_real, span_imag = (power_real[-1], power_imag[-1])
-    device_ids = lax.iota(jnp.int32, seq_devices)
-    lag = position - device_ids
-    lead_real, lead_imag = power_table(span_real, span_imag, jnp.maximum(lag, 0), seq_devices)
-    earlier = (lag > 0).astype(F32)[:, None]
-    lead = rows_of(lead_real * earlier, lead_imag * earlier)
-    tail = rows_of(*power_table(span_real, span_imag, seq_devices - device_ids, seq_devices))
+    row_devices = inner * 2
+    outer = seq_devices // row_devices
+    in_row = position % row_devices
+    row = position // row_devices
+    lag = in_row - lax.iota(jnp.int32, row_devices)
+    lag_rows = row - lax.iota(jnp.int32, outer)
+
+    def spans(exponent, chosen=None):
+        real, imag = power_table(span_real, span_imag, jnp.maximum(exponent, 0), seq_devices)
+        if chosen is not None:
+            real, imag = (part * chosen.astype(F32)[:, None] for part in (real, imag))
+        return rows_of(real, imag)
+
+    lead = spans(lag, lag > 0)
+    tail = spans(row_devices - lax.iota(jnp.int32, row_devices))
+    lead_rows = spans((lag_rows - 1) * row_devices + in_row, lag_rows > 0)
+    tail_rows = spans((outer - 1 - lax.iota(jnp.int32, outer)) * row_devices)
     ends = rows_of(
         *rotate(
             *power_table(span_real, span_imag, jnp.stack([position, jnp.int32(seq_devices)]), seq_devices),
@@ -417,9 +449,11 @@
         )
     )
     (
-        keep, drive_real, drive_imag, mix_real, mix_imag, power_real, power_imag, undo_real, undo_imag, lead, tail, ends
+        keep, drive_real, drive_imag, mix_real, mix_imag, power_real, power_imag, undo_real, undo_imag, lead, tail, lead_rows,
+        tail_rows, ends
     ) = lax.optimization_barrier((
-        keep, drive_real, drive_imag, mix_real, mix_imag, power_real, power_imag, undo_real, undo_imag, lead, tail, ends
+        keep, drive_real, drive_imag, mix_real, mix_imag, power_real, power_imag, undo_real, undo_imag, lead, tail, lead_rows,
+        tail_rows, ends
     ))
     chunks = flat // LANES
 
@@ -440,7 +474,7 @@
             jax.ShapeDtypeStruct((length, width), BF),
             jax.ShapeDtypeStruct((length, flat), F32),
             jax.ShapeDtypeStruct((length, flat), F32),
-            jax.ShapeDtypeStruct((seq_devices, 2 * chunks, LANES), F32),
+            jax.ShapeDtypeStruct((row_devices, 2 * chunks, LANES), F32),
         ],
         scratch_shapes=[pltpu.VMEM((2 * chunks, LANES), F32)],
         name="first",
@@ -451,7 +485,13 @@
     before = lax.ppermute(
         gated[length - halo :], SEQUENCE, [(source, source + 1) for source in range(seq_devices - 1)]
     )
-    totals = lax.all_to_all(total, SEQUENCE, 0, 0, tiled=True)
+    totals = lax.all_to_all(total, SEQUENCE[1:], 0, 0, tiled=True)
+    end_of_row = pl.pallas_call(
+        row_kernel,
+        out_shape=jax.ShapeDtypeStruct((outer, 2 * chunks, LANES), F32),
+        name="row",
+    )(totals, tail)
+    ends_of_rows = lax.all_to_all(end_of_row, SEQUENCE[0], 0, 0, tiled=True)
     conv_out = pl.pallas_call(
         conv_kernel,
         out_shape=jax.ShapeDtypeStruct((length, width), BF),
@@ -469,7 +509,8 @@
         scratch_shapes=[pltpu.VMEM((2 * chunks, LANES), F32)],
         name="second",
     )(
-        totals, lead, tail, ends, power_real, power_imag, sums_real, sums_imag, mix_real, mix_imag, feed,
+        totals, lead, ends_of_rows, lead_rows, tail_rows, ends, power_real, power_imag, sums_real, sums_imag,
+        mix_real, mix_imag, feed,
         skip.reshape(1, width), conv_out,
     )
     final = swapped(final)

time: 217 us -> 205 us (0.945)
  waiting for transfers between devices: 84.6 us -> 57.1 us
  blocking collectives: 0 us -> 14.6 us
  Pallas kernels: 24 us -> 28.4 us
  local copies, waits for them, and re-layouts: 16.4 us -> 12.2 us
  starting transfers between devices: 53.4 us -> 50.6 us
    all_to_all x3, waiting for transfers between devices: 35.6 us -> 6.56 us  [the longest x1 3.66 us: local(): rows_first = lax.all_to_all(wide_first, 'yh', 0, 0, tiled=True)]
    all_to_all x0 -> x1, blocking collectives: none -> 14.6 us  [local(): totals = lax.all_to_all(total, SEQUENCE[1:], 0, 0, tiled=True)]
    ppermute x4, waiting for transfers between devices: 4.12 us -> 16.1 us  [swapped(): lax.ppermute(value, ('yl', 'c'), [(a * 2 + b, b * 2 + a) for a in range(2...]
    unnamed x55 -> x85, local copies, waits for them, and re-layouts: 9.92 us -> 4.55 us
    all_gather x1, waiting for transfers between devices: 12.3 us -> 6.94 us  [local(): weights_first = lax.all_gather(rows_first, 'z', axis=0, tiled=False)]
    all_to_all x3, starting transfers between devices: 18.4 us -> 13.7 us  [the longest x1 6.05 us: local(): rows_first = lax.all_to_all(wide_first, 'yh', 0, 0, tiled=True)]
    ppermute x1, waiting for transfers between devices: 4.48 us -> 0.07 us  [local(): lax.ppermute(gated[length - halo:], SEQUENCE, [(source, source + 1) for s...]
    all_gather x1, waiting for transfers between devices: 4.3 us -> 0.01 us  [local(): weights_last = lax.all_gather(rows_last, 'z', axis=0, tiled=False)]
  transfers between devices with their start and end apart: 15 -> 15, of which waited for: 11 -> 11; matrix products, arithmetic and copies ran while one was open for 12% -> 15% of each run, Pallas kernels for 9% -> 9%
where the time goes in v5:
time: 205 us; the launch traced here: 204 us
  waiting for transfers between devices  57.1 us (28%)
  starting transfers between devices  50.6 us (25%)
  Pallas kernels  28.4 us (14%)
  other arithmetic  18.3 us (9%)
  between operations  14.9 us (7%)
  blocking collectives  14.6 us (7%)
  local copies, waits for them, and re-layouts  12.2 us (6%)
  matrix products  7.35 us (4%)
    all_to_all x1, waiting for transfers between devices, local(): exchanged = lax.all_to_all(copies, ('x', 'yl'), 0, 0, tiled=True)  18.7 us
    ppermute x4, waiting for transfers between devices, swapped(): lax.ppermute(value, ('yl', 'c'), [(a * 2 + b, b * 2 + a) for a in range(2...  16.1 us
    ppermute x4, starting transfers between devices, swapped(): lax.ppermute(value, ('yl', 'c'), [(a * 2 + b, b * 2 + a) for a in range(2...  15.9 us
    all_to_all x1, blocking collectives, local(): totals = lax.all_to_all(total, SEQUENCE[1:], 0, 0, tiled=True)  14.6 us
    dot_general x4, matrix products, spread(): jnp.dot(blocks.astype(BF), pick.astype(BF), preferred_element_type=F32)  7.35 us
    all_gather x1, waiting for transfers between devices, local(): weights_first = lax.all_gather(rows_first, 'z', axis=0, tiled=False)  6.94 us
    all_to_all x1, starting transfers between devices, local(): rows_first = lax.all_to_all(wide_first, 'yh', 0, 0, tiled=True)  6.05 us
    pallas_call x1, Pallas kernels, local(): pl.pallas_call(project_kernel, in_specs=[whole(keep.shape), whole(send.sh...  5.77 us
  transfers between devices with their start and end apart: 15, of which 11 were waited for; matrix products, arithmetic and copies ran while one was open for 15% of the time, Pallas kernels for 9%

profile of v5, /device:TPU:1, one launch (start us, length us, event | category | flops | bytes accessed | tf_op | source)
XLA Modules:
  0.0 203.5 jit_solution(13989244779657353674)
XLA Ops:
  8.6 4.6 %collective-permute-start = (bf16[192,256]{1,0:T(8,128)(2,1)}, bf16[192,256]{1,0:T(8,128)(2,1)S(1)}, u32[]{:S(2)}, u32[]{:S(2)}) collective-permute-start(bf16[192,256]{1,0:T(8,128)(2,1)} %pack.3), channel_id=1, source_target_pairs={{0,0},{1,8},{8,1},{9,9},{2,2},{3,10},{10,3},{11,11},{4,4},{5,12},{... | collective-permute-start | bytes 294920 | tf_op jit(solution)/shard_map/ppermute | solution.py:328
  21.0 6.0 %all-to-all-start = ((bf16[4,192,256]{2,1,0:T(8,128)(2,1)}), bf16[4,192,256]{2,1,0:T(8,128)(2,1)S(1)}, u32[]{:S(2)}, u32[]{:S(2)}) async-start(bf16[4,192,256]{2,1,0:T(8,128)(2,1)} %broadcast_in_dim.868), calls=%async_computation | async-start | bytes 786432 | tf_op jit(solution)/shard_map/all_to_all | solution.py:347
  30.0 3.3 %collective-permute-start.3 = (f32[608,128]{1,0:T(8,128)S(1)}, f32[608,128]{1,0:T(8,128)S(1)}, u32[]{:S(2)}, u32[]{:S(2)}) collective-permute-start(f32[608,128]{1,0:T(8,128)S(1)} %concatenate.65), channel_id=1, source_target_pairs={{0,1},{1,0},{2,3},{3,2},{4,5},{5,4},{6,7},{7,6},{8,9},{9,8},{10,11... | collective-permute-start | bytes 933896 | tf_op jit(solution)/shard_map/ppermute | solution.py:383
  34.5 3.7 %all-to-all-done = bf16[4,192,256]{2,1,0:T(8,128)(2,1)S(1)} async-done(((bf16[4,192,256]{2,1,0:T(8,128)(2,1)}), bf16[4,192,256]{2,1,0:T(8,128)(2,1)S(1)}, u32[]{:S(2)}, u32[]{:S(2)}) %all-to-all-start) | async-done | bytes 393248 | tf_op jit(solution)/shard_map/all_to_all | solution.py:347
  38.2 3.4 %norm.1 = bf16[192,2048]{1,0:T(8,128)(2,1)} custom-call(s32[1]{0:T(128)} %bitcast.core_ref, bf16[192,4096]{1,0:T(8,128)(2,1)} %tokens_ref, f32[1,4096]{1,0:T(1,128)} %bitcast.202), custom_call_target="tpu_custom_call" | custom-call | tf_op jit(solution)/shard_map/norm/pallas_call | solution.py:354
  44.6 5.8 %collective-permute-start.1 = (bf16[192,256]{1,0:T(8,128)(2,1)S(1)}, bf16[192,256]{1,0:T(8,128)(2,1)S(1)}, u32[]{:S(2)}, u32[]{:S(2)}) collective-permute-start(bf16[192,256]{1,0:T(8,128)(2,1)S(1)} %copy-done.10), channel_id=1, source_target_pairs={{0,0},{1,8},{8,1},{9,9},{2,2},{3,10},{10,3},{11,11},{4,4},{5,12},{... | collective-permute-start | bytes 294920 | tf_op jit(solution)/shard_map/ppermute | solution.py:328
  55.6 14.0 %collective-permute-done.1 = bf16[192,256]{1,0:T(8,128)(2,1)S(1)} collective-permute-done((bf16[192,256]{1,0:T(8,128)(2,1)S(1)}, bf16[192,256]{1,0:T(8,128)(2,1)S(1)}, u32[]{:S(2)}, u32[]{:S(2)}) %collective-permute-start.1) | collective-permute-done | bytes 98336 | tf_op jit(solution)/shard_map/ppermute | solution.py:328
  70.4 3.8 %all-to-all-start.1 = ((bf16[4,192,256]{2,1,0:T(8,128)(2,1)}), bf16[4,192,256]{2,1,0:T(8,128)(2,1)S(1)}, u32[]{:S(2)}, u32[]{:S(2)}) async-start(bf16[4,192,256]{2,1,0:T(8,128)(2,1)} %broadcast_in_dim.869), calls=%async_computation.1 | async-start | bytes 786432 | tf_op jit(solution)/shard_map/all_to_all | solution.py:363
  78.7 2.2 %fusion.3.mix_imag_ref = bf16[1024,256]{1,0:T(8,128)(2,1)} fusion(bf16[1024,16]{0,1:T(8,128)(2,1)} %convert_element_type.71, s32[256]{0:T(256)} %get-tuple-element.190, s32[256]{0:T(256)} %get-tuple-element.191, s32[1024]{0:T(1024)} %get-tuple-element.184, s32[1024]{0:T(1024)} %get-tuple-element.187, pred[1024]{0:T(1024)(128)(4,1)} %get-tuple-element.189, ...), kind=kOutput, calls=%fused_computation.7 | convolution fusion | flops 9707520 | bytes 570880 | tf_op jit(solution)/shard_map/dot_general | solution.py:285
  92.9 6.9 %all-gather.7.cloned.1.call-done = bf16[32,192,256]{2,1,0:T(8,128)(2,1)} async-done(((bf16[4,192,256]{2,1,0:T(8,128)(2,1)}), bf16[32,192,256]{2,1,0:T(8,128)(2,1)}) %all-gather.7.cloned.1.call-update) | async-done | bytes 3145744 | tf_op jit(solution)/shard_map/all_gather | solution.py:348
  99.9 5.8 %project.1 = (f32[192,768]{1,0:T(8,128)}, f32[192,768]{1,0:T(8,128)}) custom-call(bf16[192,2048]{1,0:T(8,128)(2,1)} %get-tuple-element.49.keep_ref, bf16[192,2048]{1,0:T(8,128)(2,1)} %get-tuple-element.119.send_ref, bf16[8,4,192,256]{3,2,1,0:T(8,128)(2,1)} %bitcast.77), custom_call_target="tpu_custom_call" | custom-call | tf_op jit(solution)/shard_map/project/pallas_call | solution.py:462
  105.6 2.7 %collective-permute-start.4 = (f32[192,768]{1,0:T(8,128)}, f32[192,768]{1,0:T(8,128)S(1)}, u32[]{:S(2)}, u32[]{:S(2)}) collective-permute-start(f32[192,768]{1,0:T(8,128)} %get-tuple-element.51), channel_id=1, source_target_pairs={{0,1},{1,0},{2,3},{3,2},{4,5},{5,4},{6,7},{7,6},{8,9},{9,8},{10,11... | collective-permute-start | bytes 1769480 | tf_op jit(solution)/shard_map/ppermute | solution.py:469
  111.0 4.3 %first.1 = (bf16[192,256]{1,0:T(8,128)(2,1)}, bf16[192,256]{1,0:T(8,128)(2,1)}, f32[192,1024]{1,0:T(8,128)}, f32[192,1024]{1,0:T(8,128)}, f32[8,16,128]{2,1,0:T(8,128)}) custom-call(f32[192,768]{1,0:T(8,128)} %get-tuple-element.50.kept_ref, f32[192,768]{1,0:T(8,128)} %copy-done.8, bf16[256,1024]{1,0:T(8,128)(2,1)} %fusion.drive_real_ref, ...), custom_call_target="tpu_custom_call" | custom-call | tf_op jit(solution)/shard_map/first/pallas_call | solution.py:470
  115.4 14.6 %all_to_all.25.totals_ref = f32[8,16,128]{2,1,0:T(8,128)} all-to-all(f32[8,16,128]{2,1,0:T(8,128)} %get-tuple-element.56), channel_id=1, replica_groups=mesh['z'=8,'yh'=4,'yl'=2,'x'=4,'c'=2] {'yh','c'}, dimensions={0} | all-to-all | bytes 131072 | tf_op jit(solution)/shard_map/all_to_all | solution.py:488
  131.5 3.9 %all-to-all-start.3 = ((f32[8,16,128]{2,1,0:T(8,128)}), f32[8,16,128]{2,1,0:T(8,128)S(1)}, u32[]{:S(2)}, u32[]{:S(2)}) async-start(f32[8,16,128]{2,1,0:T(8,128)} %row.1), calls=%async_computation.3 | async-start | bytes 131072 | tf_op jit(solution)/shard_map/all_to_all | solution.py:494
  136.1 3.5 %collective-permute-start.5 = (bf16[32,256]{1,0:T(8,128)(2,1)S(1)}, bf16[32,256]{1,0:T(8,128)(2,1)S(1)}, u32[]{:S(2)}, u32[]{:S(2)}) collective-permute-start(bf16[32,256]{1,0:T(8,128)(2,1)S(1)} %slice.35), channel_id=1, source_target_pairs={{0,1},{1,16},{16,17},{17,32},{32,33},{33,48},{48,49},{49,64},{64,6... | collective-permute-start | bytes 49160 | tf_op jit(solution)/shard_map/ppermute | solution.py:485
  144.1 4.2 %second.1 = (bf16[8,384,256]{2,1,0:T(8,128)(2,1)}, f32[16,128]{1,0:T(8,128)}) custom-call(f32[8,16,128]{2,1,0:T(8,128)} %all_to_all.25.totals_ref, f32[8,16,128]{2,1,0:T(8,128)} %pad_maximum_fusion.2.lead_ref, f32[8,16,128]{2,1,0:T(8,128)} %copy-done.9, f32[8,16,128]{2,1,0:T(8,128)} %pad_maximum_fusion.4.lead_rows_ref, ...), custom_call_target="tpu_custom_call" | custom-call | tf_op jit(solution)/shard_map/second/pallas_call | solution.py:503
  148.3 4.0 %all-to-all-start.4 = ((bf16[8,384,256]{2,1,0:T(8,128)(2,1)}), bf16[8,384,256]{2,1,0:T(8,128)(2,1)S(1)}, u32[]{:S(2)}, u32[]{:S(2)}) async-start(bf16[8,384,256]{2,1,0:T(8,128)(2,1)} %get-tuple-element.70), calls=%async_computation.4 | async-start | bytes 3145728 | tf_op jit(solution)/shard_map/all_to_all | solution.py:518
  152.3 18.7 %all-to-all-done.4.rows_ref = bf16[8,384,256]{2,1,0:T(8,128)(2,1)S(1)} async-done(((bf16[8,384,256]{2,1,0:T(8,128)(2,1)}), bf16[8,384,256]{2,1,0:T(8,128)(2,1)S(1)}, u32[]{:S(2)}, u32[]{:S(2)}) %all-to-all-start.4) | async-done | bytes 1572896 | tf_op jit(solution)/shard_map/all_to_all | solution.py:518
  171.0 5.5 %collective-permute-start.6 = (bf16[8,4,192,256]{3,2,1,0:T(8,128)(2,1)}, bf16[8,4,192,256]{3,2,1,0:T(8,128)(2,1)}, u32[]{:S(2)}, u32[]{:S(2)}) collective-permute-start(bf16[8,4,192,256]{3,2,1,0:T(8,128)(2,1)} %bitcast.78), channel_id=1, source_target_pairs={{0,1},{1,0},{2,3},{3,2},{4,5},{5,4},{6,7},{7,6},{8,9},{9,8},{10,11... | collective-permute-start | bytes 9437192 | tf_op jit(solution)/shard_map/ppermute | solution.py:521
  176.5 5.6 %collective-permute-done.6.other_ref = bf16[8,4,192,256]{3,2,1,0:T(8,128)(2,1)} collective-permute-done((bf16[8,4,192,256]{3,2,1,0:T(8,128)(2,1)}, bf16[8,4,192,256]{3,2,1,0:T(8,128)(2,1)}, u32[]{:S(2)}, u32[]{:S(2)}) %collective-permute-start.6) | collective-permute-done | bytes 3145760 | tf_op jit(solution)/shard_map/ppermute | solution.py:521
  182.1 5.5 %last.1 = bf16[192,512]{1,0:T(8,128)(2,1)} custom-call(s32[1]{0:T(128)} %bitcast.core_ref, bf16[8,384,256]{2,1,0:T(8,128)(2,1)} %copy-done.2, bf16[8,4,192,256]{3,2,1,0:T(8,128)(2,1)} %bitcast.79, bf16[8,4,192,256]{3,2,1,0:T(8,128)(2,1)} %collective-permute-done.6.other_ref, f32[1,2048]{1,0:T(1,128)} %bitcast.203, f32[1,2048]{1,0:T(1,128)} %bitcast.204), custom_call_target="tpu_custom_call" | custom-call | tf_op jit(solution)/shard_map/last/pallas_call | solution.py:522
  187.6 2.7 %collective-permute-start.7 = (bf16[192,512]{1,0:T(8,128)(2,1)}, bf16[192,512]{1,0:T(8,128)(2,1)S(1)}, u32[]{:S(2)}, u32[]{:S(2)}) collective-permute-start(bf16[192,512]{1,0:T(8,128)(2,1)} %last.1), channel_id=1, source_target_pairs={{0,0},{1,8},{8,1},{9,9},{2,2},{3,10},{10,3},{11,11},{4,4},{5,12},{... | collective-permute-start | bytes 589832 | tf_op jit(solution)/shard_map/ppermute | solution.py:328
  190.3 2.9 %collective-permute-start.8 = (f32[16,128]{1,0:T(8,128)S(1)}, f32[16,128]{1,0:T(8,128)S(1)}, u32[]{:S(2)}, u32[]{:S(2)}) collective-permute-start(f32[16,128]{1,0:T(8,128)S(1)} %copy-done.40), channel_id=1, source_target_pairs={{0,0},{1,8},{8,1},{9,9},{2,2},{3,10},{10,3},{11,11},{4,4},{5,12},{... | collective-permute-start | bytes 24584 | tf_op jit(solution)/shard_map/ppermute | solution.py:328
  (197 shorter events, 50.9 us)
Async XLA Ops:
  8.6 10.9 %collective-permute-start = (bf16[192,256]{1,0:T(8,128)(2,1)}, bf16[192,256]{1,0:T(8,128)(2,1)S(1)}, u32[]{:S(2)}, u32[]{:S(2)}) collective-permute-start(bf16[192,256]{1,0:T(8,128)(2,1)} %pack.3), channel_id=1, source_target_pairs={{0,0},{1,8},{8,1},{9,9},{2,2},{3,10},{10,3},{11,11},{4,4},{5,12},{... | collective-permute-start | bytes 294920 | tf_op jit(solution)/shard_map/ppermute | solution.py:328
  13.2 41.4 %copy-start.14 = (pred[24]{0:T(512)(128)(4,1)}, pred[24]{0:T(512)(128)(4,1)S(1)}, u32[]{:S(2)}) copy-start(pred[24]{0:T(512)(128)(4,1)S(1)} %get-tuple-element.200) | copy-start | bytes 76
  13.2 41.4 %copy-start.15 = (pred[24]{0:T(512)(128)(4,1)}, pred[24]{0:T(512)(128)(4,1)S(1)}, u32[]{:S(2)}) copy-start(pred[24]{0:T(512)(128)(4,1)S(1)} %get-tuple-element.201) | copy-start | bytes 76
  13.2 41.4 %copy-start.16 = (pred[24]{0:T(512)(128)(4,1)}, pred[24]{0:T(512)(128)(4,1)S(1)}, u32[]{:S(2)}) copy-start(pred[24]{0:T(512)(128)(4,1)S(1)} %get-tuple-element.202) | copy-start | bytes 76
  13.2 41.4 %copy-start.17 = (pred[24]{0:T(512)(128)(4,1)}, pred[24]{0:T(512)(128)(4,1)S(1)}, u32[]{:S(2)}) copy-start(pred[24]{0:T(512)(128)(4,1)S(1)} %get-tuple-element.203) | copy-start | bytes 76
  13.3 41.4 %copy-start.18 = (pred[24]{0:T(512)(128)(4,1)}, pred[24]{0:T(512)(128)(4,1)S(1)}, u32[]{:S(2)}) copy-start(pred[24]{0:T(512)(128)(4,1)S(1)} %get-tuple-element.204) | copy-start | bytes 76
  13.3 41.4 %copy-start.19 = (pred[24]{0:T(512)(128)(4,1)}, pred[24]{0:T(512)(128)(4,1)S(1)}, u32[]{:S(2)}) copy-start(pred[24]{0:T(512)(128)(4,1)S(1)} %get-tuple-element.205) | copy-start | bytes 76
  13.3 41.4 %copy-start.20 = (pred[24]{0:T(512)(128)(4,1)}, pred[24]{0:T(512)(128)(4,1)S(1)}, u32[]{:S(2)}) copy-start(pred[24]{0:T(512)(128)(4,1)S(1)} %get-tuple-element.206) | copy-start | bytes 76
  13.3 37.1 %copy-start.27 = (pred[8]{0:T(512)(128)(4,1)}, pred[8]{0:T(512)(128)(4,1)S(1)}, u32[]{:S(2)}) copy-start(pred[8]{0:T(512)(128)(4,1)S(1)} %get-tuple-element.196) | copy-start | bytes 28
  13.3 37.1 %copy-start.29 = (pred[8]{0:T(512)(128)(4,1)}, pred[8]{0:T(512)(128)(4,1)S(1)}, u32[]{:S(2)}) copy-start(pred[8]{0:T(512)(128)(4,1)S(1)} %get-tuple-element.197) | copy-start | bytes 28
  21.0 17.2 %all-to-all-start = ((bf16[4,192,256]{2,1,0:T(8,128)(2,1)}), bf16[4,192,256]{2,1,0:T(8,128)(2,1)S(1)}, u32[]{:S(2)}, u32[]{:S(2)}) async-start(bf16[4,192,256]{2,1,0:T(8,128)(2,1)} %broadcast_in_dim.868), calls=%async_computation | async-start | bytes 786432 | tf_op jit(solution)/shard_map/all_to_all | solution.py:347
  27.1 72.8 %all-gather.7.cloned.1.call-start = ((), (), s32[]{:S(2)}) async-start(), calls=%async_computation.6 | async-start | bytes 3538944 | tf_op jit(solution)/shard_map/all_gather | solution.py:348
  30.0 4.5 %collective-permute-start.3 = (f32[608,128]{1,0:T(8,128)S(1)}, f32[608,128]{1,0:T(8,128)S(1)}, u32[]{:S(2)}, u32[]{:S(2)}) collective-permute-start(f32[608,128]{1,0:T(8,128)S(1)} %concatenate.65), channel_id=1, source_target_pairs={{0,1},{1,0},{2,3},{3,2},{4,5},{5,4},{6,7},{7,6},{8,9},{9,8},{10,11... | collective-permute-start | bytes 933896 | tf_op jit(solution)/shard_map/ppermute | solution.py:383
  42.6 49.1 %collective-permute-start.2 = (bf16[192,2048]{1,0:T(8,128)(2,1)}, bf16[192,2048]{1,0:T(8,128)(2,1)S(1)}, u32[]{:S(2)}, u32[]{:S(2)}) collective-permute-start(bf16[192,2048]{1,0:T(8,128)(2,1)} %norm.1), channel_id=1, source_target_pairs={{0,8},{8,0},{1,9},{9,1},{2,10},{10,2},{3,11},{11,3},{4,12},{12,4},... | collective-permute-start | bytes 2359304 | tf_op jit(solution)/shard_map/ppermute | solution.py:361
  44.6 25.0 %collective-permute-start.1 = (bf16[192,256]{1,0:T(8,128)(2,1)S(1)}, bf16[192,256]{1,0:T(8,128)(2,1)S(1)}, u32[]{:S(2)}, u32[]{:S(2)}) collective-permute-start(bf16[192,256]{1,0:T(8,128)(2,1)S(1)} %copy-done.10), channel_id=1, source_target_pairs={{0,0},{1,8},{8,1},{9,9},{2,2},{3,10},{10,3},{11,11},{4,4},{5,12},{... | collective-permute-start | bytes 294920 | tf_op jit(solution)/shard_map/ppermute | solution.py:328
  70.4 12.6 %all-to-all-start.1 = ((bf16[4,192,256]{2,1,0:T(8,128)(2,1)}), bf16[4,192,256]{2,1,0:T(8,128)(2,1)S(1)}, u32[]{:S(2)}, u32[]{:S(2)}) async-start(bf16[4,192,256]{2,1,0:T(8,128)(2,1)} %broadcast_in_dim.869), calls=%async_computation.1 | async-start | bytes 786432 | tf_op jit(solution)/shard_map/all_to_all | solution.py:363
  74.2 78.2 %all-gather.5.cloned.1.call-start = ((), (), s32[]{:S(2)}) async-start(), calls=%async_computation.5 | async-start | bytes 3538944 | tf_op jit(solution)/shard_map/all_gather | solution.py:364
  105.6 4.6 %collective-permute-start.4 = (f32[192,768]{1,0:T(8,128)}, f32[192,768]{1,0:T(8,128)S(1)}, u32[]{:S(2)}, u32[]{:S(2)}) collective-permute-start(f32[192,768]{1,0:T(8,128)} %get-tuple-element.51), channel_id=1, source_target_pairs={{0,1},{1,0},{2,3},{3,2},{4,5},{5,4},{6,7},{7,6},{8,9},{9,8},{10,11... | collective-permute-start | bytes 1769480 | tf_op jit(solution)/shard_map/ppermute | solution.py:469
  131.5 11.9 %all-to-all-start.3 = ((f32[8,16,128]{2,1,0:T(8,128)}), f32[8,16,128]{2,1,0:T(8,128)S(1)}, u32[]{:S(2)}, u32[]{:S(2)}) async-start(f32[8,16,128]{2,1,0:T(8,128)} %row.1), calls=%async_computation.3 | async-start | bytes 131072 | tf_op jit(solution)/shard_map/all_to_all | solution.py:494
  136.1 4.2 %collective-permute-start.5 = (bf16[32,256]{1,0:T(8,128)(2,1)S(1)}, bf16[32,256]{1,0:T(8,128)(2,1)S(1)}, u32[]{:S(2)}, u32[]{:S(2)}) collective-permute-start(bf16[32,256]{1,0:T(8,128)(2,1)S(1)} %slice.35), channel_id=1, source_target_pairs={{0,1},{1,16},{16,17},{17,32},{32,33},{33,48},{48,49},{49,64},{64,6... | collective-permute-start | bytes 49160 | tf_op jit(solution)/shard_map/ppermute | solution.py:485
  148.3 22.7 %all-to-all-start.4 = ((bf16[8,384,256]{2,1,0:T(8,128)(2,1)}), bf16[8,384,256]{2,1,0:T(8,128)(2,1)S(1)}, u32[]{:S(2)}, u32[]{:S(2)}) async-start(bf16[8,384,256]{2,1,0:T(8,128)(2,1)} %get-tuple-element.70), calls=%async_computation.4 | async-start | bytes 3145728 | tf_op jit(solution)/shard_map/all_to_all | solution.py:518
  171.0 11.1 %collective-permute-start.6 = (bf16[8,4,192,256]{3,2,1,0:T(8,128)(2,1)}, bf16[8,4,192,256]{3,2,1,0:T(8,128)(2,1)}, u32[]{:S(2)}, u32[]{:S(2)}) collective-permute-start(bf16[8,4,192,256]{3,2,1,0:T(8,128)(2,1)} %bitcast.78), channel_id=1, source_target_pairs={{0,1},{1,0},{2,3},{3,2},{4,5},{5,4},{6,7},{7,6},{8,9},{9,8},{10,11... | collective-permute-start | bytes 9437192 | tf_op jit(solution)/shard_map/ppermute | solution.py:521
  187.6 8.4 %collective-permute-start.7 = (bf16[192,512]{1,0:T(8,128)(2,1)}, bf16[192,512]{1,0:T(8,128)(2,1)S(1)}, u32[]{:S(2)}, u32[]{:S(2)}) collective-permute-start(bf16[192,512]{1,0:T(8,128)(2,1)} %last.1), channel_id=1, source_target_pairs={{0,0},{1,8},{8,1},{9,9},{2,2},{3,10},{10,3},{11,11},{4,4},{5,12},{... | collective-permute-start | bytes 589832 | tf_op jit(solution)/shard_map/ppermute | solution.py:328
  190.3 5.0 %collective-permute-start.8 = (f32[16,128]{1,0:T(8,128)S(1)}, f32[16,128]{1,0:T(8,128)S(1)}, u32[]{:S(2)}, u32[]{:S(2)}) collective-permute-start(f32[16,128]{1,0:T(8,128)S(1)} %copy-done.40), channel_id=1, source_target_pairs={{0,0},{1,8},{8,1},{9,9},{2,2},{3,10},{10,3},{11,11},{4,4},{5,12},{... | collective-permute-start | bytes 24584 | tf_op jit(solution)/shard_map/ppermute | solution.py:328
  (33 other events, 379.8 us)
Sparse Core Ops, SparseCore 0:
  50.7 49.0 all-gather.6
  101.9 47.8 all-gather.4

commit v6 on v5

--- a/solution.py
+++ b/solution.py
@@ -42,6 +42,12 @@
         for col in range(0, ref.shape[1], width):
             out_ref[at : at + ref.shape[0]] = ref[:, col : col + width]
             at += ref.shape[0]
+
+
+def arrange_kernel(places_ref, *refs):
+    out_ref = refs[-1]
+    for at, ref in enumerate(refs[:-1]):
+        out_ref[places_ref[at]] = ref[...]
 
 
 def norm_kernel(core_ref, tokens_ref, gain_ref, out_ref):
@@ -65,32 +71,45 @@
         out_ref[:, at // 2 : at // 2 + LANES] = taken.astype(BF)
 
 
-def project_kernel(keep_ref, send_ref, weights_ref, keep_out_ref, send_out_ref, buffer_ref, sems):
+def project_kernel(
+    keep_ref, send_ref, weights_ref, keep_out_ref, send_out_ref, buffer_ref, tokens_ref, sems, token_sems
+):
     outer, inner, rows, width = buffer_ref.shape
     rows //= 3
     parts = sems.shape[0]
     per_part = outer // parts
+    length = keep_out_ref.shape[0]
+    span = per_part * inner * rows
 
     def fetch(part):
         at = pl.ds(part * per_part, per_part)
         return pltpu.make_async_copy(weights_ref.at[at], buffer_ref.at[at], sems.at[part])
 
+    def fetch_tokens(part, half):
+        ref = (send_ref, keep_ref)[half]
+        return pltpu.make_async_copy(
+            ref.at[:, pl.ds(part * span, span)],
+            tokens_ref.at[part, pl.ds(half * length, length)],
+            token_sems.at[part, half],
+        )
+
     for part in range(parts):
+        fetch_tokens(part, 0).start()
+        fetch_tokens(part, 1).start()
         fetch(part).start()
-    span = per_part * inner * rows
-    length = keep_ref.shape[0]
     for part in range(parts):
+        fetch_tokens(part, 0).wait()
+        fetch_tokens(part, 1).wait()
         fetch(part).wait()
-        lhs = jnp.concatenate([ref[:, part * span : (part + 1) * span] for ref in (send_ref, keep_ref)], axis=0)
         for kind in range(3):
             block = buffer_ref[
                 part * per_part : (part + 1) * per_part, :, kind * rows : (kind + 1) * rows, :
             ].reshape(span, width)
             cols = slice(kind * width, (kind + 1) * width)
-            product = jnp.dot(lhs, block, preferred_element_type=F32)
+            product = jnp.dot(tokens_ref[part], block, preferred_element_type=F32)
             for at, out_ref in ((0, send_out_ref), (length, keep_out_ref)):
-                rows_of_it = product[at : at + length]
-                out_ref[:, cols] = rows_of_it if part == 0 else out_ref[:, cols] + rows_of_it
+                its_rows = product[at : at + length]
+                out_ref[:, cols] = its_rows if part == 0 else out_ref[:, cols] + its_rows
 
 
 def first_kernel(
@@ -337,20 +356,32 @@
     def copies_of(shard):
         return jnp.broadcast_to(shard[None], (inner, *shard.shape))
 
-    shard_first = swapped(packed(3 * rows_in, conv_value, conv_gate, state_feed))
-    wide_first = copies_of(shard_first)
-    wide_first, decay_rate, skip_gain, conv_taps, input_real, input_imag, output_real, output_imag = (
+    smem = pl.BlockSpec(memory_space=pltpu.SMEM)
+    shard_first = packed(3 * rows_in, conv_value, conv_gate, state_feed)
+    tokens, decay_rate, skip_gain, conv_taps, input_real, input_imag, output_real, output_imag, shard_first = (
         lax.optimization_barrier(
-            (wide_first, decay_rate, skip_gain, conv_taps, input_real, input_imag, output_real, output_imag)
+            (tokens, decay_rate, skip_gain, conv_taps, input_real, input_imag, output_real, output_imag, shard_first)
         )
     )
-    rows_first = lax.all_to_all(wide_first, "yh", 0, 0, tiled=True)
+    blocks = []
+    for shift in range(inner):
+        pairs = [
+            (h * 4 + a * 2 + b, (h + shift) % inner * 4 + b * 2 + a)
+            for h in range(inner)
+            for a in range(2)
+            for b in range(2)
+        ]
+        blocks.append(lax.ppermute(shard_first, ("yh", "yl", "c"), pairs))
+    places = (lax.axis_index("yh") - lax.iota(jnp.int32, inner)) % inner
+    rows_first = pl.pallas_call(
+        arrange_kernel,
+        in_specs=[smem] + [whole(shard_first.shape)] * inner,
+        out_shape=jax.ShapeDtypeStruct((inner, *shard_first.shape), BF),
+        name="arrange",
+    )(places, *blocks)
     weights_first = lax.all_gather(rows_first, "z", axis=0, tiled=False)
     shard_last = packed(6 * rows_out, conv_project, state_value, state_gate)
-    tokens, _ = lax.optimization_barrier((tokens, rows_first))
-
     core_scalar = core.astype(jnp.int32).reshape(1)
-    smem = pl.BlockSpec(memory_space=pltpu.SMEM)
     own_half = pl.pallas_call(
         norm_kernel,
         in_specs=[smem, whole(tokens.shape), whole((1, model))],
@@ -358,8 +389,9 @@
         name="norm",
     )(core_scalar, tokens, norm_gain.reshape(1, model))
     across = [(0, 1), (1, 0)]
-    other_half = lax.ppermute(own_half, "yl", across)
-    shard_last, _ = lax.optimization_barrier((shard_last, own_half))
+    half_sent, _ = lax.optimization_barrier((own_half, rows_first))
+    other_half = lax.ppermute(half_sent, "yl", across)
+    shard_last, _ = lax.optimization_barrier((shard_last, rows_first))
     rows_last = lax.all_to_all(copies_of(swapped(shard_last)), "yh", 0, 0, tiled=True)
     weights_last = lax.all_gather(rows_last, "z", axis=0, tiled=False)
     keep = jnp.where(same, own_half, other_half)
@@ -461,9 +493,14 @@
     hbm = pl.BlockSpec(memory_space=pl.ANY)
     kept, sent = pl.pallas_call(
         project_kernel,
-        in_specs=[whole(keep.shape), whole(send.shape), hbm],
+        in_specs=[hbm, hbm, hbm],
         out_shape=[jax.ShapeDtypeStruct((length, 3 * width), F32)] * 2,
-        scratch_shapes=[pltpu.VMEM(weights_first.shape, BF), pltpu.SemaphoreType.DMA((parts,))],
+        scratch_shapes=[
+            pltpu.VMEM(weights_first.shape, BF),
+            pltpu.VMEM((parts, 2 * length, model // 2 // parts), BF),
+            pltpu.SemaphoreType.DMA((parts,)),
+            pltpu.SemaphoreType.DMA((parts, 2)),
+        ],
         name="project",
     )(keep, send, weights_first)
     received = lax.ppermute(sent, "c", across)
@@ -514,10 +551,10 @@
         skip.reshape(1, width), conv_out,
     )
     final = swapped(final)
-    final_state = final.reshape(2, groups, state_size)
     exchanged = lax.all_to_all(copies, ("x", "yl"), 0, 0, tiled=True)
 
-    weights_sent, exchanged = lax.optimization_barrier((weights_last, exchanged))
+    exchanged, final = lax.optimization_barrier((exchanged, final))
+    weights_sent, _ = lax.optimization_barrier((weights_last, copies))
     weights_other = lax.ppermute(weights_sent, "c", across)
     mixed = pl.pallas_call(
         last_kernel,
@@ -539,7 +576,7 @@
         name="last",
     )(core_scalar, exchanged, weights_last, weights_other, chan_gain.reshape(1, -1), chan_shift.reshape(1, -1))
     mixer_out = swapped(mixed)
-    return (mixer_out, final_state)
+    return (mixer_out, final.reshape(2, groups, state_size))
 
 
 def solution(mesh):

time: 205 us -> 205 us (level)
  waiting for transfers between devices: 57.1 us -> 36.6 us
  starting transfers between devices: 50.6 us -> 65.5 us
  other arithmetic: 18.3 us -> 22.8 us
  blocking collectives: 14.6 us -> 11.8 us
    ppermute x1 -> x5, starting transfers between devices: 1.91 us -> 20.3 us  [the longest x4 18.4 us: local(): blocks.append(lax.ppermute(shard_first, ('yh', 'yl', 'c'), pairs))]
    all_to_all x1, waiting for transfers between devices: 18.7 us -> 0.37 us  [local(): exchanged = lax.all_to_all(copies, ('x', 'yl'), 0, 0, tiled=True)]
    all_to_all x1, waiting for transfers between devices: 2.12 us -> 12.8 us  [local(): lax.all_to_all(copies_of(swapped(shard_last)), 'yh', 0, 0, tiled=True)]
    all_gather x1, waiting for transfers between devices: 6.94 us -> 0.01 us  [local(): weights_first = lax.all_gather(rows_first, 'z', axis=0, tiled=False)]
    all_to_all x1 -> x0, starting transfers between devices: 6.05 us -> none  [local(): rows_first = lax.all_to_all(wide_first, 'yh', 0, 0, tiled=True)]
    ppermute x4 -> x3, starting transfers between devices: 15.9 us -> 9.87 us  [swapped(): lax.ppermute(value, ('yl', 'c'), [(a * 2 + b, b * 2 + a) for a in range(2...]
    ppermute x1, waiting for transfers between devices: 5.61 us -> 0.01 us  [local(): weights_other = lax.ppermute(weights_sent, 'c', across)]
    ppermute x4 -> x3, waiting for transfers between devices: 16.1 us -> 21.1 us  [swapped(): lax.ppermute(value, ('yl', 'c'), [(a * 2 + b, b * 2 + a) for a in range(2...]
  transfers between devices with their start and end apart: 15 -> 17, of which waited for: 11 -> 8; matrix products, arithmetic and copies ran while one was open for 15% -> 18% of each run, Pallas kernels for 9% -> 11%
where the time goes in v6:
time: 205 us; the launch traced here: 202 us
  starting transfers between devices  65.5 us (32%)
  waiting for transfers between devices  36.6 us (18%)
  Pallas kernels  29.4 us (14%)
  other arithmetic  22.8 us (11%)
  between operations  14.8 us (7%)
  local copies, waits for them, and re-layouts  12.6 us (6%)
  blocking collectives  11.8 us (6%)
  matrix products  8.09 us (4%)
    ppermute x3, waiting for transfers between devices, swapped(): lax.ppermute(value, ('yl', 'c'), [(a * 2 + b, b * 2 + a) for a in range(2...  21.1 us
    ppermute x4, starting transfers between devices, local(): blocks.append(lax.ppermute(shard_first, ('yh', 'yl', 'c'), pairs))  18.4 us
    all_to_all x1, waiting for transfers between devices, local(): lax.all_to_all(copies_of(swapped(shard_last)), 'yh', 0, 0, tiled=True)  12.8 us
    all_to_all x1, blocking collectives, local(): totals = lax.all_to_all(total, SEQUENCE[1:], 0, 0, tiled=True)  11.8 us
    ppermute x3, starting transfers between devices, swapped(): lax.ppermute(value, ('yl', 'c'), [(a * 2 + b, b * 2 + a) for a in range(2...  9.87 us
    all_to_all x1, starting transfers between devices, local(): ends_of_rows = lax.all_to_all(end_of_row, SEQUENCE[0], 0, 0, tiled=True)  8.62 us
    dot_general x4, matrix products, spread(): jnp.dot(blocks.astype(BF), pick.astype(BF), preferred_element_type=F32)  8.09 us
    unnamed x57, local copies, waits for them, and re-layouts  7 us
  transfers between devices with their start and end apart: 17, of which 8 were waited for; matrix products, arithmetic and copies ran while one was open for 18% of the time, Pallas kernels for 11%

profile of v6, /device:TPU:1, one launch (start us, length us, event | category | flops | bytes accessed | tf_op | source)
XLA Modules:
  0.0 201.6 jit_solution(17853550801531018827)
XLA Ops:
  8.6 4.6 %collective-permute-start = (bf16[192,256]{1,0:T(8,128)(2,1)}, bf16[192,256]{1,0:T(8,128)(2,1)S(1)}, u32[]{:S(2)}, u32[]{:S(2)}) collective-permute-start(bf16[192,256]{1,0:T(8,128)(2,1)} %pack.2), channel_id=1, source_target_pairs={{0,0},{1,8},{8,1},{9,9},{16,16},{17,24},{24,17},{25,25},{32,32},{3... | collective-permute-start | bytes 294920 | tf_op jit(solution)/shard_map/ppermute | solution.py:374
  13.2 3.9 %collective-permute-start.1 = (bf16[192,256]{1,0:T(8,128)(2,1)}, bf16[192,256]{1,0:T(8,128)(2,1)S(1)}, u32[]{:S(2)}, u32[]{:S(2)}) collective-permute-start(bf16[192,256]{1,0:T(8,128)(2,1)} %pack.2), channel_id=1, source_target_pairs={{0,16},{1,24},{8,17},{9,25},{16,32},{17,40},{24,33},{25,41},{32,48... | collective-permute-start | bytes 294920 | tf_op jit(solution)/shard_map/ppermute | solution.py:374
  17.2 4.4 %collective-permute-start.2 = (bf16[192,256]{1,0:T(8,128)(2,1)}, bf16[192,256]{1,0:T(8,128)(2,1)S(1)}, u32[]{:S(2)}, u32[]{:S(2)}) collective-permute-start(bf16[192,256]{1,0:T(8,128)(2,1)} %pack.2), channel_id=1, source_target_pairs={{0,32},{1,40},{8,33},{9,41},{16,48},{17,56},{24,49},{25,57},{32,0}... | collective-permute-start | bytes 294920 | tf_op jit(solution)/shard_map/ppermute | solution.py:374
  21.6 5.5 %collective-permute-start.3 = (bf16[192,256]{1,0:T(8,128)(2,1)}, bf16[192,256]{1,0:T(8,128)(2,1)S(1)}, u32[]{:S(2)}, u32[]{:S(2)}) collective-permute-start(bf16[192,256]{1,0:T(8,128)(2,1)} %pack.2), channel_id=1, source_target_pairs={{0,48},{1,56},{8,49},{9,57},{16,0},{17,8},{24,1},{25,9},{32,16},{3... | collective-permute-start | bytes 294920 | tf_op jit(solution)/shard_map/ppermute | solution.py:374
  42.6 3.4 %norm.1 = bf16[192,2048]{1,0:T(8,128)(2,1)} custom-call(s32[1]{0:T(128)} %bitcast.core_ref, bf16[192,4096]{1,0:T(8,128)(2,1)} %tokens_ref, f32[1,4096]{1,0:T(1,128)} %bitcast.202), custom_call_target="tpu_custom_call" | custom-call | tf_op jit(solution)/shard_map/norm/pallas_call | solution.py:385
  48.1 2.6 %collective-permute-start.9 = (bf16[192,256]{1,0:T(8,128)(2,1)}, bf16[192,256]{1,0:T(8,128)(2,1)S(1)}, u32[]{:S(2)}, u32[]{:S(2)}) collective-permute-start(bf16[192,256]{1,0:T(8,128)(2,1)} %pack.3), channel_id=1, source_target_pairs={{0,0},{1,8},{8,1},{9,9},{2,2},{3,10},{10,3},{11,11},{4,4},{5,12},{... | collective-permute-start | bytes 294920 | tf_op jit(solution)/shard_map/ppermute | solution.py:347
  55.0 6.4 %all-to-all-start.3 = ((bf16[4,192,256]{2,1,0:T(8,128)(2,1)}), bf16[4,192,256]{2,1,0:T(8,128)(2,1)S(1)}, u32[]{:S(2)}, u32[]{:S(2)}) async-start(bf16[4,192,256]{2,1,0:T(8,128)(2,1)} %broadcast_in_dim.913), calls=%async_computation.3 | async-start | bytes 786432 | tf_op jit(solution)/shard_map/all_to_all | solution.py:395
  68.0 12.8 %all-to-all-done.3 = bf16[4,192,256]{2,1,0:T(8,128)(2,1)S(1)} async-done(((bf16[4,192,256]{2,1,0:T(8,128)(2,1)}), bf16[4,192,256]{2,1,0:T(8,128)(2,1)S(1)}, u32[]{:S(2)}, u32[]{:S(2)}) %all-to-all-start.3) | async-done | bytes 393248 | tf_op jit(solution)/shard_map/all_to_all | solution.py:395
  86.5 2.6 %fusion.3.mix_imag_ref = bf16[1024,256]{1,0:T(8,128)(2,1)} fusion(bf16[1024,16]{0,1:T(8,128)(2,1)S(1)} %convert_element_type.71, s32[256]{0:T(256)} %get-tuple-element.194, s32[256]{0:T(256)} %get-tuple-element.195, s32[1024]{0:T(1024)S(1)} %get-tuple-element.188, s32[1024]{0:T(1024)S(1)} %get-tuple-element.191, pred[1024]{0:T(1024)(128)(4,1)} %get-tuple-element.193, ...), kind=kOutput, calls=%fused_computation.7 | convolution fusion | flops 9707520 | bytes 570880 | tf_op jit(solution)/shard_map/dot_general | solution.py:304
  89.1 2.6 %fusion.2.mix_real_ref = bf16[1024,256]{1,0:T(8,128)(2,1)} fusion(bf16[1024,16]{0,1:T(8,128)(2,1)S(1)} %convert_element_type.66, s32[256]{0:T(256)} %get-tuple-element.194, s32[256]{0:T(256)} %get-tuple-element.195, s32[1024]{0:T(1024)S(1)} %get-tuple-element.188, s32[1024]{0:T(1024)S(1)} %get-tuple-element.191, pred[1024]{0:T(1024)(128)(4,1)} %get-tuple-element.193, ...), kind=kOutput, calls=%fused_computation.6 | convolution fusion | flops 9707520 | bytes 570880 | tf_op jit(solution)/shard_map/dot_general | solution.py:304
  98.0 4.9 %project.1 = (f32[192,768]{1,0:T(8,128)}, f32[192,768]{1,0:T(8,128)}) custom-call(bf16[192,2048]{1,0:T(8,128)(2,1)} %get-tuple-element.51.keep_ref, bf16[192,2048]{1,0:T(8,128)(2,1)} %get-tuple-element.123.send_ref, bf16[8,4,192,256]{3,2,1,0:T(8,128)(2,1)} %bitcast.77), custom_call_target="tpu_custom_call" | custom-call | tf_op jit(solution)/shard_map/project/pallas_call | solution.py:494
  102.9 6.0 %collective-permute-start.6 = (f32[192,768]{1,0:T(8,128)}, f32[192,768]{1,0:T(8,128)S(1)}, u32[]{:S(2)}, u32[]{:S(2)}) collective-permute-start(f32[192,768]{1,0:T(8,128)} %get-tuple-element.53), channel_id=1, source_target_pairs={{0,1},{1,0},{2,3},{3,2},{4,5},{5,4},{6,7},{7,6},{8,9},{9,8},{10,11... | collective-permute-start | bytes 1769480 | tf_op jit(solution)/shard_map/ppermute | solution.py:506
  111.5 4.4 %first.1 = (bf16[192,256]{1,0:T(8,128)(2,1)}, bf16[192,256]{1,0:T(8,128)(2,1)}, f32[192,1024]{1,0:T(8,128)}, f32[192,1024]{1,0:T(8,128)}, f32[8,16,128]{2,1,0:T(8,128)}) custom-call(f32[192,768]{1,0:T(8,128)} %get-tuple-element.52.kept_ref, f32[192,768]{1,0:T(8,128)} %copy-done.7, bf16[256,1024]{1,0:T(8,128)(2,1)} %fusion.drive_real_ref, ...), custom_call_target="tpu_custom_call" | custom-call | tf_op jit(solution)/shard_map/first/pallas_call | solution.py:507
  115.9 11.8 %all_to_all.20.totals_ref = f32[8,16,128]{2,1,0:T(8,128)} all-to-all(f32[8,16,128]{2,1,0:T(8,128)} %get-tuple-element.58), channel_id=1, replica_groups=mesh['z'=8,'yh'=4,'yl'=2,'x'=4,'c'=2] {'yh','c'}, dimensions={0} | all-to-all | bytes 131072 | tf_op jit(solution)/shard_map/all_to_all | solution.py:525
  129.3 8.6 %all-to-all-start.1 = ((f32[8,16,128]{2,1,0:T(8,128)}), f32[8,16,128]{2,1,0:T(8,128)S(1)}, u32[]{:S(2)}, u32[]{:S(2)}) async-start(f32[8,16,128]{2,1,0:T(8,128)} %row.1), calls=%async_computation.1 | async-start | bytes 131072 | tf_op jit(solution)/shard_map/all_to_all | solution.py:531
  138.6 3.0 %collective-permute-start.7 = (bf16[32,256]{1,0:T(8,128)(2,1)S(1)}, bf16[32,256]{1,0:T(8,128)(2,1)S(1)}, u32[]{:S(2)}, u32[]{:S(2)}) collective-permute-start(bf16[32,256]{1,0:T(8,128)(2,1)S(1)} %slice.35), channel_id=1, source_target_pairs={{0,1},{1,16},{16,17},{17,32},{32,33},{33,48},{48,49},{49,64},{64,6... | collective-permute-start | bytes 49160 | tf_op jit(solution)/shard_map/ppermute | solution.py:522
  145.7 4.2 %second.1 = (bf16[8,384,256]{2,1,0:T(8,128)(2,1)}, f32[16,128]{1,0:T(8,128)}) custom-call(f32[8,16,128]{2,1,0:T(8,128)} %all_to_all.20.totals_ref, f32[8,16,128]{2,1,0:T(8,128)} %pad_maximum_fusion.2.lead_ref, f32[8,16,128]{2,1,0:T(8,128)} %copy-done.8, f32[8,16,128]{2,1,0:T(8,128)} %pad_maximum_fusion.4.lead_rows_ref, ...), custom_call_target="tpu_custom_call" | custom-call | tf_op jit(solution)/shard_map/second/pallas_call | solution.py:540
  150.0 4.3 %collective-permute-start.10 = (bf16[8,4,192,256]{3,2,1,0:T(8,128)(2,1)}, bf16[8,4,192,256]{3,2,1,0:T(8,128)(2,1)}, u32[]{:S(2)}, u32[]{:S(2)}) collective-permute-start(bf16[8,4,192,256]{3,2,1,0:T(8,128)(2,1)} %bitcast.78), channel_id=1, source_target_pairs={{0,1},{1,0},{2,3},{3,2},{4,5},{5,4},{6,7},{7,6},{8,9},{9,8},{10,11... | collective-permute-start | bytes 9437192 | tf_op jit(solution)/shard_map/ppermute | solution.py:558
  154.3 4.7 %all-to-all-start.2 = ((bf16[8,384,256]{2,1,0:T(8,128)(2,1)}), bf16[8,384,256]{2,1,0:T(8,128)(2,1)S(1)}, u32[]{:S(2)}, u32[]{:S(2)}) async-start(bf16[8,384,256]{2,1,0:T(8,128)(2,1)} %get-tuple-element.72), calls=%async_computation.2 | async-start | bytes 3145728 | tf_op jit(solution)/shard_map/all_to_all | solution.py:554
  159.0 3.8 %collective-permute-start.8 = (f32[16,128]{1,0:T(8,128)S(1)}, f32[16,128]{1,0:T(8,128)S(1)}, u32[]{:S(2)}, u32[]{:S(2)}) collective-permute-start(f32[16,128]{1,0:T(8,128)S(1)} %copy-done.26), channel_id=1, source_target_pairs={{0,0},{1,8},{8,1},{9,9},{2,2},{3,10},{10,3},{11,11},{4,4},{5,12},{... | collective-permute-start | bytes 24584 | tf_op jit(solution)/shard_map/ppermute | solution.py:347
  162.8 17.0 %collective-permute-done.8 = f32[16,128]{1,0:T(8,128)S(1)} collective-permute-done((f32[16,128]{1,0:T(8,128)S(1)}, f32[16,128]{1,0:T(8,128)S(1)}, u32[]{:S(2)}, u32[]{:S(2)}) %collective-permute-start.8) | collective-permute-done | bytes 8224 | tf_op jit(solution)/shard_map/ppermute | solution.py:347
  181.4 5.5 %last.1 = bf16[192,512]{1,0:T(8,128)(2,1)} custom-call(s32[1]{0:T(128)} %bitcast.core_ref, bf16[8,384,256]{2,1,0:T(8,128)(2,1)} %copy-done.2, bf16[8,4,192,256]{3,2,1,0:T(8,128)(2,1)} %bitcast.79, bf16[8,4,192,256]{3,2,1,0:T(8,128)(2,1)} %collective-permute-done.10.other_ref, f32[1,2048]{1,0:T(1,128)} %bitcast.203, f32[1,2048]{1,0:T(1,128)} %bitcast.204), custom_call_target="tpu_custom_call" | custom-call | tf_op jit(solution)/shard_map/last/pallas_call | solution.py:559
  186.9 3.5 %collective-permute-start.11 = (bf16[192,512]{1,0:T(8,128)(2,1)}, bf16[192,512]{1,0:T(8,128)(2,1)S(1)}, u32[]{:S(2)}, u32[]{:S(2)}) collective-permute-start(bf16[192,512]{1,0:T(8,128)(2,1)} %last.1), channel_id=1, source_target_pairs={{0,0},{1,8},{8,1},{9,9},{2,2},{3,10},{10,3},{11,11},{4,4},{5,12},{... | collective-permute-start | bytes 589832 | tf_op jit(solution)/shard_map/ppermute | solution.py:347
  191.1 3.0 %collective-permute-done.11 = bf16[192,512]{1,0:T(8,128)(2,1)S(1)} collective-permute-done((bf16[192,512]{1,0:T(8,128)(2,1)}, bf16[192,512]{1,0:T(8,128)(2,1)S(1)}, u32[]{:S(2)}, u32[]{:S(2)}) %collective-permute-start.11) | collective-permute-done | bytes 196640 | tf_op jit(solution)/shard_map/ppermute | solution.py:347
  (174 shorter events, 53.3 us)
Async XLA Ops:
  7.2 90.9 %all-gather.5.cloned.1.call-start = ((), (), s32[]{:S(2)}) async-start(), calls=%async_computation.4 | async-start | bytes 3538944 | tf_op jit(solution)/shard_map/all_gather | solution.py:382
  8.6 30.7 %collective-permute-start = (bf16[192,256]{1,0:T(8,128)(2,1)}, bf16[192,256]{1,0:T(8,128)(2,1)S(1)}, u32[]{:S(2)}, u32[]{:S(2)}) collective-permute-start(bf16[192,256]{1,0:T(8,128)(2,1)} %pack.2), channel_id=1, source_target_pairs={{0,0},{1,8},{8,1},{9,9},{16,16},{17,24},{24,17},{25,25},{32,32},{3... | collective-permute-start | bytes 294920 | tf_op jit(solution)/shard_map/ppermute | solution.py:374
  13.2 26.1 %collective-permute-start.1 = (bf16[192,256]{1,0:T(8,128)(2,1)}, bf16[192,256]{1,0:T(8,128)(2,1)S(1)}, u32[]{:S(2)}, u32[]{:S(2)}) collective-permute-start(bf16[192,256]{1,0:T(8,128)(2,1)} %pack.2), channel_id=1, source_target_pairs={{0,16},{1,24},{8,17},{9,25},{16,32},{17,40},{24,33},{25,41},{32,48... | collective-permute-start | bytes 294920 | tf_op jit(solution)/shard_map/ppermute | solution.py:374
  17.2 22.2 %collective-permute-start.2 = (bf16[192,256]{1,0:T(8,128)(2,1)}, bf16[192,256]{1,0:T(8,128)(2,1)S(1)}, u32[]{:S(2)}, u32[]{:S(2)}) collective-permute-start(bf16[192,256]{1,0:T(8,128)(2,1)} %pack.2), channel_id=1, source_target_pairs={{0,32},{1,40},{8,33},{9,41},{16,48},{17,56},{24,49},{25,57},{32,0}... | collective-permute-start | bytes 294920 | tf_op jit(solution)/shard_map/ppermute | solution.py:374
  21.6 17.8 %collective-permute-start.3 = (bf16[192,256]{1,0:T(8,128)(2,1)}, bf16[192,256]{1,0:T(8,128)(2,1)S(1)}, u32[]{:S(2)}, u32[]{:S(2)}) collective-permute-start(bf16[192,256]{1,0:T(8,128)(2,1)} %pack.2), channel_id=1, source_target_pairs={{0,48},{1,56},{8,49},{9,57},{16,0},{17,8},{24,1},{25,9},{32,16},{3... | collective-permute-start | bytes 294920 | tf_op jit(solution)/shard_map/ppermute | solution.py:374
  31.5 29.9 %collective-permute-start.5 = (f32[608,128]{1,0:T(8,128)S(1)}, f32[608,128]{1,0:T(8,128)S(1)}, u32[]{:S(2)}, u32[]{:S(2)}) collective-permute-start(f32[608,128]{1,0:T(8,128)S(1)} %concatenate.65), channel_id=1, source_target_pairs={{0,1},{1,0},{2,3},{3,2},{4,5},{5,4},{6,7},{7,6},{8,9},{9,8},{10,11... | collective-permute-start | bytes 933896 | tf_op jit(solution)/shard_map/ppermute | solution.py:415
  33.9 30.0 %copy-start.15 = (pred[8]{0:T(512)(128)(4,1)}, pred[8]{0:T(512)(128)(4,1)S(1)}, u32[]{:S(2)}) copy-start(pred[8]{0:T(512)(128)(4,1)S(1)} %get-tuple-element.219) | copy-start | bytes 28
  33.9 30.0 %copy-start.16 = (pred[8]{0:T(512)(128)(4,1)}, pred[8]{0:T(512)(128)(4,1)S(1)}, u32[]{:S(2)}) copy-start(pred[8]{0:T(512)(128)(4,1)S(1)} %get-tuple-element.220) | copy-start | bytes 28
  34.0 30.0 %copy-start.17 = (pred[8]{0:T(512)(128)(4,1)}, pred[8]{0:T(512)(128)(4,1)S(1)}, u32[]{:S(2)}) copy-start(pred[8]{0:T(512)(128)(4,1)S(1)} %get-tuple-element.221) | copy-start | bytes 28
  34.0 30.0 %copy-start.18 = (pred[8]{0:T(512)(128)(4,1)}, pred[8]{0:T(512)(128)(4,1)S(1)}, u32[]{:S(2)}) copy-start(pred[8]{0:T(512)(128)(4,1)S(1)} %get-tuple-element.222) | copy-start | bytes 28
  34.0 30.0 %copy-start.19 = (pred[8]{0:T(512)(128)(4,1)}, pred[8]{0:T(512)(128)(4,1)S(1)}, u32[]{:S(2)}) copy-start(pred[8]{0:T(512)(128)(4,1)S(1)} %get-tuple-element.223) | copy-start | bytes 28
  34.0 30.0 %copy-start.20 = (pred[8]{0:T(512)(128)(4,1)}, pred[8]{0:T(512)(128)(4,1)S(1)}, u32[]{:S(2)}) copy-start(pred[8]{0:T(512)(128)(4,1)S(1)} %get-tuple-element.224) | copy-start | bytes 28
  48.1 6.1 %collective-permute-start.9 = (bf16[192,256]{1,0:T(8,128)(2,1)}, bf16[192,256]{1,0:T(8,128)(2,1)S(1)}, u32[]{:S(2)}, u32[]{:S(2)}) collective-permute-start(bf16[192,256]{1,0:T(8,128)(2,1)} %pack.3), channel_id=1, source_target_pairs={{0,0},{1,8},{8,1},{9,9},{2,2},{3,10},{10,3},{11,11},{4,4},{5,12},{... | collective-permute-start | bytes 294920 | tf_op jit(solution)/shard_map/ppermute | solution.py:347
  51.2 45.5 %collective-permute-start.4 = (bf16[192,2048]{1,0:T(8,128)(2,1)}, bf16[192,2048]{1,0:T(8,128)(2,1)S(1)}, u32[]{:S(2)}, u32[]{:S(2)}) collective-permute-start(bf16[192,2048]{1,0:T(8,128)(2,1)} %norm.1), channel_id=1, source_target_pairs={{0,8},{8,0},{1,9},{9,1},{2,10},{10,2},{3,11},{11,3},{4,12},{12,4},... | collective-permute-start | bytes 2359304 | tf_op jit(solution)/shard_map/ppermute | solution.py:393
  55.0 25.7 %all-to-all-start.3 = ((bf16[4,192,256]{2,1,0:T(8,128)(2,1)}), bf16[4,192,256]{2,1,0:T(8,128)(2,1)S(1)}, u32[]{:S(2)}, u32[]{:S(2)}) async-start(bf16[4,192,256]{2,1,0:T(8,128)(2,1)} %broadcast_in_dim.913), calls=%async_computation.3 | async-start | bytes 786432 | tf_op jit(solution)/shard_map/all_to_all | solution.py:395
  61.4 88.5 %all-gather.7.cloned.1.call-start = ((), (), s32[]{:S(2)}) async-start(), calls=%async_computation.5 | async-start | bytes 3538944 | tf_op jit(solution)/shard_map/all_gather | solution.py:396
  62.7 29.0 %copy-start.3 = (f32[192,1024]{1,0:T(8,128)}, f32[192,1024]{1,0:T(8,128)S(1)}, u32[]{:S(2)}) copy-start(f32[192,1024]{1,0:T(8,128)S(1)} %get-tuple-element.65.power_imag_ref) | copy-start | bytes 2359300
  102.9 7.8 %collective-permute-start.6 = (f32[192,768]{1,0:T(8,128)}, f32[192,768]{1,0:T(8,128)S(1)}, u32[]{:S(2)}, u32[]{:S(2)}) collective-permute-start(f32[192,768]{1,0:T(8,128)} %get-tuple-element.53), channel_id=1, source_target_pairs={{0,1},{1,0},{2,3},{3,2},{4,5},{5,4},{6,7},{7,6},{8,9},{9,8},{10,11... | collective-permute-start | bytes 1769480 | tf_op jit(solution)/shard_map/ppermute | solution.py:506
  129.3 15.8 %all-to-all-start.1 = ((f32[8,16,128]{2,1,0:T(8,128)}), f32[8,16,128]{2,1,0:T(8,128)S(1)}, u32[]{:S(2)}, u32[]{:S(2)}) async-start(f32[8,16,128]{2,1,0:T(8,128)} %row.1), calls=%async_computation.1 | async-start | bytes 131072 | tf_op jit(solution)/shard_map/all_to_all | solution.py:531
  138.6 3.7 %collective-permute-start.7 = (bf16[32,256]{1,0:T(8,128)(2,1)S(1)}, bf16[32,256]{1,0:T(8,128)(2,1)S(1)}, u32[]{:S(2)}, u32[]{:S(2)}) collective-permute-start(bf16[32,256]{1,0:T(8,128)(2,1)S(1)} %slice.35), channel_id=1, source_target_pairs={{0,1},{1,16},{16,17},{17,32},{32,33},{33,48},{48,49},{49,64},{64,6... | collective-permute-start | bytes 49160 | tf_op jit(solution)/shard_map/ppermute | solution.py:522
  150.0 30.2 %collective-permute-start.10 = (bf16[8,4,192,256]{3,2,1,0:T(8,128)(2,1)}, bf16[8,4,192,256]{3,2,1,0:T(8,128)(2,1)}, u32[]{:S(2)}, u32[]{:S(2)}) collective-permute-start(bf16[8,4,192,256]{3,2,1,0:T(8,128)(2,1)} %bitcast.78), channel_id=1, source_target_pairs={{0,1},{1,0},{2,3},{3,2},{4,5},{5,4},{6,7},{7,6},{8,9},{9,8},{10,11... | collective-permute-start | bytes 9437192 | tf_op jit(solution)/shard_map/ppermute | solution.py:558
  154.3 25.9 %all-to-all-start.2 = ((bf16[8,384,256]{2,1,0:T(8,128)(2,1)}), bf16[8,384,256]{2,1,0:T(8,128)(2,1)S(1)}, u32[]{:S(2)}, u32[]{:S(2)}) async-start(bf16[8,384,256]{2,1,0:T(8,128)(2,1)} %get-tuple-element.72), calls=%async_computation.2 | async-start | bytes 3145728 | tf_op jit(solution)/shard_map/all_to_all | solution.py:554
  159.0 20.8 %collective-permute-start.8 = (f32[16,128]{1,0:T(8,128)S(1)}, f32[16,128]{1,0:T(8,128)S(1)}, u32[]{:S(2)}, u32[]{:S(2)}) collective-permute-start(f32[16,128]{1,0:T(8,128)S(1)} %copy-done.26), channel_id=1, source_target_pairs={{0,0},{1,8},{8,1},{9,9},{2,2},{3,10},{10,3},{11,11},{4,4},{5,12},{... | collective-permute-start | bytes 24584 | tf_op jit(solution)/shard_map/ppermute | solution.py:347
  186.9 7.2 %collective-permute-start.11 = (bf16[192,512]{1,0:T(8,128)(2,1)}, bf16[192,512]{1,0:T(8,128)(2,1)S(1)}, u32[]{:S(2)}, u32[]{:S(2)}) collective-permute-start(bf16[192,512]{1,0:T(8,128)(2,1)} %last.1), channel_id=1, source_target_pairs={{0,0},{1,8},{8,1},{9,9},{2,2},{3,10},{10,3},{11,11},{4,4},{5,12},{... | collective-permute-start | bytes 589832 | tf_op jit(solution)/shard_map/ppermute | solution.py:347
  (21 other events, 166.4 us)
Sparse Core Ops, SparseCore 0:
  42.7 47.5 all-gather.4
  92.4 46.4 all-gather.6

commit v7 on v6

--- a/solution.py
+++ b/solution.py
@@ -377,6 +377,7 @@
         arrange_kernel,
         in_specs=[smem] + [whole(shard_first.shape)] * inner,
         out_shape=jax.ShapeDtypeStruct((inner, *shard_first.shape), BF),
+        compiler_params=grant(4),
         name="arrange",
     )(places, *blocks)
     weights_first = lax.all_gather(rows_first, "z", axis=0, tiled=False)
@@ -393,7 +394,6 @@
     other_half = lax.ppermute(half_sent, "yl", across)
     shard_last, _ = lax.optimization_barrier((shard_last, rows_first))
     rows_last = lax.all_to_all(copies_of(swapped(shard_last)), "yh", 0, 0, tiled=True)
-    weights_last = lax.all_gather(rows_last, "z", axis=0, tiled=False)
     keep = jnp.where(same, own_half, other_half)
     send = jnp.where(same, other_half, own_half)
 
@@ -481,12 +481,13 @@
         )
     )
     (
-        keep, drive_real, drive_imag, mix_real, mix_imag, power_real, power_imag, undo_real, undo_imag, lead, tail, lead_rows,
+        rows_last, keep, drive_real, drive_imag, mix_real, mix_imag, power_real, power_imag, undo_real, undo_imag, lead, tail, lead_rows,
         tail_rows, ends
     ) = lax.optimization_barrier((
-        keep, drive_real, drive_imag, mix_real, mix_imag, power_real, power_imag, undo_real, undo_imag, lead, tail, lead_rows,
+        rows_last, keep, drive_real, drive_imag, mix_real, mix_imag, power_real, power_imag, undo_real, undo_imag, lead, tail, lead_rows,
         tail_rows, ends
     ))
+    weights_last = lax.all_gather(rows_last, "z", axis=0, tiled=False)
     chunks = flat // LANES
 
     parts = 4

time: 205 us -> 201 us (0.980); the launches traced: 202 us -> 200 us
  starting transfers between devices: 65.5 us -> 55.4 us
  other arithmetic: 22.8 us -> 26.8 us
  waiting for transfers between devices: 36.6 us -> 39.8 us
  blocking collectives: 11.8 us -> 14.7 us
    all_gather x1, waiting for transfers between devices: 0.01 us -> 13.6 us  [local(): weights_first = lax.all_gather(rows_first, 'z', axis=0, tiled=False)]
    all_to_all x1, waiting for transfers between devices: 12.8 us -> 0.01 us  [local(): lax.all_to_all(copies_of(swapped(shard_last)), 'yh', 0, 0, tiled=True)]
    all_to_all x1, starting transfers between devices: 8.62 us -> 3.84 us  [local(): ends_of_rows = lax.all_to_all(end_of_row, SEQUENCE[0], 0, 0, tiled=True)]
    ppermute x1, starting transfers between devices: 5.95 us -> 2.75 us  [local(): received = lax.ppermute(sent, 'c', across)]
    all_to_all x1, blocking collectives: 11.8 us -> 14.7 us  [local(): totals = lax.all_to_all(total, SEQUENCE[1:], 0, 0, tiled=True)]
    all_gather x1, waiting for transfers between devices: 0.02 us -> 2.36 us  [local(): weights_last = lax.all_gather(rows_last, 'z', axis=0, tiled=False)]
    unnamed x57 -> x55, local copies, waits for them, and re-layouts: 7 us -> 5.7 us
  transfers between devices with their start and end apart: 17 -> 17, of which waited for: 8 -> 9; matrix products, arithmetic and copies ran while one was open for 18% -> 20% of each run, Pallas kernels for 11% -> 11%
where the time goes in v7:
time: 201 us; the launch traced here: 200 us
  starting transfers between devices  55.4 us (28%)
  waiting for transfers between devices  39.8 us (20%)
  Pallas kernels  28.8 us (14%)
  other arithmetic  26.8 us (13%)
  between operations  14.8 us (7%)
  blocking collectives  14.7 us (7%)
  local copies, waits for them, and re-layouts  12 us (6%)
  matrix products  7.43 us (4%)
    ppermute x3, waiting for transfers between devices, swapped(): lax.ppermute(value, ('yl', 'c'), [(a * 2 + b, b * 2 + a) for a in range(2...  20.8 us
    ppermute x4, starting transfers between devices, local(): blocks.append(lax.ppermute(shard_first, ('yh', 'yl', 'c'), pairs))  17.2 us
    all_to_all x1, blocking collectives, local(): totals = lax.all_to_all(total, SEQUENCE[1:], 0, 0, tiled=True)  14.7 us
    all_gather x1, waiting for transfers between devices, local(): weights_first = lax.all_gather(rows_first, 'z', axis=0, tiled=False)  13.6 us
    ppermute x3, starting transfers between devices, swapped(): lax.ppermute(value, ('yl', 'c'), [(a * 2 + b, b * 2 + a) for a in range(2...  9.85 us
    dot_general x4, matrix products, spread(): jnp.dot(blocks.astype(BF), pick.astype(BF), preferred_element_type=F32)  7.43 us
    all_to_all x1, starting transfers between devices, local(): lax.all_to_all(copies_of(swapped(shard_last)), 'yh', 0, 0, tiled=True)  6.44 us
    unnamed x55, local copies, waits for them, and re-layouts  5.7 us
  transfers between devices with their start and end apart: 17, of which 9 were waited for; matrix products, arithmetic and copies ran while one was open for 20% of the time, Pallas kernels for 11%

profile of v7, /device:TPU:1, one launch (start us, length us, event | category | flops | bytes accessed | tf_op | source)
XLA Modules:
  0.0 199.7 jit_solution(11392305056082606988)
XLA Ops:
  8.6 6.5 %collective-permute-start.3 = (bf16[192,256]{1,0:T(8,128)(2,1)}, bf16[192,256]{1,0:T(8,128)(2,1)S(1)}, u32[]{:S(2)}, u32[]{:S(2)}) collective-permute-start(bf16[192,256]{1,0:T(8,128)(2,1)} %pack.3), channel_id=1, source_target_pairs={{0,48},{1,56},{8,49},{9,57},{16,0},{17,8},{24,1},{25,9},{32,16},{3... | collective-permute-start | bytes 294920 | tf_op jit(solution)/shard_map/ppermute | solution.py:374
  15.1 4.0 %collective-permute-start.2 = (bf16[192,256]{1,0:T(8,128)(2,1)}, bf16[192,256]{1,0:T(8,128)(2,1)S(1)}, u32[]{:S(2)}, u32[]{:S(2)}) collective-permute-start(bf16[192,256]{1,0:T(8,128)(2,1)} %pack.3), channel_id=1, source_target_pairs={{0,32},{1,40},{8,33},{9,41},{16,48},{17,56},{24,49},{25,57},{32,0}... | collective-permute-start | bytes 294920 | tf_op jit(solution)/shard_map/ppermute | solution.py:374
  19.2 4.0 %collective-permute-start.1 = (bf16[192,256]{1,0:T(8,128)(2,1)}, bf16[192,256]{1,0:T(8,128)(2,1)S(1)}, u32[]{:S(2)}, u32[]{:S(2)}) collective-permute-start(bf16[192,256]{1,0:T(8,128)(2,1)} %pack.3), channel_id=1, source_target_pairs={{0,16},{1,24},{8,17},{9,25},{16,32},{17,40},{24,33},{25,41},{32,48... | collective-permute-start | bytes 294920 | tf_op jit(solution)/shard_map/ppermute | solution.py:374
  23.2 2.7 %collective-permute-start = (bf16[192,256]{1,0:T(8,128)(2,1)}, bf16[192,256]{1,0:T(8,128)(2,1)S(1)}, u32[]{:S(2)}, u32[]{:S(2)}) collective-permute-start(bf16[192,256]{1,0:T(8,128)(2,1)} %pack.3), channel_id=1, source_target_pairs={{0,0},{1,8},{8,1},{9,9},{16,16},{17,24},{24,17},{25,25},{32,32},{3... | collective-permute-start | bytes 294920 | tf_op jit(solution)/shard_map/ppermute | solution.py:374
  41.7 3.4 %norm.1 = bf16[192,2048]{1,0:T(8,128)(2,1)} custom-call(s32[1]{0:T(128)} %bitcast.core_ref, bf16[192,4096]{1,0:T(8,128)(2,1)} %tokens_ref, f32[1,4096]{1,0:T(1,128)} %bitcast.202), custom_call_target="tpu_custom_call" | custom-call | tf_op jit(solution)/shard_map/norm/pallas_call | solution.py:386
  47.0 2.6 %collective-permute-start.4 = (bf16[192,256]{1,0:T(8,128)(2,1)S(1)}, bf16[192,256]{1,0:T(8,128)(2,1)S(1)}, u32[]{:S(2)}, u32[]{:S(2)}) collective-permute-start(bf16[192,256]{1,0:T(8,128)(2,1)S(1)} %copy-done.9), channel_id=1, source_target_pairs={{0,0},{1,8},{8,1},{9,9},{2,2},{3,10},{10,3},{11,11},{4,4},{5,12},{... | collective-permute-start | bytes 294920 | tf_op jit(solution)/shard_map/ppermute | solution.py:347
  53.7 6.4 %all-to-all-start = ((bf16[4,192,256]{2,1,0:T(8,128)(2,1)}), bf16[4,192,256]{2,1,0:T(8,128)(2,1)S(1)}, u32[]{:S(2)}, u32[]{:S(2)}) async-start(bf16[4,192,256]{2,1,0:T(8,128)(2,1)} %broadcast_in_dim.862), calls=%async_computation | async-start | bytes 786432 | tf_op jit(solution)/shard_map/all_to_all | solution.py:396
  75.3 2.3 %fusion.2.mix_real_ref = bf16[1024,256]{1,0:T(8,128)(2,1)} fusion(bf16[1024,16]{0,1:T(8,128)(2,1)S(1)} %convert_element_type.66, s32[256]{0:T(256)} %get-tuple-element.196, s32[256]{0:T(256)} %get-tuple-element.197, s32[1024]{0:T(1024)} %get-tuple-element.190, s32[1024]{0:T(1024)} %get-tuple-element.193, pred[1024]{0:T(1024)(128)(4,1)} %get-tuple-element.195, ...), kind=kOutput, calls=%fused_computation.6 | convolution fusion | flops 9707520 | bytes 570880 | tf_op jit(solution)/shard_map/dot_general | solution.py:304
  86.0 13.6 %all-gather.5.cloned.1.call-done = bf16[32,192,256]{2,1,0:T(8,128)(2,1)} async-done(((bf16[4,192,256]{2,1,0:T(8,128)(2,1)}), bf16[32,192,256]{2,1,0:T(8,128)(2,1)}) %all-gather.5.cloned.1.call-update) | async-done | bytes 3145744 | tf_op jit(solution)/shard_map/all_gather | solution.py:383
  99.6 4.9 %project.1 = (f32[192,768]{1,0:T(8,128)}, f32[192,768]{1,0:T(8,128)}) custom-call(bf16[192,2048]{1,0:T(8,128)(2,1)} %get-tuple-element.53.keep_ref, bf16[192,2048]{1,0:T(8,128)(2,1)} %get-tuple-element.125.send_ref, bf16[8,4,192,256]{3,2,1,0:T(8,128)(2,1)} %bitcast.77), custom_call_target="tpu_custom_call" | custom-call | tf_op jit(solution)/shard_map/project/pallas_call | solution.py:495
  104.5 2.7 %collective-permute-start.7 = (f32[192,768]{1,0:T(8,128)}, f32[192,768]{1,0:T(8,128)S(1)}, u32[]{:S(2)}, u32[]{:S(2)}) collective-permute-start(f32[192,768]{1,0:T(8,128)} %get-tuple-element.55), channel_id=1, source_target_pairs={{0,1},{1,0},{2,3},{3,2},{4,5},{5,4},{6,7},{7,6},{8,9},{9,8},{10,11... | collective-permute-start | bytes 1769480 | tf_op jit(solution)/shard_map/ppermute | solution.py:507
  109.9 4.3 %first.1 = (bf16[192,256]{1,0:T(8,128)(2,1)}, bf16[192,256]{1,0:T(8,128)(2,1)}, f32[192,1024]{1,0:T(8,128)}, f32[192,1024]{1,0:T(8,128)}, f32[8,16,128]{2,1,0:T(8,128)}) custom-call(f32[192,768]{1,0:T(8,128)} %get-tuple-element.54.kept_ref, f32[192,768]{1,0:T(8,128)} %copy-done.7, bf16[256,1024]{1,0:T(8,128)(2,1)} %fusion.drive_real_ref, ...), custom_call_target="tpu_custom_call" | custom-call | tf_op jit(solution)/shard_map/first/pallas_call | solution.py:508
  114.2 14.7 %all_to_all.20.totals_ref = f32[8,16,128]{2,1,0:T(8,128)} all-to-all(f32[8,16,128]{2,1,0:T(8,128)} %get-tuple-element.60), channel_id=1, replica_groups=mesh['z'=8,'yh'=4,'yl'=2,'x'=4,'c'=2] {'yh','c'}, dimensions={0} | all-to-all | bytes 131072 | tf_op jit(solution)/shard_map/all_to_all | solution.py:526
  130.3 3.8 %all-to-all-start.2 = ((f32[8,16,128]{2,1,0:T(8,128)}), f32[8,16,128]{2,1,0:T(8,128)S(1)}, u32[]{:S(2)}, u32[]{:S(2)}) async-start(f32[8,16,128]{2,1,0:T(8,128)} %row.1), calls=%async_computation.2 | async-start | bytes 131072 | tf_op jit(solution)/shard_map/all_to_all | solution.py:532
  134.9 3.5 %collective-permute-start.8 = (bf16[32,256]{1,0:T(8,128)(2,1)S(1)}, bf16[32,256]{1,0:T(8,128)(2,1)S(1)}, u32[]{:S(2)}, u32[]{:S(2)}) collective-permute-start(bf16[32,256]{1,0:T(8,128)(2,1)S(1)} %slice.35), channel_id=1, source_target_pairs={{0,1},{1,16},{16,17},{17,32},{32,33},{33,48},{48,49},{49,64},{64,6... | collective-permute-start | bytes 49160 | tf_op jit(solution)/shard_map/ppermute | solution.py:523
  142.9 4.3 %second.1 = (bf16[8,384,256]{2,1,0:T(8,128)(2,1)}, f32[16,128]{1,0:T(8,128)}) custom-call(f32[8,16,128]{2,1,0:T(8,128)} %all_to_all.20.totals_ref, f32[8,16,128]{2,1,0:T(8,128)} %pad_maximum_fusion.2.lead_ref, f32[8,16,128]{2,1,0:T(8,128)} %copy-done.8, f32[8,16,128]{2,1,0:T(8,128)} %pad_maximum_fusion.4.lead_rows_ref, ...), custom_call_target="tpu_custom_call" | custom-call | tf_op jit(solution)/shard_map/second/pallas_call | solution.py:541
  147.2 2.4 %all-gather.7.cloned.1.call-done = bf16[32,192,256]{2,1,0:T(8,128)(2,1)} async-done(((bf16[4,192,256]{2,1,0:T(8,128)(2,1)}), bf16[32,192,256]{2,1,0:T(8,128)(2,1)}) %all-gather.7.cloned.1.call-update) | async-done | bytes 3145744 | tf_op jit(solution)/shard_map/all_gather | solution.py:490
  149.5 2.7 %collective-permute-start.10 = (bf16[8,4,192,256]{3,2,1,0:T(8,128)(2,1)}, bf16[8,4,192,256]{3,2,1,0:T(8,128)(2,1)}, u32[]{:S(2)}, u32[]{:S(2)}) collective-permute-start(bf16[8,4,192,256]{3,2,1,0:T(8,128)(2,1)} %bitcast.78), channel_id=1, source_target_pairs={{0,1},{1,0},{2,3},{3,2},{4,5},{5,4},{6,7},{7,6},{8,9},{9,8},{10,11... | collective-permute-start | bytes 9437192 | tf_op jit(solution)/shard_map/ppermute | solution.py:559
  152.3 4.9 %all-to-all-start.3 = ((bf16[8,384,256]{2,1,0:T(8,128)(2,1)}), bf16[8,384,256]{2,1,0:T(8,128)(2,1)S(1)}, u32[]{:S(2)}, u32[]{:S(2)}) async-start(bf16[8,384,256]{2,1,0:T(8,128)(2,1)} %get-tuple-element.74), calls=%async_computation.3 | async-start | bytes 3145728 | tf_op jit(solution)/shard_map/all_to_all | solution.py:555
  157.2 3.8 %collective-permute-start.9 = (f32[16,128]{1,0:T(8,128)S(1)}, f32[16,128]{1,0:T(8,128)S(1)}, u32[]{:S(2)}, u32[]{:S(2)}) collective-permute-start(f32[16,128]{1,0:T(8,128)S(1)} %copy-done.25), channel_id=1, source_target_pairs={{0,0},{1,8},{8,1},{9,9},{2,2},{3,10},{10,3},{11,11},{4,4},{5,12},{... | collective-permute-start | bytes 24584 | tf_op jit(solution)/shard_map/ppermute | solution.py:347
  161.0 17.0 %collective-permute-done.9 = f32[16,128]{1,0:T(8,128)S(1)} collective-permute-done((f32[16,128]{1,0:T(8,128)S(1)}, f32[16,128]{1,0:T(8,128)S(1)}, u32[]{:S(2)}, u32[]{:S(2)}) %collective-permute-start.9) | collective-permute-done | bytes 8224 | tf_op jit(solution)/shard_map/ppermute | solution.py:347
  179.6 5.5 %last.1 = bf16[192,512]{1,0:T(8,128)(2,1)} custom-call(s32[1]{0:T(128)} %bitcast.core_ref, bf16[8,384,256]{2,1,0:T(8,128)(2,1)} %copy-done.2, bf16[8,4,192,256]{3,2,1,0:T(8,128)(2,1)} %bitcast.79, bf16[8,4,192,256]{3,2,1,0:T(8,128)(2,1)} %collective-permute-done.10.other_ref, f32[1,2048]{1,0:T(1,128)} %bitcast.203, f32[1,2048]{1,0:T(1,128)} %bitcast.204), custom_call_target="tpu_custom_call" | custom-call | tf_op jit(solution)/shard_map/last/pallas_call | solution.py:560
  185.0 3.5 %collective-permute-start.11 = (bf16[192,512]{1,0:T(8,128)(2,1)}, bf16[192,512]{1,0:T(8,128)(2,1)S(1)}, u32[]{:S(2)}, u32[]{:S(2)}) collective-permute-start(bf16[192,512]{1,0:T(8,128)(2,1)} %last.1), channel_id=1, source_target_pairs={{0,0},{1,8},{8,1},{9,9},{2,2},{3,10},{10,3},{11,11},{4,4},{5,12},{... | collective-permute-start | bytes 589832 | tf_op jit(solution)/shard_map/ppermute | solution.py:347
  189.2 3.0 %collective-permute-done.11 = bf16[192,512]{1,0:T(8,128)(2,1)S(1)} collective-permute-done((bf16[192,512]{1,0:T(8,128)(2,1)}, bf16[192,512]{1,0:T(8,128)(2,1)S(1)}, u32[]{:S(2)}, u32[]{:S(2)}) %collective-permute-start.11) | collective-permute-done | bytes 196640 | tf_op jit(solution)/shard_map/ppermute | solution.py:347
  (172 shorter events, 58.5 us)
Async XLA Ops:
  7.2 92.4 %all-gather.5.cloned.1.call-start = ((), (), s32[]{:S(2)}) async-start(), calls=%async_computation.4 | async-start | bytes 3538944 | tf_op jit(solution)/shard_map/all_gather | solution.py:383
  8.6 36.9 %collective-permute-start.3 = (bf16[192,256]{1,0:T(8,128)(2,1)}, bf16[192,256]{1,0:T(8,128)(2,1)S(1)}, u32[]{:S(2)}, u32[]{:S(2)}) collective-permute-start(bf16[192,256]{1,0:T(8,128)(2,1)} %pack.3), channel_id=1, source_target_pairs={{0,48},{1,56},{8,49},{9,57},{16,0},{17,8},{24,1},{25,9},{32,16},{3... | collective-permute-start | bytes 294920 | tf_op jit(solution)/shard_map/ppermute | solution.py:374
  15.1 30.5 %collective-permute-start.2 = (bf16[192,256]{1,0:T(8,128)(2,1)}, bf16[192,256]{1,0:T(8,128)(2,1)S(1)}, u32[]{:S(2)}, u32[]{:S(2)}) collective-permute-start(bf16[192,256]{1,0:T(8,128)(2,1)} %pack.3), channel_id=1, source_target_pairs={{0,32},{1,40},{8,33},{9,41},{16,48},{17,56},{24,49},{25,57},{32,0}... | collective-permute-start | bytes 294920 | tf_op jit(solution)/shard_map/ppermute | solution.py:374
  19.2 26.4 %collective-permute-start.1 = (bf16[192,256]{1,0:T(8,128)(2,1)}, bf16[192,256]{1,0:T(8,128)(2,1)S(1)}, u32[]{:S(2)}, u32[]{:S(2)}) collective-permute-start(bf16[192,256]{1,0:T(8,128)(2,1)} %pack.3), channel_id=1, source_target_pairs={{0,16},{1,24},{8,17},{9,25},{16,32},{17,40},{24,33},{25,41},{32,48... | collective-permute-start | bytes 294920 | tf_op jit(solution)/shard_map/ppermute | solution.py:374
  23.2 22.4 %collective-permute-start = (bf16[192,256]{1,0:T(8,128)(2,1)}, bf16[192,256]{1,0:T(8,128)(2,1)S(1)}, u32[]{:S(2)}, u32[]{:S(2)}) collective-permute-start(bf16[192,256]{1,0:T(8,128)(2,1)} %pack.3), channel_id=1, source_target_pairs={{0,0},{1,8},{8,1},{9,9},{16,16},{17,24},{24,17},{25,25},{32,32},{3... | collective-permute-start | bytes 294920 | tf_op jit(solution)/shard_map/ppermute | solution.py:374
  30.3 29.8 %collective-permute-start.6 = (f32[608,128]{1,0:T(8,128)S(1)}, f32[608,128]{1,0:T(8,128)S(1)}, u32[]{:S(2)}, u32[]{:S(2)}) collective-permute-start(f32[608,128]{1,0:T(8,128)S(1)} %concatenate.65), channel_id=1, source_target_pairs={{0,1},{1,0},{2,3},{3,2},{4,5},{5,4},{6,7},{7,6},{8,9},{9,8},{10,11... | collective-permute-start | bytes 933896 | tf_op jit(solution)/shard_map/ppermute | solution.py:415
  32.7 28.1 %copy-start.10 = (pred[24]{0:T(512)(128)(4,1)}, pred[24]{0:T(512)(128)(4,1)S(1)}, u32[]{:S(2)}) copy-start(pred[24]{0:T(512)(128)(4,1)S(1)} %get-tuple-element.209) | copy-start | bytes 76
  32.7 28.1 %copy-start.11 = (pred[24]{0:T(512)(128)(4,1)}, pred[24]{0:T(512)(128)(4,1)S(1)}, u32[]{:S(2)}) copy-start(pred[24]{0:T(512)(128)(4,1)S(1)} %get-tuple-element.206) | copy-start | bytes 76
  32.7 28.1 %copy-start.12 = (pred[24]{0:T(512)(128)(4,1)}, pred[24]{0:T(512)(128)(4,1)S(1)}, u32[]{:S(2)}) copy-start(pred[24]{0:T(512)(128)(4,1)S(1)} %get-tuple-element.207) | copy-start | bytes 76
  32.7 28.4 %copy-start.17 = (pred[8]{0:T(512)(128)(4,1)}, pred[8]{0:T(512)(128)(4,1)S(1)}, u32[]{:S(2)}) copy-start(pred[8]{0:T(512)(128)(4,1)S(1)} %get-tuple-element.204) | copy-start | bytes 28
  32.7 28.4 %copy-start.18 = (pred[8]{0:T(512)(128)(4,1)}, pred[8]{0:T(512)(128)(4,1)S(1)}, u32[]{:S(2)}) copy-start(pred[8]{0:T(512)(128)(4,1)S(1)} %get-tuple-element.205) | copy-start | bytes 28
  32.8 28.3 %copy-start.19 = (pred[8]{0:T(512)(128)(4,1)}, pred[8]{0:T(512)(128)(4,1)S(1)}, u32[]{:S(2)}) copy-start(pred[8]{0:T(512)(128)(4,1)S(1)} %get-tuple-element.202) | copy-start | bytes 28
  32.8 28.3 %copy-start.20 = (pred[8]{0:T(512)(128)(4,1)}, pred[8]{0:T(512)(128)(4,1)S(1)}, u32[]{:S(2)}) copy-start(pred[8]{0:T(512)(128)(4,1)S(1)} %get-tuple-element.203) | copy-start | bytes 28
  47.0 5.9 %collective-permute-start.4 = (bf16[192,256]{1,0:T(8,128)(2,1)S(1)}, bf16[192,256]{1,0:T(8,128)(2,1)S(1)}, u32[]{:S(2)}, u32[]{:S(2)}) collective-permute-start(bf16[192,256]{1,0:T(8,128)(2,1)S(1)} %copy-done.9), channel_id=1, source_target_pairs={{0,0},{1,8},{8,1},{9,9},{2,2},{3,10},{10,3},{11,11},{4,4},{5,12},{... | collective-permute-start | bytes 294920 | tf_op jit(solution)/shard_map/ppermute | solution.py:347
  50.2 33.8 %collective-permute-start.5 = (bf16[192,2048]{1,0:T(8,128)(2,1)}, bf16[192,2048]{1,0:T(8,128)(2,1)S(1)}, u32[]{:S(2)}, u32[]{:S(2)}) collective-permute-start(bf16[192,2048]{1,0:T(8,128)(2,1)} %norm.1), channel_id=1, source_target_pairs={{0,8},{8,0},{1,9},{9,1},{2,10},{10,2},{3,11},{11,3},{4,12},{12,4},... | collective-permute-start | bytes 2359304 | tf_op jit(solution)/shard_map/ppermute | solution.py:394
  53.7 31.5 %all-to-all-start = ((bf16[4,192,256]{2,1,0:T(8,128)(2,1)}), bf16[4,192,256]{2,1,0:T(8,128)(2,1)S(1)}, u32[]{:S(2)}, u32[]{:S(2)}) async-start(bf16[4,192,256]{2,1,0:T(8,128)(2,1)} %broadcast_in_dim.862), calls=%async_computation | async-start | bytes 786432 | tf_op jit(solution)/shard_map/all_to_all | solution.py:396
  60.2 89.4 %all-gather.7.cloned.1.call-start = ((), (), s32[]{:S(2)}) async-start(), calls=%async_computation.5 | async-start | bytes 3538944 | tf_op jit(solution)/shard_map/all_gather | solution.py:490
  104.5 4.6 %collective-permute-start.7 = (f32[192,768]{1,0:T(8,128)}, f32[192,768]{1,0:T(8,128)S(1)}, u32[]{:S(2)}, u32[]{:S(2)}) collective-permute-start(f32[192,768]{1,0:T(8,128)} %get-tuple-element.55), channel_id=1, source_target_pairs={{0,1},{1,0},{2,3},{3,2},{4,5},{5,4},{6,7},{7,6},{8,9},{9,8},{10,11... | collective-permute-start | bytes 1769480 | tf_op jit(solution)/shard_map/ppermute | solution.py:507
  130.3 11.9 %all-to-all-start.2 = ((f32[8,16,128]{2,1,0:T(8,128)}), f32[8,16,128]{2,1,0:T(8,128)S(1)}, u32[]{:S(2)}, u32[]{:S(2)}) async-start(f32[8,16,128]{2,1,0:T(8,128)} %row.1), calls=%async_computation.2 | async-start | bytes 131072 | tf_op jit(solution)/shard_map/all_to_all | solution.py:532
  134.9 4.2 %collective-permute-start.8 = (bf16[32,256]{1,0:T(8,128)(2,1)S(1)}, bf16[32,256]{1,0:T(8,128)(2,1)S(1)}, u32[]{:S(2)}, u32[]{:S(2)}) collective-permute-start(bf16[32,256]{1,0:T(8,128)(2,1)S(1)} %slice.35), channel_id=1, source_target_pairs={{0,1},{1,16},{16,17},{17,32},{32,33},{33,48},{48,49},{49,64},{64,6... | collective-permute-start | bytes 49160 | tf_op jit(solution)/shard_map/ppermute | solution.py:523
  149.5 28.8 %collective-permute-start.10 = (bf16[8,4,192,256]{3,2,1,0:T(8,128)(2,1)}, bf16[8,4,192,256]{3,2,1,0:T(8,128)(2,1)}, u32[]{:S(2)}, u32[]{:S(2)}) collective-permute-start(bf16[8,4,192,256]{3,2,1,0:T(8,128)(2,1)} %bitcast.78), channel_id=1, source_target_pairs={{0,1},{1,0},{2,3},{3,2},{4,5},{5,4},{6,7},{7,6},{8,9},{9,8},{10,11... | collective-permute-start | bytes 9437192 | tf_op jit(solution)/shard_map/ppermute | solution.py:559
  152.3 26.1 %all-to-all-start.3 = ((bf16[8,384,256]{2,1,0:T(8,128)(2,1)}), bf16[8,384,256]{2,1,0:T(8,128)(2,1)S(1)}, u32[]{:S(2)}, u32[]{:S(2)}) async-start(bf16[8,384,256]{2,1,0:T(8,128)(2,1)} %get-tuple-element.74), calls=%async_computation.3 | async-start | bytes 3145728 | tf_op jit(solution)/shard_map/all_to_all | solution.py:555
  157.2 20.8 %collective-permute-start.9 = (f32[16,128]{1,0:T(8,128)S(1)}, f32[16,128]{1,0:T(8,128)S(1)}, u32[]{:S(2)}, u32[]{:S(2)}) collective-permute-start(f32[16,128]{1,0:T(8,128)S(1)} %copy-done.25), channel_id=1, source_target_pairs={{0,0},{1,8},{8,1},{9,9},{2,2},{3,10},{10,3},{11,11},{4,4},{5,12},{... | collective-permute-start | bytes 24584 | tf_op jit(solution)/shard_map/ppermute | solution.py:347
  185.0 7.2 %collective-permute-start.11 = (bf16[192,512]{1,0:T(8,128)(2,1)}, bf16[192,512]{1,0:T(8,128)(2,1)S(1)}, u32[]{:S(2)}, u32[]{:S(2)}) collective-permute-start(bf16[192,512]{1,0:T(8,128)(2,1)} %last.1), channel_id=1, source_target_pairs={{0,0},{1,8},{8,1},{9,9},{2,2},{3,10},{10,3},{11,11},{4,4},{5,12},{... | collective-permute-start | bytes 589832 | tf_op jit(solution)/shard_map/ppermute | solution.py:347
  (20 other events, 127.7 us)
Sparse Core Ops, SparseCore 0:
  50.3 49.2 all-gather.4
  101.7 47.8 all-gather.6

commit v8 on v7

--- a/solution.py
+++ b/solution.py
@@ -358,9 +358,9 @@
 
     smem = pl.BlockSpec(memory_space=pltpu.SMEM)
     shard_first = packed(3 * rows_in, conv_value, conv_gate, state_feed)
-    tokens, decay_rate, skip_gain, conv_taps, input_real, input_imag, output_real, output_imag, shard_first = (
+    decay_rate, skip_gain, conv_taps, input_real, input_imag, output_real, output_imag, shard_first = (
         lax.optimization_barrier(
-            (tokens, decay_rate, skip_gain, conv_taps, input_real, input_imag, output_real, output_imag, shard_first)
+            (decay_rate, skip_gain, conv_taps, input_real, input_imag, output_real, output_imag, shard_first)
         )
     )
     blocks = []
@@ -381,6 +381,9 @@
         name="arrange",
     )(places, *blocks)
     weights_first = lax.all_gather(rows_first, "z", axis=0, tiled=False)
+    tokens, conv_project, state_value, state_gate, _ = lax.optimization_barrier(
+        (tokens, conv_project, state_value, state_gate, rows_first)
+    )
     shard_last = packed(6 * rows_out, conv_project, state_value, state_gate)
     core_scalar = core.astype(jnp.int32).reshape(1)
     own_half = pl.pallas_call(
@@ -447,14 +450,21 @@
     base_imag = step_imag.reshape(flat)
     square_size = base_real * base_real + base_imag * base_imag
 
-    def powers(real, imag):
-        low = power_table(real, imag, lax.iota(jnp.int32, 8) + 1, 8)
-        high = power_table(real, imag, lax.iota(jnp.int32, length // 8) * 8, length)
-        table = rotate(high[0][:, None], high[1][:, None], low[0][None], low[1][None])
+    counted = jnp.concatenate([lax.iota(jnp.int32, 8) + 1, lax.iota(jnp.int32, length // 8) * 8])
+    counted_real, counted_imag = power_table(
+        jnp.concatenate([base_real, base_real / square_size]),
+        jnp.concatenate([base_imag, -base_imag / square_size]),
+        counted,
+        length,
+    )
+
+    def powers(cols):
+        real, imag = (counted_real[:, cols], counted_imag[:, cols])
+        table = rotate(real[8:, None], imag[8:, None], real[None, :8], imag[None, :8])
         return tuple(part.reshape(length, flat) for part in table)
 
-    power_real, power_imag = powers(base_real, base_imag)
-    undo_real, undo_imag = powers(base_real / square_size, -base_imag / square_size)
+    power_real, power_imag = powers(slice(0, flat))
+    undo_real, undo_imag = powers(slice(flat, 2 * flat))
     span_real, span_imag = (power_real[-1], power_imag[-1])
     row_devices = inner * 2
     outer = seq_devices // row_devices
@@ -463,19 +473,26 @@
     lag = in_row - lax.iota(jnp.int32, row_devices)
     lag_rows = row - lax.iota(jnp.int32, outer)
 
-    def spans(exponent, chosen=None):
-        real, imag = power_table(span_real, span_imag, jnp.maximum(exponent, 0), seq_devices)
-        if chosen is not None:
-            real, imag = (part * chosen.astype(F32)[:, None] for part in (real, imag))
-        return rows_of(real, imag)
-
-    lead = spans(lag, lag > 0)
-    tail = spans(row_devices - lax.iota(jnp.int32, row_devices))
-    lead_rows = spans((lag_rows - 1) * row_devices + in_row, lag_rows > 0)
-    tail_rows = spans((outer - 1 - lax.iota(jnp.int32, outer)) * row_devices)
+    exponents = (
+        lag,
+        row_devices - lax.iota(jnp.int32, row_devices),
+        (lag_rows - 1) * row_devices + in_row,
+        (outer - 1 - lax.iota(jnp.int32, outer)) * row_devices,
+        jnp.stack([position, jnp.int32(seq_devices)] + [jnp.int32(0)] * 6),
+    )
+    chosen = jnp.concatenate(
+        [lag > 0, jnp.ones(row_devices, bool), lag_rows > 0, jnp.ones(outer + 8, bool)]
+    ).astype(F32)[:, None]
+    spans_real, spans_imag = power_table(
+        span_real, span_imag, jnp.maximum(jnp.concatenate(exponents), 0), seq_devices
+    )
+    spans = rows_of(spans_real * chosen, spans_imag * chosen)
+    cuts = (0, row_devices, 2 * row_devices, 2 * row_devices + outer, 2 * row_devices + 2 * outer)
+    lead, tail, lead_rows, tail_rows = (spans[first:last] for first, last in zip(cuts[:-1], cuts[1:]))
     ends = rows_of(
         *rotate(
-            *power_table(span_real, span_imag, jnp.stack([position, jnp.int32(seq_devices)]), seq_devices),
+            spans_real[cuts[-1] : cuts[-1] + 2],
+            spans_imag[cuts[-1] : cuts[-1] + 2],
             initial_state[0].reshape(1, flat),
             initial_state[1].reshape(1, flat),
         )

time: 201 us -> 190 us (0.945)
  other arithmetic: 26.8 us -> 9.59 us
  waiting for transfers between devices: 39.8 us -> 48.9 us
    eq x22 -> x3, other arithmetic: 4.78 us -> 0.1 us  [power_table(): chosen = (exponent >> place & 1 == 1)[:, None]]
    all_to_all x1, waiting for transfers between devices: 0.01 us -> 4.45 us  [local(): lax.all_to_all(copies_of(swapped(shard_last)), 'yh', 0, 0, tiled=True)]
    select_n x8 -> x2, other arithmetic: 4.6 us -> 1.01 us  [power_table(): result_real = jnp.where(chosen, next_real, result_real)]
    ppermute x1, waiting for transfers between devices: 0.01 us -> 2.69 us  [local(): other_half = lax.ppermute(half_sent, 'yl', across)]
    all_gather x1, waiting for transfers between devices: 13.6 us -> 16.2 us  [local(): weights_first = lax.all_gather(rows_first, 'z', axis=0, tiled=False)]
    unnamed x55 -> x23, local copies, waits for them, and re-layouts: 5.7 us -> 5.66 us
  transfers between devices with their start and end apart: 17 -> 17, of which waited for: 9 -> 10; matrix products, arithmetic and copies ran while one was open for 20% -> 11% of each run, Pallas kernels for 11% -> 12%
where the time goes in v8:
time: 190 us; the launch traced here: 188 us
  starting transfers between devices  54.6 us (29%)
  waiting for transfers between devices  48.9 us (26%)
  Pallas kernels  28.9 us (15%)
  blocking collectives  14.6 us (8%)
  between operations  14.6 us (8%)
  local copies, waits for them, and re-layouts  11.6 us (6%)
  other arithmetic  9.59 us (5%)
  matrix products  5.47 us (3%)
    ppermute x3, waiting for transfers between devices, swapped(): lax.ppermute(value, ('yl', 'c'), [(a * 2 + b, b * 2 + a) for a in range(2...  20 us
    ppermute x4, starting transfers between devices, local(): blocks.append(lax.ppermute(shard_first, ('yh', 'yl', 'c'), pairs))  17.2 us
    all_gather x1, waiting for transfers between devices, local(): weights_first = lax.all_gather(rows_first, 'z', axis=0, tiled=False)  16.2 us
    all_to_all x1, blocking collectives, local(): totals = lax.all_to_all(total, SEQUENCE[1:], 0, 0, tiled=True)  14.6 us
    ppermute x3, starting transfers between devices, swapped(): lax.ppermute(value, ('yl', 'c'), [(a * 2 + b, b * 2 + a) for a in range(2...  9.85 us
    all_to_all x1, starting transfers between devices, local(): lax.all_to_all(copies_of(swapped(shard_last)), 'yh', 0, 0, tiled=True)  5.79 us
    unnamed x23, local copies, waits for them, and re-layouts  5.66 us
    dot_general x4, matrix products, spread(): jnp.dot(blocks.astype(BF), pick.astype(BF), preferred_element_type=F32)  5.47 us
  transfers between devices with their start and end apart: 17, of which 10 were waited for; matrix products, arithmetic and copies ran while one was open for 11% of the time, Pallas kernels for 12%

profile of v8, /device:TPU:1, one launch (start us, length us, event | category | flops | bytes accessed | tf_op | source)
XLA Modules:
  0.0 188.3 jit_solution(6221222717335665376)
XLA Ops:
  8.6 6.5 %collective-permute-start.3 = (bf16[192,256]{1,0:T(8,128)(2,1)}, bf16[192,256]{1,0:T(8,128)(2,1)S(1)}, u32[]{:S(2)}, u32[]{:S(2)}) collective-permute-start(bf16[192,256]{1,0:T(8,128)(2,1)} %pack.2), channel_id=1, source_target_pairs={{0,48},{1,56},{8,49},{9,57},{16,0},{17,8},{24,1},{25,9},{32,16},{3... | collective-permute-start | bytes 294920 | tf_op jit(solution)/shard_map/ppermute | solution.py:374
  15.1 4.0 %collective-permute-start.2 = (bf16[192,256]{1,0:T(8,128)(2,1)}, bf16[192,256]{1,0:T(8,128)(2,1)S(1)}, u32[]{:S(2)}, u32[]{:S(2)}) collective-permute-start(bf16[192,256]{1,0:T(8,128)(2,1)} %pack.2), channel_id=1, source_target_pairs={{0,32},{1,40},{8,33},{9,41},{16,48},{17,56},{24,49},{25,57},{32,0}... | collective-permute-start | bytes 294920 | tf_op jit(solution)/shard_map/ppermute | solution.py:374
  19.2 4.0 %collective-permute-start.1 = (bf16[192,256]{1,0:T(8,128)(2,1)}, bf16[192,256]{1,0:T(8,128)(2,1)S(1)}, u32[]{:S(2)}, u32[]{:S(2)}) collective-permute-start(bf16[192,256]{1,0:T(8,128)(2,1)} %pack.2), channel_id=1, source_target_pairs={{0,16},{1,24},{8,17},{9,25},{16,32},{17,40},{24,33},{25,41},{32,48... | collective-permute-start | bytes 294920 | tf_op jit(solution)/shard_map/ppermute | solution.py:374
  23.2 2.7 %collective-permute-start = (bf16[192,256]{1,0:T(8,128)(2,1)}, bf16[192,256]{1,0:T(8,128)(2,1)S(1)}, u32[]{:S(2)}, u32[]{:S(2)}) collective-permute-start(bf16[192,256]{1,0:T(8,128)(2,1)} %pack.2), channel_id=1, source_target_pairs={{0,0},{1,8},{8,1},{9,9},{16,16},{17,24},{24,17},{25,25},{32,32},{3... | collective-permute-start | bytes 294920 | tf_op jit(solution)/shard_map/ppermute | solution.py:374
  35.8 2.6 %collective-permute-start.4 = (bf16[192,256]{1,0:T(8,128)(2,1)}, bf16[192,256]{1,0:T(8,128)(2,1)S(1)}, u32[]{:S(2)}, u32[]{:S(2)}) collective-permute-start(bf16[192,256]{1,0:T(8,128)(2,1)} %pack.3), channel_id=1, source_target_pairs={{0,0},{1,8},{8,1},{9,9},{2,2},{3,10},{10,3},{11,11},{4,4},{5,12},{... | collective-permute-start | bytes 294920 | tf_op jit(solution)/shard_map/ppermute | solution.py:347
  38.5 3.4 %norm.1 = bf16[192,2048]{1,0:T(8,128)(2,1)} custom-call(s32[1]{0:T(128)} %bitcast.core_ref, bf16[192,4096]{1,0:T(8,128)(2,1)} %tokens_ref, f32[1,4096]{1,0:T(1,128)} %bitcast.154), custom_call_target="tpu_custom_call" | custom-call | tf_op jit(solution)/shard_map/norm/pallas_call | solution.py:389
  44.6 5.8 %all-to-all-start = ((bf16[4,192,256]{2,1,0:T(8,128)(2,1)}), bf16[4,192,256]{2,1,0:T(8,128)(2,1)S(1)}, u32[]{:S(2)}, u32[]{:S(2)}) async-start(bf16[4,192,256]{2,1,0:T(8,128)(2,1)} %broadcast_in_dim.262), calls=%async_computation | async-start | bytes 786432 | tf_op jit(solution)/shard_map/all_to_all | solution.py:399
  62.7 2.7 %collective-permute-done.5 = bf16[192,2048]{1,0:T(8,128)(2,1)S(1)} collective-permute-done((bf16[192,2048]{1,0:T(8,128)(2,1)}, bf16[192,2048]{1,0:T(8,128)(2,1)S(1)}, u32[]{:S(2)}, u32[]{:S(2)}) %collective-permute-start.5) | collective-permute-done | bytes 786464 | tf_op jit(solution)/shard_map/ppermute | solution.py:397
  66.6 4.4 %all-to-all-done = bf16[4,192,256]{2,1,0:T(8,128)(2,1)S(1)} async-done(((bf16[4,192,256]{2,1,0:T(8,128)(2,1)}), bf16[4,192,256]{2,1,0:T(8,128)(2,1)S(1)}, u32[]{:S(2)}, u32[]{:S(2)}) %all-to-all-start) | async-done | bytes 393248 | tf_op jit(solution)/shard_map/all_to_all | solution.py:399
  71.8 16.2 %all-gather.5.cloned.1.call-done = bf16[32,192,256]{2,1,0:T(8,128)(2,1)} async-done(((bf16[4,192,256]{2,1,0:T(8,128)(2,1)}), bf16[32,192,256]{2,1,0:T(8,128)(2,1)}) %all-gather.5.cloned.1.call-update) | async-done | bytes 3145744 | tf_op jit(solution)/shard_map/all_gather | solution.py:383
  88.0 4.9 %project.1 = (f32[192,768]{1,0:T(8,128)}, f32[192,768]{1,0:T(8,128)}) custom-call(bf16[192,2048]{1,0:T(8,128)(2,1)} %get-tuple-element.59.keep_ref, bf16[192,2048]{1,0:T(8,128)(2,1)} %get-tuple-element.112.send_ref, bf16[8,4,192,256]{3,2,1,0:T(8,128)(2,1)} %bitcast.101), custom_call_target="tpu_custom_call" | custom-call | tf_op jit(solution)/shard_map/project/pallas_call | solution.py:512
  92.9 2.7 %collective-permute-start.7 = (f32[192,768]{1,0:T(8,128)}, f32[192,768]{1,0:T(8,128)S(1)}, u32[]{:S(2)}, u32[]{:S(2)}) collective-permute-start(f32[192,768]{1,0:T(8,128)} %get-tuple-element.61), channel_id=1, source_target_pairs={{0,1},{1,0},{2,3},{3,2},{4,5},{5,4},{6,7},{7,6},{8,9},{9,8},{10,11... | collective-permute-start | bytes 1769480 | tf_op jit(solution)/shard_map/ppermute | solution.py:524
  98.3 4.4 %first.1 = (bf16[192,256]{1,0:T(8,128)(2,1)}, bf16[192,256]{1,0:T(8,128)(2,1)}, f32[192,1024]{1,0:T(8,128)}, f32[192,1024]{1,0:T(8,128)}, f32[8,16,128]{2,1,0:T(8,128)}) custom-call(f32[192,768]{1,0:T(8,128)} %get-tuple-element.60.kept_ref, f32[192,768]{1,0:T(8,128)} %copy-done.7, bf16[256,1024]{1,0:T(8,128)(2,1)} %fusion.drive_real_ref, ...), custom_call_target="tpu_custom_call" | custom-call | tf_op jit(solution)/shard_map/first/pallas_call | solution.py:525
  102.6 14.6 %all_to_all.20.totals_ref = f32[8,16,128]{2,1,0:T(8,128)} all-to-all(f32[8,16,128]{2,1,0:T(8,128)} %get-tuple-element.66), channel_id=1, replica_groups=mesh['z'=8,'yh'=4,'yl'=2,'x'=4,'c'=2] {'yh','c'}, dimensions={0} | all-to-all | bytes 131072 | tf_op jit(solution)/shard_map/all_to_all | solution.py:543
  118.8 3.9 %all-to-all-start.2 = ((f32[8,16,128]{2,1,0:T(8,128)}), f32[8,16,128]{2,1,0:T(8,128)S(1)}, u32[]{:S(2)}, u32[]{:S(2)}) async-start(f32[8,16,128]{2,1,0:T(8,128)} %row.1), calls=%async_computation.2 | async-start | bytes 131072 | tf_op jit(solution)/shard_map/all_to_all | solution.py:549
  123.4 3.4 %collective-permute-start.8 = (bf16[32,256]{1,0:T(8,128)(2,1)S(1)}, bf16[32,256]{1,0:T(8,128)(2,1)S(1)}, u32[]{:S(2)}, u32[]{:S(2)}) collective-permute-start(bf16[32,256]{1,0:T(8,128)(2,1)S(1)} %slice.103), channel_id=1, source_target_pairs={{0,1},{1,16},{16,17},{17,32},{32,33},{33,48},{48,49},{49,64},{64,6... | collective-permute-start | bytes 49160 | tf_op jit(solution)/shard_map/ppermute | solution.py:540
  131.4 4.3 %second.1 = (bf16[8,384,256]{2,1,0:T(8,128)(2,1)}, f32[16,128]{1,0:T(8,128)}) custom-call(f32[8,16,128]{2,1,0:T(8,128)} %all_to_all.20.totals_ref, f32[8,16,128]{2,1,0:T(8,128)} %get-tuple-element.67.lead_ref, f32[8,16,128]{2,1,0:T(8,128)} %copy-done.8, f32[8,16,128]{2,1,0:T(8,128)} %get-tuple-element.69.lead_rows_ref, ...), custom_call_target="tpu_custom_call" | custom-call | tf_op jit(solution)/shard_map/second/pallas_call | solution.py:558
  138.0 2.7 %collective-permute-start.10 = (bf16[8,4,192,256]{3,2,1,0:T(8,128)(2,1)}, bf16[8,4,192,256]{3,2,1,0:T(8,128)(2,1)}, u32[]{:S(2)}, u32[]{:S(2)}) collective-permute-start(bf16[8,4,192,256]{3,2,1,0:T(8,128)(2,1)} %bitcast.102), channel_id=1, source_target_pairs={{0,1},{1,0},{2,3},{3,2},{4,5},{5,4},{6,7},{7,6},{8,9},{9,8},{10,11... | collective-permute-start | bytes 9437192 | tf_op jit(solution)/shard_map/ppermute | solution.py:576
  140.7 4.9 %all-to-all-start.3 = ((bf16[8,384,256]{2,1,0:T(8,128)(2,1)}), bf16[8,384,256]{2,1,0:T(8,128)(2,1)S(1)}, u32[]{:S(2)}, u32[]{:S(2)}) async-start(bf16[8,384,256]{2,1,0:T(8,128)(2,1)} %get-tuple-element.80), calls=%async_computation.3 | async-start | bytes 3145728 | tf_op jit(solution)/shard_map/all_to_all | solution.py:572
  145.7 3.8 %collective-permute-start.9 = (f32[16,128]{1,0:T(8,128)S(1)}, f32[16,128]{1,0:T(8,128)S(1)}, u32[]{:S(2)}, u32[]{:S(2)}) collective-permute-start(f32[16,128]{1,0:T(8,128)S(1)} %copy-done.9), channel_id=1, source_target_pairs={{0,0},{1,8},{8,1},{9,9},{2,2},{3,10},{10,3},{11,11},{4,4},{5,12},{... | collective-permute-start | bytes 24584 | tf_op jit(solution)/shard_map/ppermute | solution.py:347
  149.5 17.0 %collective-permute-done.9 = f32[16,128]{1,0:T(8,128)S(1)} collective-permute-done((f32[16,128]{1,0:T(8,128)S(1)}, f32[16,128]{1,0:T(8,128)S(1)}, u32[]{:S(2)}, u32[]{:S(2)}) %collective-permute-start.9) | collective-permute-done | bytes 8224 | tf_op jit(solution)/shard_map/ppermute | solution.py:347
  168.1 5.5 %last.1 = bf16[192,512]{1,0:T(8,128)(2,1)} custom-call(s32[1]{0:T(128)} %bitcast.core_ref, bf16[8,384,256]{2,1,0:T(8,128)(2,1)} %copy-done.2, bf16[8,4,192,256]{3,2,1,0:T(8,128)(2,1)} %bitcast.103, bf16[8,4,192,256]{3,2,1,0:T(8,128)(2,1)} %collective-permute-done.10.other_ref, f32[1,2048]{1,0:T(1,128)} %bitcast.155, f32[1,2048]{1,0:T(1,128)} %bitcast.156), custom_call_target="tpu_custom_call" | custom-call | tf_op jit(solution)/shard_map/last/pallas_call | solution.py:577
  173.5 3.5 %collective-permute-start.11 = (bf16[192,512]{1,0:T(8,128)(2,1)}, bf16[192,512]{1,0:T(8,128)(2,1)S(1)}, u32[]{:S(2)}, u32[]{:S(2)}) collective-permute-start(bf16[192,512]{1,0:T(8,128)(2,1)} %last.1), channel_id=1, source_target_pairs={{0,0},{1,8},{8,1},{9,9},{2,2},{3,10},{10,3},{11,11},{4,4},{5,12},{... | collective-permute-start | bytes 589832 | tf_op jit(solution)/shard_map/ppermute | solution.py:347
  177.7 3.0 %collective-permute-done.11 = bf16[192,512]{1,0:T(8,128)(2,1)S(1)} collective-permute-done((bf16[192,512]{1,0:T(8,128)(2,1)}, bf16[192,512]{1,0:T(8,128)(2,1)S(1)}, u32[]{:S(2)}, u32[]{:S(2)}) %collective-permute-start.11) | collective-permute-done | bytes 196640 | tf_op jit(solution)/shard_map/ppermute | solution.py:347
  (121 shorter events, 42.9 us)
Async XLA Ops:
  7.2 80.9 %all-gather.5.cloned.1.call-start = ((), (), s32[]{:S(2)}) async-start(), calls=%async_computation.4 | async-start | bytes 3538944 | tf_op jit(solution)/shard_map/all_gather | solution.py:383
  8.6 24.4 %collective-permute-start.3 = (bf16[192,256]{1,0:T(8,128)(2,1)}, bf16[192,256]{1,0:T(8,128)(2,1)S(1)}, u32[]{:S(2)}, u32[]{:S(2)}) collective-permute-start(bf16[192,256]{1,0:T(8,128)(2,1)} %pack.2), channel_id=1, source_target_pairs={{0,48},{1,56},{8,49},{9,57},{16,0},{17,8},{24,1},{25,9},{32,16},{3... | collective-permute-start | bytes 294920 | tf_op jit(solution)/shard_map/ppermute | solution.py:374
  15.1 17.9 %collective-permute-start.2 = (bf16[192,256]{1,0:T(8,128)(2,1)}, bf16[192,256]{1,0:T(8,128)(2,1)S(1)}, u32[]{:S(2)}, u32[]{:S(2)}) collective-permute-start(bf16[192,256]{1,0:T(8,128)(2,1)} %pack.2), channel_id=1, source_target_pairs={{0,32},{1,40},{8,33},{9,41},{16,48},{17,56},{24,49},{25,57},{32,0}... | collective-permute-start | bytes 294920 | tf_op jit(solution)/shard_map/ppermute | solution.py:374
  19.2 13.9 %collective-permute-start.1 = (bf16[192,256]{1,0:T(8,128)(2,1)}, bf16[192,256]{1,0:T(8,128)(2,1)S(1)}, u32[]{:S(2)}, u32[]{:S(2)}) collective-permute-start(bf16[192,256]{1,0:T(8,128)(2,1)} %pack.2), channel_id=1, source_target_pairs={{0,16},{1,24},{8,17},{9,25},{16,32},{17,40},{24,33},{25,41},{32,48... | collective-permute-start | bytes 294920 | tf_op jit(solution)/shard_map/ppermute | solution.py:374
  23.2 9.9 %collective-permute-start = (bf16[192,256]{1,0:T(8,128)(2,1)}, bf16[192,256]{1,0:T(8,128)(2,1)S(1)}, u32[]{:S(2)}, u32[]{:S(2)}) collective-permute-start(bf16[192,256]{1,0:T(8,128)(2,1)} %pack.2), channel_id=1, source_target_pairs={{0,0},{1,8},{8,1},{9,9},{16,16},{17,24},{24,17},{25,25},{32,32},{3... | collective-permute-start | bytes 294920 | tf_op jit(solution)/shard_map/ppermute | solution.py:374
  30.3 20.1 %collective-permute-start.6 = (f32[608,128]{1,0:T(8,128)S(1)}, f32[608,128]{1,0:T(8,128)S(1)}, u32[]{:S(2)}, u32[]{:S(2)}) collective-permute-start(f32[608,128]{1,0:T(8,128)S(1)} %concatenate.245), channel_id=1, source_target_pairs={{0,1},{1,0},{2,3},{3,2},{4,5},{5,4},{6,7},{7,6},{8,9},{9,8},{10,11... | collective-permute-start | bytes 933896 | tf_op jit(solution)/shard_map/ppermute | solution.py:418
  35.8 8.0 %collective-permute-start.4 = (bf16[192,256]{1,0:T(8,128)(2,1)}, bf16[192,256]{1,0:T(8,128)(2,1)S(1)}, u32[]{:S(2)}, u32[]{:S(2)}) collective-permute-start(bf16[192,256]{1,0:T(8,128)(2,1)} %pack.3), channel_id=1, source_target_pairs={{0,0},{1,8},{8,1},{9,9},{2,2},{3,10},{10,3},{11,11},{4,4},{5,12},{... | collective-permute-start | bytes 294920 | tf_op jit(solution)/shard_map/ppermute | solution.py:347
  41.9 23.5 %collective-permute-start.5 = (bf16[192,2048]{1,0:T(8,128)(2,1)}, bf16[192,2048]{1,0:T(8,128)(2,1)S(1)}, u32[]{:S(2)}, u32[]{:S(2)}) collective-permute-start(bf16[192,2048]{1,0:T(8,128)(2,1)} %norm.1), channel_id=1, source_target_pairs={{0,8},{8,0},{1,9},{9,1},{2,10},{10,2},{3,11},{11,3},{4,12},{12,4},... | collective-permute-start | bytes 2359304 | tf_op jit(solution)/shard_map/ppermute | solution.py:397
  44.6 26.5 %all-to-all-start = ((bf16[4,192,256]{2,1,0:T(8,128)(2,1)}), bf16[4,192,256]{2,1,0:T(8,128)(2,1)S(1)}, u32[]{:S(2)}, u32[]{:S(2)}) async-start(bf16[4,192,256]{2,1,0:T(8,128)(2,1)} %broadcast_in_dim.262), calls=%async_computation | async-start | bytes 786432 | tf_op jit(solution)/shard_map/all_to_all | solution.py:399
  50.4 87.6 %all-gather.7.cloned.1.call-start = ((), (), s32[]{:S(2)}) async-start(), calls=%async_computation.5 | async-start | bytes 3538944 | tf_op jit(solution)/shard_map/all_gather | solution.py:507
  52.8 5.9 %copy-start.3 = (f32[192,1024]{1,0:T(8,128)}, f32[192,1024]{1,0:T(8,128)S(1)}, u32[]{:S(2)}) copy-start(f32[192,1024]{1,0:T(8,128)S(1)} %get-tuple-element.73.power_imag_ref) | copy-start | bytes 2359300
  52.9 5.9 %copy-start.4 = (f32[192,1024]{1,0:T(8,128)}, f32[192,1024]{1,0:T(8,128)S(1)}, u32[]{:S(2)}) copy-start(f32[192,1024]{1,0:T(8,128)S(1)} %get-tuple-element.72.power_real_ref) | copy-start | bytes 2359300
  57.6 7.7 %copy-start.5 = (bf16[192,2048]{1,0:T(8,128)(2,1)S(1)}, bf16[192,2048]{1,0:T(8,128)(2,1)}, u32[]{:S(2)}) copy-start(bf16[192,2048]{1,0:T(8,128)(2,1)} %norm.1) | copy-start | bytes 2359300
  92.9 4.6 %collective-permute-start.7 = (f32[192,768]{1,0:T(8,128)}, f32[192,768]{1,0:T(8,128)S(1)}, u32[]{:S(2)}, u32[]{:S(2)}) collective-permute-start(f32[192,768]{1,0:T(8,128)} %get-tuple-element.61), channel_id=1, source_target_pairs={{0,1},{1,0},{2,3},{3,2},{4,5},{5,4},{6,7},{7,6},{8,9},{9,8},{10,11... | collective-permute-start | bytes 1769480 | tf_op jit(solution)/shard_map/ppermute | solution.py:524
  97.5 0.8 copy-start.7
  118.8 11.9 %all-to-all-start.2 = ((f32[8,16,128]{2,1,0:T(8,128)}), f32[8,16,128]{2,1,0:T(8,128)S(1)}, u32[]{:S(2)}, u32[]{:S(2)}) async-start(f32[8,16,128]{2,1,0:T(8,128)} %row.1), calls=%async_computation.2 | async-start | bytes 131072 | tf_op jit(solution)/shard_map/all_to_all | solution.py:549
  123.4 4.2 %collective-permute-start.8 = (bf16[32,256]{1,0:T(8,128)(2,1)S(1)}, bf16[32,256]{1,0:T(8,128)(2,1)S(1)}, u32[]{:S(2)}, u32[]{:S(2)}) collective-permute-start(bf16[32,256]{1,0:T(8,128)(2,1)S(1)} %slice.103), channel_id=1, source_target_pairs={{0,1},{1,16},{16,17},{17,32},{32,33},{33,48},{48,49},{49,64},{64,6... | collective-permute-start | bytes 49160 | tf_op jit(solution)/shard_map/ppermute | solution.py:540
  127.6 0.9 copy-start.1
  135.6 10.0 %copy-start.9 = (f32[16,128]{1,0:T(8,128)S(1)}, f32[16,128]{1,0:T(8,128)}, u32[]{:S(2)}) copy-start(f32[16,128]{1,0:T(8,128)} %get-tuple-element.81) | copy-start | bytes 24580
  138.0 28.8 %collective-permute-start.10 = (bf16[8,4,192,256]{3,2,1,0:T(8,128)(2,1)}, bf16[8,4,192,256]{3,2,1,0:T(8,128)(2,1)}, u32[]{:S(2)}, u32[]{:S(2)}) collective-permute-start(bf16[8,4,192,256]{3,2,1,0:T(8,128)(2,1)} %bitcast.102), channel_id=1, source_target_pairs={{0,1},{1,0},{2,3},{3,2},{4,5},{5,4},{6,7},{7,6},{8,9},{9,8},{10,11... | collective-permute-start | bytes 9437192 | tf_op jit(solution)/shard_map/ppermute | solution.py:576
  140.7 26.1 %all-to-all-start.3 = ((bf16[8,384,256]{2,1,0:T(8,128)(2,1)}), bf16[8,384,256]{2,1,0:T(8,128)(2,1)S(1)}, u32[]{:S(2)}, u32[]{:S(2)}) async-start(bf16[8,384,256]{2,1,0:T(8,128)(2,1)} %get-tuple-element.80), calls=%async_computation.3 | async-start | bytes 3145728 | tf_op jit(solution)/shard_map/all_to_all | solution.py:572
  145.7 20.8 %collective-permute-start.9 = (f32[16,128]{1,0:T(8,128)S(1)}, f32[16,128]{1,0:T(8,128)S(1)}, u32[]{:S(2)}, u32[]{:S(2)}) collective-permute-start(f32[16,128]{1,0:T(8,128)S(1)} %copy-done.9), channel_id=1, source_target_pairs={{0,0},{1,8},{8,1},{9,9},{2,2},{3,10},{10,3},{11,11},{4,4},{5,12},{... | collective-permute-start | bytes 24584 | tf_op jit(solution)/shard_map/ppermute | solution.py:347
  166.8 1.2 copy-start.2
  173.5 7.2 %collective-permute-start.11 = (bf16[192,512]{1,0:T(8,128)(2,1)}, bf16[192,512]{1,0:T(8,128)(2,1)S(1)}, u32[]{:S(2)}, u32[]{:S(2)}) collective-permute-start(bf16[192,512]{1,0:T(8,128)(2,1)} %last.1), channel_id=1, source_target_pairs={{0,0},{1,8},{8,1},{9,9},{2,2},{3,10},{10,3},{11,11},{4,4},{5,12},{... | collective-permute-start | bytes 589832 | tf_op jit(solution)/shard_map/ppermute | solution.py:347
  (3 other events, 2.0 us)
Sparse Core Ops, SparseCore 0:
  38.7 49.3 all-gather.4
  90.1 47.8 all-gather.6

commit v9 on v8

--- a/solution.py
+++ b/solution.py
@@ -198,7 +198,6 @@
     mix_imag_ref,
     feed_ref,
     skip_ref,
-    conv_ref,
     out_ref,
     final_ref,
     entry_ref,
@@ -226,24 +225,20 @@
         response = response + jnp.dot(state_real.astype(BF), mix_real_ref[cols, :], preferred_element_type=F32)
         response = response + jnp.dot(state_imag.astype(BF), mix_imag_ref[cols, :], preferred_element_type=F32)
     activated = jax.nn.gelu(response).astype(BF)
-    length = activated.shape[0]
-    conv = conv_ref[...]
     for copy in range(out_ref.shape[0]):
-        out_ref[copy, :length] = conv
-        out_ref[copy, length:] = activated
+        out_ref[copy] = activated
 
 
 def last_kernel(
-    core_ref, rows_ref, own_ref, other_ref, gain_ref, shift_ref, out_ref, buffer_ref, act_ref, acc_ref, sems
+    place_ref, conv_own_ref, conv_other_ref, rows_ref, own_ref, other_ref, gain_ref, shift_ref, out_ref, buffer_ref, act_ref, acc_ref, sems
 ):
     blocks, length, width = rows_ref.shape
-    length //= 2
     outer, inner, cores, rows, _ = buffer_ref.shape
     rows //= 6
     parts = sems.shape[0]
     per_part = outer // parts
     per_block = blocks // parts
-    core = core_ref[0]
+    core = place_ref[0]
 
     def fetch(part, half):
         at = pl.ds(part * per_part, per_part)
@@ -253,18 +248,21 @@
     for part in range(parts):
         fetch(part, 0).start()
         fetch(part, 1).start()
+    def conv_block(at):
+        return jnp.where(place_ref[1] == at % 2, conv_own_ref[at // 2], conv_other_ref[at // 2]).astype(F32)
+
     channels = blocks * width
     total = jnp.zeros((length, width), F32)
     squares = jnp.zeros((length, width), F32)
     for at in range(blocks):
-        total = total + rows_ref[at, :length, :].astype(F32)
+        total = total + conv_block(at)
     mean = jnp.sum(total, axis=1, keepdims=True) / channels
     for at in range(blocks):
-        centred = rows_ref[at, :length, :].astype(F32) - mean
+        centred = conv_block(at) - mean
         squares = squares + centred * centred
     scale = lax.rsqrt(jnp.sum(squares, axis=1, keepdims=True) / channels + 1e-05)
     for at in range(blocks):
-        centred = rows_ref[at, :length, :].astype(F32) - mean
+        centred = conv_block(at) - mean
         cols = slice(at * width, (at + 1) * width)
         act_ref[:, cols] = jax.nn.silu(centred * scale * gain_ref[:, cols] + shift_ref[:, cols]).astype(BF)
     span = per_part * inner * cores * rows
@@ -273,7 +271,7 @@
         fetch(part, 1).wait()
         conv_act = act_ref[:, part * span : (part + 1) * span]
         activated = jnp.concatenate(
-            [rows_ref[part * per_block + at, length:, :] for at in range(per_block)], axis=1
+            [rows_ref[part * per_block + at] for at in range(per_block)], axis=1
         )
         for kind in range(6):
             block = buffer_ref[
@@ -373,13 +371,18 @@
         ]
         blocks.append(lax.ppermute(shard_first, ("yh", "yl", "c"), pairs))
     places = (lax.axis_index("yh") - lax.iota(jnp.int32, inner)) % inner
-    rows_first = pl.pallas_call(
-        arrange_kernel,
-        in_specs=[smem] + [whole(shard_first.shape)] * inner,
-        out_shape=jax.ShapeDtypeStruct((inner, *shard_first.shape), BF),
-        compiler_params=grant(4),
-        name="arrange",
-    )(places, *blocks)
+
+    def arranged(places, blocks):
+        shape = blocks[0].shape
+        return pl.pallas_call(
+            arrange_kernel,
+            in_specs=[smem] + [whole(shape)] * len(blocks),
+            out_shape=jax.ShapeDtypeStruct((len(blocks), *shape), BF),
+            compiler_params=grant(4),
+            name="arrange",
+        )(places, *blocks)
+
+    rows_first = arranged(places, blocks)
     weights_first = lax.all_gather(rows_first, "z", axis=0, tiled=False)
     tokens, conv_project, state_value, state_gate, _ = lax.optimization_barrier(
         (tokens, conv_project, state_value, state_gate, rows_first)
@@ -546,7 +549,6 @@
         out_shape=jax.ShapeDtypeStruct((outer, 2 * chunks, LANES), F32),
         name="row",
     )(totals, tail)
-    ends_of_rows = lax.all_to_all(end_of_row, SEQUENCE[0], 0, 0, tiled=True)
     conv_out = pl.pallas_call(
         conv_kernel,
         out_shape=jax.ShapeDtypeStruct((length, width), BF),
@@ -555,10 +557,21 @@
         name="conv",
     )(before, gated, conv_taps)
 
+    spread_x = lax.axis_size("x")
+    conv_blocks = [conv_out] + [
+        lax.ppermute(conv_out, "x", [(i, (i + shift) % spread_x) for i in range(spread_x)])
+        for shift in range(1, spread_x)
+    ]
+    conv_own = arranged((lax.axis_index("x") - lax.iota(jnp.int32, spread_x)) % spread_x, conv_blocks)
+    end_of_row, conv_own = lax.optimization_barrier((end_of_row, conv_own))
+    ends_of_rows = lax.all_to_all(end_of_row, SEQUENCE[0], 0, 0, tiled=True)
+    conv_other = lax.ppermute(conv_own, "yl", across)
+    place = jnp.stack([core, lax.axis_index("yl")]).astype(jnp.int32)
+
     copies, final = pl.pallas_call(
         second_kernel,
         out_shape=[
-            jax.ShapeDtypeStruct((tp_devices, 2 * length, width), BF),
+            jax.ShapeDtypeStruct((tp_devices, length, width), BF),
             jax.ShapeDtypeStruct((2 * chunks, LANES), F32),
         ],
         scratch_shapes=[pltpu.VMEM((2 * chunks, LANES), F32)],
@@ -566,7 +579,7 @@
     )(
         totals, lead, ends_of_rows, lead_rows, tail_rows, ends, power_real, power_imag, sums_real, sums_imag,
         mix_real, mix_imag, feed,
-        skip.reshape(1, width), conv_out,
+        skip.reshape(1, width),
     )
     final = swapped(final)
     exchanged = lax.all_to_all(copies, ("x", "yl"), 0, 0, tiled=True)
@@ -578,6 +591,8 @@
         last_kernel,
         in_specs=[
             smem,
+            whole(conv_own.shape),
+            whole(conv_other.shape),
             whole(exchanged.shape),
             hbm,
             hbm,
@@ -592,7 +607,7 @@
             pltpu.SemaphoreType.DMA((parts, 2)),
         ],
         name="last",
-    )(core_scalar, exchanged, weights_last, weights_other, chan_gain.reshape(1, -1), chan_shift.reshape(1, -1))
+    )(place, conv_own, conv_other, exchanged, weights_last, weights_other, chan_gain.reshape(1, -1), chan_shift.reshape(1, -1))
     mixer_out = swapped(mixed)
     return (mixer_out, final.reshape(2, groups, state_size))
 

time: 190 us -> 203 us (1.068)
  starting transfers between devices: 54.6 us -> 76.7 us
  blocking collectives: 14.6 us -> 0 us
  waiting for transfers between devices: 48.9 us -> 53.9 us
    all_to_all x1 -> x0, blocking collectives: 14.6 us -> none  [local(): totals = lax.all_to_all(total, SEQUENCE[1:], 0, 0, tiled=True)]
    ppermute x0 -> x4, starting transfers between devices: none -> 12.5 us  [the longest x3 9.23 us: local(): lax.ppermute(conv_out, 'x', [(i, (i + shift) % spread_x) for i in range(s...]
    all_to_all x0 -> x1, starting transfers between devices: none -> 7.15 us  [local(): totals = lax.all_to_all(total, SEQUENCE[1:], 0, 0, tiled=True)]
    ppermute x1, starting transfers between devices: 2.74 us -> 8.74 us  [local(): weights_other = lax.ppermute(weights_sent, 'c', across)]
    all_to_all x1, waiting for transfers between devices: 0.77 us -> 6.66 us  [local(): ends_of_rows = lax.all_to_all(end_of_row, SEQUENCE[0], 0, 0, tiled=True)]
    ppermute x3, starting transfers between devices: 9.85 us -> 6.69 us  [swapped(): lax.ppermute(value, ('yl', 'c'), [(a * 2 + b, b * 2 + a) for a in range(2...]
    ppermute x0 -> x4, waiting for transfers between devices: none -> 2.5 us  [the longest x3 2.49 us: local(): lax.ppermute(conv_out, 'x', [(i, (i + shift) % spread_x) for i in range(s...]
    all_gather x1, waiting for transfers between devices: 2.35 us -> 0.01 us  [local(): weights_last = lax.all_gather(rows_last, 'z', axis=0, tiled=False)]
  transfers between devices with their start and end apart: 17 -> 22, of which waited for: 10 -> 10; matrix products, arithmetic and copies ran while one was open for 11% -> 11% of each run, Pallas kernels for 12% -> 11%
where the time goes in v9:
time: 203 us; the launch traced here: 201 us
  starting transfers between devices  76.7 us (38%)
  waiting for transfers between devices  53.9 us (27%)
  Pallas kernels  29 us (14%)
  between operations  14.7 us (7%)
  local copies, waits for them, and re-layouts  11.4 us (6%)
  other arithmetic  10.1 us (5%)
  matrix products  5.48 us (3%)
    ppermute x3, waiting for transfers between devices, swapped(): lax.ppermute(value, ('yl', 'c'), [(a * 2 + b, b * 2 + a) for a in range(2...  18.8 us
    ppermute x4, starting transfers between devices, local(): blocks.append(lax.ppermute(shard_first, ('yh', 'yl', 'c'), pairs))  17.2 us
    all_gather x1, waiting for transfers between devices, local(): weights_first = lax.all_gather(rows_first, 'z', axis=0, tiled=False)  16.1 us
    ppermute x3, starting transfers between devices, local(): lax.ppermute(conv_out, 'x', [(i, (i + shift) % spread_x) for i in range(s...  9.23 us
    ppermute x1, starting transfers between devices, local(): weights_other = lax.ppermute(weights_sent, 'c', across)  8.74 us
    all_to_all x1, starting transfers between devices, local(): totals = lax.all_to_all(total, SEQUENCE[1:], 0, 0, tiled=True)  7.15 us
    ppermute x3, starting transfers between devices, swapped(): lax.ppermute(value, ('yl', 'c'), [(a * 2 + b, b * 2 + a) for a in range(2...  6.69 us
    all_to_all x1, waiting for transfers between devices, local(): ends_of_rows = lax.all_to_all(end_of_row, SEQUENCE[0], 0, 0, tiled=True)  6.66 us
  transfers between devices with their start and end apart: 22, of which 10 were waited for; matrix products, arithmetic and copies ran while one was open for 11% of the time, Pallas kernels for 11%

profile of v9, /device:TPU:1, one launch (start us, length us, event | category | flops | bytes accessed | tf_op | source)
XLA Modules:
  0.0 201.2 jit_solution(2914658935808663853)
XLA Ops:
  8.6 6.5 %collective-permute-start.3 = (bf16[192,256]{1,0:T(8,128)(2,1)}, bf16[192,256]{1,0:T(8,128)(2,1)S(1)}, u32[]{:S(2)}, u32[]{:S(2)}) collective-permute-start(bf16[192,256]{1,0:T(8,128)(2,1)} %pack.2), channel_id=1, source_target_pairs={{0,48},{1,56},{8,49},{9,57},{16,0},{17,8},{24,1},{25,9},{32,16},{3... | collective-permute-start | bytes 294920 | tf_op jit(solution)/shard_map/ppermute | solution.py:372
  15.1 4.0 %collective-permute-start.2 = (bf16[192,256]{1,0:T(8,128)(2,1)}, bf16[192,256]{1,0:T(8,128)(2,1)S(1)}, u32[]{:S(2)}, u32[]{:S(2)}) collective-permute-start(bf16[192,256]{1,0:T(8,128)(2,1)} %pack.2), channel_id=1, source_target_pairs={{0,32},{1,40},{8,33},{9,41},{16,48},{17,56},{24,49},{25,57},{32,0}... | collective-permute-start | bytes 294920 | tf_op jit(solution)/shard_map/ppermute | solution.py:372
  19.2 4.0 %collective-permute-start.1 = (bf16[192,256]{1,0:T(8,128)(2,1)}, bf16[192,256]{1,0:T(8,128)(2,1)S(1)}, u32[]{:S(2)}, u32[]{:S(2)}) collective-permute-start(bf16[192,256]{1,0:T(8,128)(2,1)} %pack.2), channel_id=1, source_target_pairs={{0,16},{1,24},{8,17},{9,25},{16,32},{17,40},{24,33},{25,41},{32,48... | collective-permute-start | bytes 294920 | tf_op jit(solution)/shard_map/ppermute | solution.py:372
  23.2 2.7 %collective-permute-start = (bf16[192,256]{1,0:T(8,128)(2,1)}, bf16[192,256]{1,0:T(8,128)(2,1)S(1)}, u32[]{:S(2)}, u32[]{:S(2)}) collective-permute-start(bf16[192,256]{1,0:T(8,128)(2,1)} %pack.2), channel_id=1, source_target_pairs={{0,0},{1,8},{8,1},{9,9},{16,16},{17,24},{24,17},{25,25},{32,32},{3... | collective-permute-start | bytes 294920 | tf_op jit(solution)/shard_map/ppermute | solution.py:372
  38.5 3.4 %norm.1 = bf16[192,2048]{1,0:T(8,128)(2,1)} custom-call(s32[1]{0:T(128)} %bitcast.core_ref, bf16[192,4096]{1,0:T(8,128)(2,1)} %tokens_ref, f32[1,4096]{1,0:T(1,128)} %bitcast.155), custom_call_target="tpu_custom_call" | custom-call | tf_op jit(solution)/shard_map/norm/pallas_call | solution.py:392
  44.6 5.8 %all-to-all-start = ((bf16[4,192,256]{2,1,0:T(8,128)(2,1)}), bf16[4,192,256]{2,1,0:T(8,128)(2,1)S(1)}, u32[]{:S(2)}, u32[]{:S(2)}) async-start(bf16[4,192,256]{2,1,0:T(8,128)(2,1)} %broadcast_in_dim.262), calls=%async_computation | async-start | bytes 786432 | tf_op jit(solution)/shard_map/all_to_all | solution.py:402
  62.6 2.8 %collective-permute-done.5 = bf16[192,2048]{1,0:T(8,128)(2,1)S(1)} collective-permute-done((bf16[192,2048]{1,0:T(8,128)(2,1)}, bf16[192,2048]{1,0:T(8,128)(2,1)S(1)}, u32[]{:S(2)}, u32[]{:S(2)}) %collective-permute-start.5) | collective-permute-done | bytes 786464 | tf_op jit(solution)/shard_map/ppermute | solution.py:400
  66.6 4.5 %all-to-all-done = bf16[4,192,256]{2,1,0:T(8,128)(2,1)S(1)} async-done(((bf16[4,192,256]{2,1,0:T(8,128)(2,1)}), bf16[4,192,256]{2,1,0:T(8,128)(2,1)S(1)}, u32[]{:S(2)}, u32[]{:S(2)}) %all-to-all-start) | async-done | bytes 393248 | tf_op jit(solution)/shard_map/all_to_all | solution.py:402
  71.9 16.1 %all-gather.5.cloned.1.call-done = bf16[32,192,256]{2,1,0:T(8,128)(2,1)} async-done(((bf16[4,192,256]{2,1,0:T(8,128)(2,1)}), bf16[32,192,256]{2,1,0:T(8,128)(2,1)}) %all-gather.5.cloned.1.call-update) | async-done | bytes 3145744 | tf_op jit(solution)/shard_map/all_gather | solution.py:386
  87.9 4.9 %project.1 = (f32[192,768]{1,0:T(8,128)}, f32[192,768]{1,0:T(8,128)}) custom-call(bf16[192,2048]{1,0:T(8,128)(2,1)} %get-tuple-element.61.keep_ref, bf16[192,2048]{1,0:T(8,128)(2,1)} %get-tuple-element.116.send_ref, bf16[8,4,192,256]{3,2,1,0:T(8,128)(2,1)} %bitcast.102), custom_call_target="tpu_custom_call" | custom-call | tf_op jit(solution)/shard_map/project/pallas_call | solution.py:515
  92.8 2.8 %collective-permute-start.7 = (f32[192,768]{1,0:T(8,128)}, f32[192,768]{1,0:T(8,128)S(1)}, u32[]{:S(2)}, u32[]{:S(2)}) collective-permute-start(f32[192,768]{1,0:T(8,128)} %get-tuple-element.63), channel_id=1, source_target_pairs={{0,1},{1,0},{2,3},{3,2},{4,5},{5,4},{6,7},{7,6},{8,9},{9,8},{10,11... | collective-permute-start | bytes 1769480 | tf_op jit(solution)/shard_map/ppermute | solution.py:527
  98.2 4.4 %first.1 = (bf16[192,256]{1,0:T(8,128)(2,1)}, bf16[192,256]{1,0:T(8,128)(2,1)}, f32[192,1024]{1,0:T(8,128)}, f32[192,1024]{1,0:T(8,128)}, f32[8,16,128]{2,1,0:T(8,128)}) custom-call(f32[192,768]{1,0:T(8,128)} %get-tuple-element.62.kept_ref, f32[192,768]{1,0:T(8,128)} %copy-done.8, bf16[256,1024]{1,0:T(8,128)(2,1)} %fusion.drive_real_ref, ...), custom_call_target="tpu_custom_call" | custom-call | tf_op jit(solution)/shard_map/first/pallas_call | solution.py:528
  102.6 7.2 %all-to-all-start.1 = ((f32[8,16,128]{2,1,0:T(8,128)}), f32[8,16,128]{2,1,0:T(8,128)S(1)}, u32[]{:S(2)}, u32[]{:S(2)}) async-start(f32[8,16,128]{2,1,0:T(8,128)} %get-tuple-element.68), calls=%async_computation.1 | async-start | bytes 131072 | tf_op jit(solution)/shard_map/all_to_all | solution.py:546
  110.5 4.4 %collective-permute-start.8 = (bf16[32,256]{1,0:T(8,128)(2,1)S(1)}, bf16[32,256]{1,0:T(8,128)(2,1)S(1)}, u32[]{:S(2)}, u32[]{:S(2)}) collective-permute-start(bf16[32,256]{1,0:T(8,128)(2,1)S(1)} %slice.103), channel_id=1, source_target_pairs={{0,1},{1,16},{16,17},{17,32},{32,33},{33,48},{48,49},{49,64},{64,6... | collective-permute-start | bytes 49160 | tf_op jit(solution)/shard_map/ppermute | solution.py:543
  117.5 4.3 %collective-permute-start.11 = (bf16[192,256]{1,0:T(8,128)(2,1)S(1)}, bf16[192,256]{1,0:T(8,128)(2,1)S(1)}, u32[]{:S(2)}, u32[]{:S(2)}) collective-permute-start(bf16[192,256]{1,0:T(8,128)(2,1)S(1)} %conv.1.refs_0_), channel_id=1, source_target_pairs={{0,6},{2,0},{4,2},{6,4},{1,7},{3,1},{5,3},{7,5},{8,14},{10,8},{12,... | collective-permute-start | bytes 294920 | tf_op jit(solution)/shard_map/ppermute | solution.py:562
  132.0 3.7 %all-to-all-start.2 = ((f32[8,16,128]{2,1,0:T(8,128)}), f32[8,16,128]{2,1,0:T(8,128)S(1)}, u32[]{:S(2)}, u32[]{:S(2)}) async-start(f32[8,16,128]{2,1,0:T(8,128)} %row.1), calls=%async_computation.2 | async-start | bytes 131072 | tf_op jit(solution)/shard_map/all_to_all | solution.py:567
  136.3 6.7 %all-to-all-done.2.ends_of_rows_ref = f32[8,16,128]{2,1,0:T(8,128)S(1)} async-done(((f32[8,16,128]{2,1,0:T(8,128)}), f32[8,16,128]{2,1,0:T(8,128)S(1)}, u32[]{:S(2)}, u32[]{:S(2)}) %all-to-all-start.2) | async-done | bytes 65568 | tf_op jit(solution)/shard_map/all_to_all | solution.py:567
  143.6 3.8 %second.1 = (bf16[8,192,256]{2,1,0:T(8,128)(2,1)}, f32[16,128]{1,0:T(8,128)}) custom-call(f32[8,16,128]{2,1,0:T(8,128)} %copy-done.7, f32[8,16,128]{2,1,0:T(8,128)} %get-tuple-element.72.lead_ref, f32[8,16,128]{2,1,0:T(8,128)} %copy-done.10, f32[8,16,128]{2,1,0:T(8,128)} %get-tuple-element.74.lead_rows_ref, f32[8,16,128]{2,1,0:T(8,128)} %get-tuple-element.75.tail_rows_ref, ...), custom_call_target="tpu_custom_call" | custom-call | tf_op jit(solution)/shard_map/second/pallas_call | solution.py:571
  147.4 8.7 %collective-permute-start.14 = (bf16[8,4,192,256]{3,2,1,0:T(8,128)(2,1)}, bf16[8,4,192,256]{3,2,1,0:T(8,128)(2,1)}, u32[]{:S(2)}, u32[]{:S(2)}) collective-permute-start(bf16[8,4,192,256]{3,2,1,0:T(8,128)(2,1)} %bitcast.103), channel_id=1, source_target_pairs={{0,1},{1,0},{2,3},{3,2},{4,5},{5,4},{6,7},{7,6},{8,9},{9,8},{10,11... | collective-permute-start | bytes 9437192 | tf_op jit(solution)/shard_map/ppermute | solution.py:589
  156.1 3.6 %all-to-all-start.3 = ((bf16[8,192,256]{2,1,0:T(8,128)(2,1)}), bf16[8,192,256]{2,1,0:T(8,128)(2,1)S(1)}, u32[]{:S(2)}, u32[]{:S(2)}) async-start(bf16[8,192,256]{2,1,0:T(8,128)(2,1)} %get-tuple-element.84), calls=%async_computation.3 | async-start | bytes 1572864 | tf_op jit(solution)/shard_map/all_to_all | solution.py:585
  159.7 3.2 %collective-permute-start.12 = (bf16[4,192,256]{2,1,0:T(8,128)(2,1)S(1)}, bf16[4,192,256]{2,1,0:T(8,128)(2,1)S(1)}, u32[]{:S(2)}, u32[]{:S(2)}) collective-permute-start(bf16[4,192,256]{2,1,0:T(8,128)(2,1)S(1)} %arrange.3.conv_own_ref), channel_id=1, source_target_pairs={{0,8},{8,0},{1,9},{9,1},{2,10},{10,2},{3,11},{11,3},{4,12},{12,4},... | collective-permute-start | bytes 1179656 | tf_op jit(solution)/shard_map/ppermute | solution.py:568
  165.7 14.2 %collective-permute-done.13 = f32[16,128]{1,0:T(8,128)S(1)} collective-permute-done((f32[16,128]{1,0:T(8,128)}, f32[16,128]{1,0:T(8,128)S(1)}, u32[]{:S(2)}, u32[]{:S(2)}) %collective-permute-start.13) | collective-permute-done | bytes 8224 | tf_op jit(solution)/shard_map/ppermute | solution.py:345
  181.0 5.5 %last.1 = bf16[192,512]{1,0:T(8,128)(2,1)} custom-call(s32[2]{0:T(128)} %pad_add_fusion.place_ref, bf16[4,192,256]{2,1,0:T(8,128)(2,1)} %copy-done, bf16[4,192,256]{2,1,0:T(8,128)(2,1)} %copy-done.9, bf16[8,192,256]{2,1,0:T(8,128)(2,1)} %copy-done.4, bf16[8,4,192,256]{3,2,1,0:T(8,128)(2,1)} %bitcast.104, ...), custom_call_target="tpu_custom_call" | custom-call | tf_op jit(solution)/shard_map/last/pallas_call | solution.py:590
  189.1 4.6 %collective-permute-done.15 = bf16[192,512]{1,0:T(8,128)(2,1)S(1)} collective-permute-done((bf16[192,512]{1,0:T(8,128)(2,1)}, bf16[192,512]{1,0:T(8,128)(2,1)S(1)}, u32[]{:S(2)}, u32[]{:S(2)}) %collective-permute-start.15) | collective-permute-done | bytes 196640 | tf_op jit(solution)/shard_map/ppermute | solution.py:345
  (135 shorter events, 55.0 us)
Async XLA Ops:
  7.2 80.8 %all-gather.5.cloned.1.call-start = ((), (), s32[]{:S(2)}) async-start(), calls=%async_computation.4 | async-start | bytes 3538944 | tf_op jit(solution)/shard_map/all_gather | solution.py:386
  8.6 24.4 %collective-permute-start.3 = (bf16[192,256]{1,0:T(8,128)(2,1)}, bf16[192,256]{1,0:T(8,128)(2,1)S(1)}, u32[]{:S(2)}, u32[]{:S(2)}) collective-permute-start(bf16[192,256]{1,0:T(8,128)(2,1)} %pack.2), channel_id=1, source_target_pairs={{0,48},{1,56},{8,49},{9,57},{16,0},{17,8},{24,1},{25,9},{32,16},{3... | collective-permute-start | bytes 294920 | tf_op jit(solution)/shard_map/ppermute | solution.py:372
  15.1 17.9 %collective-permute-start.2 = (bf16[192,256]{1,0:T(8,128)(2,1)}, bf16[192,256]{1,0:T(8,128)(2,1)S(1)}, u32[]{:S(2)}, u32[]{:S(2)}) collective-permute-start(bf16[192,256]{1,0:T(8,128)(2,1)} %pack.2), channel_id=1, source_target_pairs={{0,32},{1,40},{8,33},{9,41},{16,48},{17,56},{24,49},{25,57},{32,0}... | collective-permute-start | bytes 294920 | tf_op jit(solution)/shard_map/ppermute | solution.py:372
  19.2 13.9 %collective-permute-start.1 = (bf16[192,256]{1,0:T(8,128)(2,1)}, bf16[192,256]{1,0:T(8,128)(2,1)S(1)}, u32[]{:S(2)}, u32[]{:S(2)}) collective-permute-start(bf16[192,256]{1,0:T(8,128)(2,1)} %pack.2), channel_id=1, source_target_pairs={{0,16},{1,24},{8,17},{9,25},{16,32},{17,40},{24,33},{25,41},{32,48... | collective-permute-start | bytes 294920 | tf_op jit(solution)/shard_map/ppermute | solution.py:372
  23.2 9.9 %collective-permute-start = (bf16[192,256]{1,0:T(8,128)(2,1)}, bf16[192,256]{1,0:T(8,128)(2,1)S(1)}, u32[]{:S(2)}, u32[]{:S(2)}) collective-permute-start(bf16[192,256]{1,0:T(8,128)(2,1)} %pack.2), channel_id=1, source_target_pairs={{0,0},{1,8},{8,1},{9,9},{16,16},{17,24},{24,17},{25,25},{32,32},{3... | collective-permute-start | bytes 294920 | tf_op jit(solution)/shard_map/ppermute | solution.py:372
  30.3 20.1 %collective-permute-start.6 = (f32[608,128]{1,0:T(8,128)S(1)}, f32[608,128]{1,0:T(8,128)S(1)}, u32[]{:S(2)}, u32[]{:S(2)}) collective-permute-start(f32[608,128]{1,0:T(8,128)S(1)} %concatenate.245), channel_id=1, source_target_pairs={{0,1},{1,0},{2,3},{3,2},{4,5},{5,4},{6,7},{7,6},{8,9},{9,8},{10,11... | collective-permute-start | bytes 933896 | tf_op jit(solution)/shard_map/ppermute | solution.py:421
  35.8 8.0 %collective-permute-start.4 = (bf16[192,256]{1,0:T(8,128)(2,1)}, bf16[192,256]{1,0:T(8,128)(2,1)S(1)}, u32[]{:S(2)}, u32[]{:S(2)}) collective-permute-start(bf16[192,256]{1,0:T(8,128)(2,1)} %pack.3), channel_id=1, source_target_pairs={{0,0},{1,8},{8,1},{9,9},{2,2},{3,10},{10,3},{11,11},{4,4},{5,12},{... | collective-permute-start | bytes 294920 | tf_op jit(solution)/shard_map/ppermute | solution.py:345
  41.9 23.5 %collective-permute-start.5 = (bf16[192,2048]{1,0:T(8,128)(2,1)}, bf16[192,2048]{1,0:T(8,128)(2,1)S(1)}, u32[]{:S(2)}, u32[]{:S(2)}) collective-permute-start(bf16[192,2048]{1,0:T(8,128)(2,1)} %norm.1), channel_id=1, source_target_pairs={{0,8},{8,0},{1,9},{9,1},{2,10},{10,2},{3,11},{11,3},{4,12},{12,4},... | collective-permute-start | bytes 2359304 | tf_op jit(solution)/shard_map/ppermute | solution.py:400
  44.6 26.5 %all-to-all-start = ((bf16[4,192,256]{2,1,0:T(8,128)(2,1)}), bf16[4,192,256]{2,1,0:T(8,128)(2,1)S(1)}, u32[]{:S(2)}, u32[]{:S(2)}) async-start(bf16[4,192,256]{2,1,0:T(8,128)(2,1)} %broadcast_in_dim.262), calls=%async_computation | async-start | bytes 786432 | tf_op jit(solution)/shard_map/all_to_all | solution.py:402
  50.4 96.9 %all-gather.7.cloned.1.call-start = ((), (), s32[]{:S(2)}) async-start(), calls=%async_computation.5 | async-start | bytes 3538944 | tf_op jit(solution)/shard_map/all_gather | solution.py:510
  57.6 7.7 %copy-start.5 = (bf16[192,2048]{1,0:T(8,128)(2,1)S(1)}, bf16[192,2048]{1,0:T(8,128)(2,1)}, u32[]{:S(2)}) copy-start(bf16[192,2048]{1,0:T(8,128)(2,1)} %norm.1) | copy-start | bytes 2359300
  92.8 4.6 %collective-permute-start.7 = (f32[192,768]{1,0:T(8,128)}, f32[192,768]{1,0:T(8,128)S(1)}, u32[]{:S(2)}, u32[]{:S(2)}) collective-permute-start(f32[192,768]{1,0:T(8,128)} %get-tuple-element.63), channel_id=1, source_target_pairs={{0,1},{1,0},{2,3},{3,2},{4,5},{5,4},{6,7},{7,6},{8,9},{9,8},{10,11... | collective-permute-start | bytes 1769480 | tf_op jit(solution)/shard_map/ppermute | solution.py:527
  102.6 24.1 %all-to-all-start.1 = ((f32[8,16,128]{2,1,0:T(8,128)}), f32[8,16,128]{2,1,0:T(8,128)S(1)}, u32[]{:S(2)}, u32[]{:S(2)}) async-start(f32[8,16,128]{2,1,0:T(8,128)} %get-tuple-element.68), calls=%async_computation.1 | async-start | bytes 131072 | tf_op jit(solution)/shard_map/all_to_all | solution.py:546
  110.5 5.3 %collective-permute-start.8 = (bf16[32,256]{1,0:T(8,128)(2,1)S(1)}, bf16[32,256]{1,0:T(8,128)(2,1)S(1)}, u32[]{:S(2)}, u32[]{:S(2)}) collective-permute-start(bf16[32,256]{1,0:T(8,128)(2,1)S(1)} %slice.103), channel_id=1, source_target_pairs={{0,1},{1,16},{16,17},{17,32},{32,33},{33,48},{48,49},{49,64},{64,6... | collective-permute-start | bytes 49160 | tf_op jit(solution)/shard_map/ppermute | solution.py:543
  117.5 11.4 %collective-permute-start.11 = (bf16[192,256]{1,0:T(8,128)(2,1)S(1)}, bf16[192,256]{1,0:T(8,128)(2,1)S(1)}, u32[]{:S(2)}, u32[]{:S(2)}) collective-permute-start(bf16[192,256]{1,0:T(8,128)(2,1)S(1)} %conv.1.refs_0_), channel_id=1, source_target_pairs={{0,6},{2,0},{4,2},{6,4},{1,7},{3,1},{5,3},{7,5},{8,14},{10,8},{12,... | collective-permute-start | bytes 294920 | tf_op jit(solution)/shard_map/ppermute | solution.py:562
  121.7 7.4 %collective-permute-start.10 = (bf16[192,256]{1,0:T(8,128)(2,1)S(1)}, bf16[192,256]{1,0:T(8,128)(2,1)S(1)}, u32[]{:S(2)}, u32[]{:S(2)}) collective-permute-start(bf16[192,256]{1,0:T(8,128)(2,1)S(1)} %conv.1.refs_0_), channel_id=1, source_target_pairs={{0,4},{2,6},{4,0},{6,2},{1,5},{3,7},{5,1},{7,3},{8,12},{10,14},{12... | collective-permute-start | bytes 294920 | tf_op jit(solution)/shard_map/ppermute | solution.py:562
  124.2 7.2 %collective-permute-start.9 = (bf16[192,256]{1,0:T(8,128)(2,1)S(1)}, bf16[192,256]{1,0:T(8,128)(2,1)S(1)}, u32[]{:S(2)}, u32[]{:S(2)}) collective-permute-start(bf16[192,256]{1,0:T(8,128)(2,1)S(1)} %conv.1.refs_0_), channel_id=1, source_target_pairs={{0,2},{2,4},{4,6},{6,0},{1,3},{3,5},{5,7},{7,1},{8,10},{10,12},{12... | collective-permute-start | bytes 294920 | tf_op jit(solution)/shard_map/ppermute | solution.py:562
  132.0 27.7 %copy-start = (bf16[4,192,256]{2,1,0:T(8,128)(2,1)}, bf16[4,192,256]{2,1,0:T(8,128)(2,1)S(1)}, u32[]{:S(2)}) copy-start(bf16[4,192,256]{2,1,0:T(8,128)(2,1)S(1)} %arrange.3.conv_own_ref) | copy-start | bytes 1179652
  132.0 11.0 %all-to-all-start.2 = ((f32[8,16,128]{2,1,0:T(8,128)}), f32[8,16,128]{2,1,0:T(8,128)S(1)}, u32[]{:S(2)}, u32[]{:S(2)}) async-start(f32[8,16,128]{2,1,0:T(8,128)} %row.1), calls=%async_computation.2 | async-start | bytes 131072 | tf_op jit(solution)/shard_map/all_to_all | solution.py:567
  147.4 32.6 %collective-permute-start.14 = (bf16[8,4,192,256]{3,2,1,0:T(8,128)(2,1)}, bf16[8,4,192,256]{3,2,1,0:T(8,128)(2,1)}, u32[]{:S(2)}, u32[]{:S(2)}) collective-permute-start(bf16[8,4,192,256]{3,2,1,0:T(8,128)(2,1)} %bitcast.103), channel_id=1, source_target_pairs={{0,1},{1,0},{2,3},{3,2},{4,5},{5,4},{6,7},{7,6},{8,9},{9,8},{10,11... | collective-permute-start | bytes 9437192 | tf_op jit(solution)/shard_map/ppermute | solution.py:589
  156.1 23.8 %all-to-all-start.3 = ((bf16[8,192,256]{2,1,0:T(8,128)(2,1)}), bf16[8,192,256]{2,1,0:T(8,128)(2,1)S(1)}, u32[]{:S(2)}, u32[]{:S(2)}) async-start(bf16[8,192,256]{2,1,0:T(8,128)(2,1)} %get-tuple-element.84), calls=%async_computation.3 | async-start | bytes 1572864 | tf_op jit(solution)/shard_map/all_to_all | solution.py:585
  159.7 20.2 %collective-permute-start.12 = (bf16[4,192,256]{2,1,0:T(8,128)(2,1)S(1)}, bf16[4,192,256]{2,1,0:T(8,128)(2,1)S(1)}, u32[]{:S(2)}, u32[]{:S(2)}) collective-permute-start(bf16[4,192,256]{2,1,0:T(8,128)(2,1)S(1)} %arrange.3.conv_own_ref), channel_id=1, source_target_pairs={{0,8},{8,0},{1,9},{9,1},{2,10},{10,2},{3,11},{11,3},{4,12},{12,4},... | collective-permute-start | bytes 1179656 | tf_op jit(solution)/shard_map/ppermute | solution.py:568
  162.9 17.0 %collective-permute-start.13 = (f32[16,128]{1,0:T(8,128)}, f32[16,128]{1,0:T(8,128)S(1)}, u32[]{:S(2)}, u32[]{:S(2)}) collective-permute-start(f32[16,128]{1,0:T(8,128)} %get-tuple-element.85), channel_id=1, source_target_pairs={{0,0},{1,8},{8,1},{9,9},{2,2},{3,10},{10,3},{11,11},{4,4},{5,12},{... | collective-permute-start | bytes 24584 | tf_op jit(solution)/shard_map/ppermute | solution.py:345
  186.5 7.2 %collective-permute-start.15 = (bf16[192,512]{1,0:T(8,128)(2,1)}, bf16[192,512]{1,0:T(8,128)(2,1)S(1)}, u32[]{:S(2)}, u32[]{:S(2)}) collective-permute-start(bf16[192,512]{1,0:T(8,128)(2,1)} %last.1), channel_id=1, source_target_pairs={{0,0},{1,8},{8,1},{9,9},{2,2},{3,10},{10,3},{11,11},{4,4},{5,12},{... | collective-permute-start | bytes 589832 | tf_op jit(solution)/shard_map/ppermute | solution.py:345
  (9 other events, 17.5 us)
Sparse Core Ops, SparseCore 0:
  38.6 49.2 all-gather.4
  90.0 46.2 all-gather.6
